TPU v7x, 512 devices: a 4x2x32 block of a 4x8x32 slice. The times are simulated.
512 devices in a mesh: grp: 2 (over y), ep: 64 (over z, core), tp: 4 (over x).
Axes of the slice: x: 4, y: 2, z: 32, core: 2. Of those that a mesh axis runs over, the one named last changes fastest.
The devices are a block of a 4x8x32 slice.
Arguments:
- tokens: bfloat16 [49152, 2048], P(('grp', 'ep'), 'tp'), parts along dimension 0
- group_choice: int32 [49152], P(('grp', 'ep')), parts along dimension 0, may hold values from 0 to 7, as said below
- expert_choice: int32 [49152, 2], P(('grp', 'ep')), parts along dimension 0, may hold values from 0 to 7, as said below
- group_weight: float32 [49152], P(('grp', 'ep')), parts along dimension 0, may hold values from 0.3 to 1
- expert_weight: float32 [49152, 2], P(('grp', 'ep')), parts along dimension 0, may hold values from 0.1 to 1
- norm_gain: float32 [2048], replicated, may hold values from 0.1 to 1.9
- w_gate: bfloat16 [64, 2048, 1024], P('ep', None, 'tp'), may hold values from -0.125 to 0.125
- w_up: bfloat16 [64, 2048, 1024], P('ep', None, 'tp'), may hold values from -0.125 to 0.125
- w_down: bfloat16 [64, 1024, 2048], P('ep', None, 'tp'), may hold values from -0.1875 to 0.1875
Outputs:
- moe_out: bfloat16 [49152, 2048], P(('grp', 'ep'), 'tp'), parts along dimension 0
There are 2 independent parts, one for each index of `grp`. A program takes and returns all parts, laid end to end along the dimension named above; an argument that names none is the same for every part. Nothing has to cross between parts.
Inputs may be any that keep to these rules, and one draw needn't show every extreme that they name: `group_choice`: group of each token, 0 to 7; within each aligned block of 384 tokens (the tokens of one index of ep) every group is chosen by the same number of tokens. `expert_choice`: a token's two entries differ; within each aligned block of 384 tokens no expert (group with entry) is named by more than 18 tokens, and in every block one expert of each group, the same one in all blocks, is named by exactly 18 tokens.
All inputs are finite; a program needn't handle non-finite values.
Results may differ from a plain program's by a relative error of at most 0.0071.
Values may be sent and summed in bfloat16 or wider, within the bound.
No kernel may reach another device: no remote copies, remote signals or barrier semaphores. Data moves between devices by JAX's collectives and lax.ppermute only.
A program may use at most 64 MiB of HBM per device.

v0:
```python
import jax
import jax.numpy as jnp
from jax import lax
from jax.sharding import Mesh
from jax.sharding import PartitionSpec as P


GROUP_SIZE = 8
TILE = 8
EP = ("g", "m")
GRP_EP = ("grp", "g", "m")
BLOCK = ("tp", "m")


def exchange(array, axis):
    return lax.all_to_all(array, axis, 0, 0, tiled=True)


def shifted(array, axis, by):
    length = lax.axis_size(axis)
    return lax.ppermute(array, axis, [(a, (a + by) % length) for a in range(length)])


def up_to(length, tile):
    return -(-length // tile) * tile


def around(array, axis):
    one = shifted(array, axis, 3)
    three = shifted(array, axis, 1)
    half = array.shape[0] // 2
    top = shifted(one[:half], axis, 3)
    bottom = shifted(three[half:], axis, 1)
    return [(array,), (one,), (top, bottom), (three,)]


def dot(a, b):
    return jnp.dot(a, b, preferred_element_type=jnp.float32)


def dot_parts(a, parts):
    total, at = None, 0
    for part in parts:
        product = dot(a[:, at : at + part.shape[0]], part)
        total = product if total is None else total + product
        at += part.shape[0]
    return total


def layer(
    tokens,
    group_choice,
    expert_choice,
    group_weight,
    expert_weight,
    norm_gain,
    w_gate,
    w_up,
    w_down,
):
    tok_rows, piece_width = tokens.shape
    groups = lax.axis_size("g")
    members = lax.axis_size("m")
    tp_count = lax.axis_size("tp")
    me = lax.axis_index("tp")
    per_group = tok_rows // groups
    mean_load = 2 * tok_rows // (groups * members)
    capacity = mean_load + min(mean_load // 2, per_group - mean_load)
    model_width = norm_gain.shape[0]
    units = w_gate.shape[2]
    width = per_group + TILE

    fused = jnp.concatenate([w_gate[0], w_up[0]], 1)
    ring_in = around(fused, "tp")
    ring_out = around(w_down[0], "tp")

    values = tokens.astype(jnp.float32)
    own_squares = jnp.sum(values * values, -1)
    all_squares = exchange(jnp.broadcast_to(own_squares[None, None], (tp_count, 1, tok_rows)), "tp")
    all_squares = jnp.sum(all_squares, (0, 1))
    inv_rms = lax.rsqrt(all_squares / model_width + 1e-06)
    gain_piece = lax.dynamic_slice_in_dim(norm_gain, me * piece_width, piece_width, 0)

    in_group = group_choice[:, None] == jnp.arange(groups, dtype=jnp.int32)[None, :]
    before = jnp.tril(jnp.ones((tok_rows, tok_rows), jnp.bfloat16), -1)
    ranks = dot(before, in_group.astype(jnp.bfloat16))
    rank = jnp.sum(jnp.where(in_group, ranks, 0.0), 1).astype(jnp.int32)

    mixing = group_weight[:, None] * expert_weight / jnp.sum(expert_weight, -1, keepdims=True)
    coarse = lax.reduce_precision(mixing, 8, 7)
    facts = [expert_choice[:, 0].astype(jnp.float32), expert_choice[:, 1].astype(jnp.float32)]
    facts += [coarse[:, 0], coarse[:, 1]]
    facts += [mixing[:, 0] - coarse[:, 0], mixing[:, 1] - coarse[:, 1]]
    lines = jnp.arange(groups * width, dtype=jnp.int32)
    line_fact = (lines % width - per_group)[:, None]
    spoken = jnp.zeros((groups * width, tok_rows), jnp.float32)
    for i, fact in enumerate(facts):
        spoken = jnp.where(line_fact == i, fact[None, :], spoken)
    spoken = jnp.where((lines // width)[:, None] == group_choice[None, :], spoken, 0.0)
    columns = rank[:, None] == jnp.arange(piece_width, dtype=jnp.int32)[None, :]
    told = dot(spoken.astype(jnp.bfloat16), columns.astype(jnp.bfloat16)).astype(jnp.bfloat16)

    normed = (values * inv_rms[:, None] * gain_piece[None, :]).astype(jnp.bfloat16)
    seating = lines[:, None] == (group_choice * width + rank)[None, :]
    seated = (dot(seating.astype(jnp.bfloat16), normed) + told.astype(jnp.float32)).astype(
        jnp.bfloat16
    )
    landed = exchange(seated.reshape(groups, width, piece_width), "g")

    heard = landed[:, per_group:, :width].astype(jnp.float32)
    choices = [heard[:, k].astype(jnp.int32) for k in range(2)]
    shares = [heard[:, 2 + k] + heard[:, 4 + k] for k in range(2)]
    experts = jnp.arange(members, dtype=jnp.int32)[None, :, None]
    inside = jnp.arange(width, dtype=jnp.int32)[None, :] < per_group
    chosen = [(choices[k][:, None, :] == experts) & inside[:, None, :] for k in range(2)]
    named = (chosen[0] | chosen[1]).astype(jnp.bfloat16).reshape(groups * members, width)
    after = jnp.triu(jnp.ones((width, width), jnp.bfloat16), 1)
    earlier = dot(named, after).reshape(groups, members, width)
    sources = groups // tp_count
    slots = sources * capacity
    depth = up_to(slots, TILE)
    block = jnp.arange(groups, dtype=jnp.int32)[:, None]
    targets = []
    for k in range(2):
        seat = jnp.sum(jnp.where(chosen[k], earlier, 0.0), 1).astype(jnp.int32)
        place = (block // sources * members + choices[k]) * depth
        place = place + block % sources * capacity + seat
        targets.append(jnp.where(inside, place, -1))
    places = jnp.arange(tp_count * members * depth, dtype=jnp.int32)
    flat = [t.reshape(-1) for t in targets]
    spread = (places[:, None] == flat[0][None, :]) | (places[:, None] == flat[1][None, :])
    buffer = dot(
        spread.astype(jnp.bfloat16), landed.reshape(groups * width, piece_width)
    ).astype(jnp.bfloat16)

    rows = exchange(buffer.reshape(tp_count * members, depth, piece_width), BLOCK)
    rows = rows.reshape(tp_count, members * depth, piece_width)
    rows = jnp.concatenate([rows[t] for t in range(tp_count)], 1)
    hidden = []
    for parts in ring_in:
        both = dot_parts(rows, parts)
        hidden.append((jax.nn.silu(both[:, :units]) * both[:, units:]).astype(jnp.bfloat16))
    start = lax.rem(tp_count - me, tp_count)
    hidden = lax.dynamic_slice_in_dim(
        jnp.concatenate(hidden + hidden[:-1], 1), start * units, tp_count * units, 1
    )
    results = [dot_parts(hidden, parts).astype(jnp.bfloat16) for parts in ring_out]
    results = lax.dynamic_slice_in_dim(jnp.stack(results + results[:-1]), start, tp_count, 0)

    returned = exchange(results.reshape(tp_count * members, depth, piece_width), BLOCK)
    returned = returned.reshape(-1, piece_width)
    combined = jnp.zeros((tok_rows, piece_width), jnp.float32)
    for k in range(2):
        back = targets[k][:, :per_group].reshape(-1)
        share = shares[k][:, :per_group].reshape(-1)
        picker = (back[:, None] == places[None, :]).astype(jnp.bfloat16)
        combined = combined + share[:, None] * dot(picker, returned)
    combined = combined.astype(jnp.bfloat16)
    home = exchange(combined.reshape(groups, per_group, piece_width), "g")
    home = home.reshape(tok_rows, piece_width)
    here = lax.axis_index("g")
    seats = jnp.arange(per_group, dtype=jnp.int32)[None, :]
    stayed = (group_choice == here)[:, None] & (rank[:, None] == seats)
    own = lax.dynamic_slice_in_dim(combined, here * per_group, per_group, 0)
    kept = dot(stayed.astype(jnp.bfloat16), own)
    slot = jnp.where(group_choice == here, -1, group_choice * per_group + rank)
    unseating = slot[:, None] == jnp.arange(tok_rows, dtype=jnp.int32)[None, :]
    return (dot(unseating.astype(jnp.bfloat16), home) + kept).astype(jnp.bfloat16)


def solution(mesh):
    groups = mesh.shape["ep"] // GROUP_SIZE
    split = Mesh(
        mesh.devices.reshape(mesh.shape["grp"], groups, GROUP_SIZE, mesh.shape["tp"]),
        ("grp", "g", "m", "tp"),
    )
    placed = (
        P(GRP_EP, "tp"),
        P(GRP_EP),
        P(GRP_EP, None),
        P(GRP_EP),
        P(GRP_EP, None),
        P(),
        P(EP, None, "tp"),
        P(EP, None, "tp"),
        P(EP, None, "tp"),
    )
    return jax.shard_map(
        layer, mesh=split, in_specs=placed, out_specs=P(GRP_EP, "tp"), check_vma=False
    )
```

profile of v0, /device:TPU:33, one launch (start us, length us, event | category | flops | bytes accessed | tf_op | source)
XLA Modules:
  0.0 364.2 jit_solution(643755825032448507)
XLA Ops:
  1.8 5.2 %all-to-all-start = ((f32[4,1,384]{2,1,0:T(1,128)}), f32[4,1,384]{2,1,0:T(1,128)S(1)}, u32[]{:S(2)}, u32[]{:S(2)}) async-start(f32[4,1,384]{2,1,0:T(1,128)} %broadcast_in_dim.167), calls=%async_computation | async-start | bytes 12288 | tf_op jit(solution)/shard_map/all_to_all | solution.py:16
  14.1 43.2 %all-to-all-start.1 = ((bf16[8,56,512]{2,1,0:T(8,128)(2,1)}), bf16[8,56,512]{2,1,0:T(8,128)(2,1)S(1)}, u32[]{:S(2)}, u32[]{:S(2)}) async-start(bf16[8,56,512]{2,1,0:T(8,128)(2,1)} %bitcast), calls=%async_computation.1 | async-start | bytes 917504 | tf_op jit(solution)/shard_map/all_to_all | solution.py:16
  57.7 32.4 %all-to-all-done.1 = bf16[8,56,512]{2,1,0:T(8,128)(2,1)S(1)} async-done(((bf16[8,56,512]{2,1,0:T(8,128)(2,1)}), bf16[8,56,512]{2,1,0:T(8,128)(2,1)S(1)}, u32[]{:S(2)}, u32[]{:S(2)}) %all-to-all-start.1) | async-done | bytes 458784 | tf_op jit(solution)/shard_map/all_to_all | solution.py:16
  90.7 2.0 convolution_convert_fusion
  92.7 33.7 %all-to-all-start.2 = ((bf16[32,40,512]{2,1,0:T(8,128)(2,1)}), bf16[32,40,512]{2,1,0:T(8,128)(2,1)S(1)}, u32[]{:S(2)}, u32[]{:S(2)}) async-start(bf16[32,40,512]{2,1,0:T(8,128)(2,1)} %bitcast.6), calls=%async_computation.2 | async-start | bytes 2621440 | tf_op jit(solution)/shard_map/all_to_all | solution.py:16
  127.9 3.3 collective-permute-start.2
  131.2 3.3 collective-permute-start
  134.5 2.0 collective-permute-start.6
  136.5 4.5 %collective-permute-start.4 = (bf16[1024,512]{1,0:T(8,128)(2,1)}, bf16[1024,512]{1,0:T(8,128)(2,1)S(1)}, u32[]{:S(2)}, u32[]{:S(2)}) collective-permute-start(bf16[1024,512]{1,0:T(8,128)(2,1)} %bitcast.13), channel_id=1, source_target_pairs={{0,3},{1,0},{2,1},{3,2},{4,7},{5,4},{6,5},{7,6},{8,11},{9,8},{10,9... | collective-permute-start | bytes 3145736 | tf_op jit(solution)/shard_map/ppermute | solution.py:21
  141.1 70.2 %collective-permute-done.6 = bf16[1024,512]{1,0:T(8,128)(2,1)S(1)} collective-permute-done((bf16[1024,512]{1,0:T(8,128)(2,1)}, bf16[1024,512]{1,0:T(8,128)(2,1)S(1)}, u32[]{:S(2)}, u32[]{:S(2)}) %collective-permute-start.6) | collective-permute-done | bytes 1048608 | tf_op jit(solution)/shard_map/ppermute | solution.py:21
  212.1 1.9 collective-permute-start.7
  214.9 4.6 %collective-permute-start.5 = (bf16[512,512]{1,0:T(8,128)(2,1)}, bf16[512,512]{1,0:T(8,128)(2,1)}, u32[]{:S(2)}, u32[]{:S(2)}) collective-permute-start(bf16[512,512]{1,0:T(8,128)(2,1)} %slice.173), channel_id=1, source_target_pairs={{0,3},{1,0},{2,1},{3,2},{4,7},{5,4},{6,5},{7,6},{8,11},{9,8},{10,9... | collective-permute-start | bytes 1572872 | tf_op jit(solution)/shard_map/ppermute | solution.py:21
  219.5 2.4 slice.168
  221.9 1.9 collective-permute-start.3
  223.9 2.3 slice.167
  226.1 4.6 %collective-permute-start.1 = (bf16[1024,512]{1,0:T(8,128)(2,1)}, bf16[1024,512]{1,0:T(8,128)(2,1)S(1)}, u32[]{:S(2)}, u32[]{:S(2)}) collective-permute-start(bf16[1024,512]{1,0:T(8,128)(2,1)} %slice.167), channel_id=1, source_target_pairs={{0,3},{1,0},{2,1},{3,2},{4,7},{5,4},{6,5},{7,6},{8,11},{9,8},{10,9... | collective-permute-start | bytes 3145736 | tf_op jit(solution)/shard_map/ppermute | solution.py:21
  233.2 2.4 fusion.118
  235.8 15.0 %collective-permute-done.3 = bf16[1024,512]{1,0:T(8,128)(2,1)} collective-permute-done((bf16[1024,512]{1,0:T(8,128)(2,1)}, bf16[1024,512]{1,0:T(8,128)(2,1)}, u32[]{:S(2)}, u32[]{:S(2)}) %collective-permute-start.3) | collective-permute-done | bytes 1048608 | tf_op jit(solution)/shard_map/ppermute | solution.py:21
  253.1 2.4 fusion.117
  262.6 10.0 %all-to-all-start.3 = ((bf16[32,40,512]{2,1,0:T(8,128)(2,1)}), bf16[32,40,512]{2,1,0:T(8,128)(2,1)S(1)}, u32[]{:S(2)}, u32[]{:S(2)}) async-start(bf16[32,40,512]{2,1,0:T(8,128)(2,1)} %bitcast.18), calls=%async_computation.3 | async-start | bytes 2621440 | tf_op jit(solution)/shard_map/all_to_all | solution.py:16
  273.0 32.8 %all-to-all-done.3 = bf16[32,40,512]{2,1,0:T(8,128)(2,1)S(1)} async-done(((bf16[32,40,512]{2,1,0:T(8,128)(2,1)}), bf16[32,40,512]{2,1,0:T(8,128)(2,1)S(1)}, u32[]{:S(2)}, u32[]{:S(2)}) %all-to-all-start.3) | async-done | bytes 1310752 | tf_op jit(solution)/shard_map/all_to_all | solution.py:16
  308.0 3.7 %all-to-all-start.4 = ((bf16[8,48,512]{2,1,0:T(8,128)(2,1)}), bf16[8,48,512]{2,1,0:T(8,128)(2,1)S(1)}, u32[]{:S(2)}, u32[]{:S(2)}) async-start(bf16[8,48,512]{2,1,0:T(8,128)(2,1)} %bitcast.21), calls=%async_computation.4 | async-start | bytes 786432 | tf_op jit(solution)/shard_map/all_to_all | solution.py:16
  311.7 50.3 %all-to-all-done.4 = bf16[8,48,512]{2,1,0:T(8,128)(2,1)S(1)} async-done(((bf16[8,48,512]{2,1,0:T(8,128)(2,1)}), bf16[8,48,512]{2,1,0:T(8,128)(2,1)S(1)}, u32[]{:S(2)}, u32[]{:S(2)}) %all-to-all-start.4) | async-done | bytes 393248 | tf_op jit(solution)/shard_map/all_to_all | solution.py:16
  362.3 1.9 fusion.11
  (98 shorter events, 27.7 us)
Async XLA Ops:
  1.8 10.2 %copy-start.7 = (s32[384]{0:T(512)S(1)}, s32[384]{0:T(512)}, u32[]{:S(2)}) copy-start(s32[384]{0:T(512)} %param.10) | copy-start | bytes 4612
  1.8 11.0 %all-to-all-start = ((f32[4,1,384]{2,1,0:T(1,128)}), f32[4,1,384]{2,1,0:T(1,128)S(1)}, u32[]{:S(2)}, u32[]{:S(2)}) async-start(f32[4,1,384]{2,1,0:T(1,128)} %broadcast_in_dim.167), calls=%async_computation | async-start | bytes 12288 | tf_op jit(solution)/shard_map/all_to_all | solution.py:16
  7.1 5.7 %copy-start = (bf16[384,512]{1,0:T(8,128)(2,1)S(1)}, bf16[384,512]{1,0:T(8,128)(2,1)}, u32[]{:S(2)}) copy-start(bf16[384,512]{1,0:T(8,128)(2,1)} %param.9) | copy-start | bytes 1179652
  14.1 76.0 %all-to-all-start.1 = ((bf16[8,56,512]{2,1,0:T(8,128)(2,1)}), bf16[8,56,512]{2,1,0:T(8,128)(2,1)S(1)}, u32[]{:S(2)}, u32[]{:S(2)}) async-start(bf16[8,56,512]{2,1,0:T(8,128)(2,1)} %bitcast), calls=%async_computation.1 | async-start | bytes 917504 | tf_op jit(solution)/shard_map/all_to_all | solution.py:16
  92.7 33.7 %copy-start.1 = (bf16[1,2048,256]{2,1,0:T(8,128)(2,1)S(1)}, bf16[1,2048,256]{2,1,0:T(8,128)(2,1)}, u32[]{:S(2)}) copy-start(bf16[1,2048,256]{2,1,0:T(8,128)(2,1)} %param.16) | copy-start | bytes 3145732
  92.7 33.7 %copy-start.3 = (bf16[1,2048,256]{2,1,0:T(8,128)(2,1)S(1)}, bf16[1,2048,256]{2,1,0:T(8,128)(2,1)}, u32[]{:S(2)}) copy-start(bf16[1,2048,256]{2,1,0:T(8,128)(2,1)} %param.15) | copy-start | bytes 3145732
  92.7 138.1 %all-to-all-start.2 = ((bf16[32,40,512]{2,1,0:T(8,128)(2,1)}), bf16[32,40,512]{2,1,0:T(8,128)(2,1)S(1)}, u32[]{:S(2)}, u32[]{:S(2)}) async-start(bf16[32,40,512]{2,1,0:T(8,128)(2,1)} %bitcast.6), calls=%async_computation.2 | async-start | bytes 2621440 | tf_op jit(solution)/shard_map/all_to_all | solution.py:16
  127.9 91.7 %collective-permute-start.2 = (bf16[2048,512]{1,0:T(8,128)(2,1)}, bf16[2048,512]{1,0:T(8,128)(2,1)}, u32[]{:S(2)}, u32[]{:S(2)}) collective-permute-start(bf16[2048,512]{1,0:T(8,128)(2,1)} %pad_maximum_fusion), channel_id=1, source_target_pairs={{0,1},{1,2},{2,3},{3,0},{4,5},{5,6},{6,7},{7,4},{8,9},{9,10},{10,1... | collective-permute-start | bytes 6291464 | tf_op jit(solution)/shard_map/ppermute | solution.py:21
  131.2 92.7 %collective-permute-start = (bf16[2048,512]{1,0:T(8,128)(2,1)}, bf16[2048,512]{1,0:T(8,128)(2,1)}, u32[]{:S(2)}, u32[]{:S(2)}) collective-permute-start(bf16[2048,512]{1,0:T(8,128)(2,1)} %pad_maximum_fusion), channel_id=1, source_target_pairs={{0,3},{1,0},{2,1},{3,2},{4,7},{5,4},{6,5},{7,6},{8,11},{9,8},{10,9... | collective-permute-start | bytes 6291464 | tf_op jit(solution)/shard_map/ppermute | solution.py:21
  134.5 76.8 %collective-permute-start.6 = (bf16[1024,512]{1,0:T(8,128)(2,1)}, bf16[1024,512]{1,0:T(8,128)(2,1)S(1)}, u32[]{:S(2)}, u32[]{:S(2)}) collective-permute-start(bf16[1024,512]{1,0:T(8,128)(2,1)} %bitcast.13), channel_id=1, source_target_pairs={{0,1},{1,2},{2,3},{3,0},{4,5},{5,6},{6,7},{7,4},{8,9},{9,10},{10,1... | collective-permute-start | bytes 3145736 | tf_op jit(solution)/shard_map/ppermute | solution.py:21
  136.5 77.6 %collective-permute-start.4 = (bf16[1024,512]{1,0:T(8,128)(2,1)}, bf16[1024,512]{1,0:T(8,128)(2,1)S(1)}, u32[]{:S(2)}, u32[]{:S(2)}) collective-permute-start(bf16[1024,512]{1,0:T(8,128)(2,1)} %bitcast.13), channel_id=1, source_target_pairs={{0,3},{1,0},{2,1},{3,2},{4,7},{5,4},{6,5},{7,6},{8,11},{9,8},{10,9... | collective-permute-start | bytes 3145736 | tf_op jit(solution)/shard_map/ppermute | solution.py:21
  211.3 10.6 %copy-start.5 = (bf16[1024,512]{1,0:T(8,128)(2,1)}, bf16[1024,512]{1,0:T(8,128)(2,1)S(1)}, u32[]{:S(2)}) copy-start(bf16[1024,512]{1,0:T(8,128)(2,1)S(1)} %collective-permute-done.6) | copy-start | bytes 3145732
  212.1 43.6 %collective-permute-start.7 = (bf16[512,512]{1,0:T(8,128)(2,1)}, bf16[512,512]{1,0:T(8,128)(2,1)}, u32[]{:S(2)}, u32[]{:S(2)}) collective-permute-start(bf16[512,512]{1,0:T(8,128)(2,1)} %slice.174), channel_id=1, source_target_pairs={{0,1},{1,2},{2,3},{3,0},{4,5},{5,6},{6,7},{7,4},{8,9},{9,10},{10,1... | collective-permute-start | bytes 1572872 | tf_op jit(solution)/shard_map/ppermute | solution.py:21
  214.9 44.4 %collective-permute-start.5 = (bf16[512,512]{1,0:T(8,128)(2,1)}, bf16[512,512]{1,0:T(8,128)(2,1)}, u32[]{:S(2)}, u32[]{:S(2)}) collective-permute-start(bf16[512,512]{1,0:T(8,128)(2,1)} %slice.173), channel_id=1, source_target_pairs={{0,3},{1,0},{2,1},{3,2},{4,7},{5,4},{6,5},{7,6},{8,11},{9,8},{10,9... | collective-permute-start | bytes 1572872 | tf_op jit(solution)/shard_map/ppermute | solution.py:21
  221.9 28.8 %collective-permute-start.3 = (bf16[1024,512]{1,0:T(8,128)(2,1)}, bf16[1024,512]{1,0:T(8,128)(2,1)}, u32[]{:S(2)}, u32[]{:S(2)}) collective-permute-start(bf16[1024,512]{1,0:T(8,128)(2,1)} %slice.168), channel_id=1, source_target_pairs={{0,1},{1,2},{2,3},{3,0},{4,5},{5,6},{6,7},{7,4},{8,9},{9,10},{10,1... | collective-permute-start | bytes 3145736 | tf_op jit(solution)/shard_map/ppermute | solution.py:21
  226.1 26.4 %collective-permute-start.1 = (bf16[1024,512]{1,0:T(8,128)(2,1)}, bf16[1024,512]{1,0:T(8,128)(2,1)S(1)}, u32[]{:S(2)}, u32[]{:S(2)}) collective-permute-start(bf16[1024,512]{1,0:T(8,128)(2,1)} %slice.167), channel_id=1, source_target_pairs={{0,3},{1,0},{2,1},{3,2},{4,7},{5,4},{6,5},{7,6},{8,11},{9,8},{10,9... | collective-permute-start | bytes 3145736 | tf_op jit(solution)/shard_map/ppermute | solution.py:21
  230.7 1.2 copy-start.2
  230.7 1.5 copy-start.4
  258.8 1.9 copy-start.6
  262.6 43.2 %all-to-all-start.3 = ((bf16[32,40,512]{2,1,0:T(8,128)(2,1)}), bf16[32,40,512]{2,1,0:T(8,128)(2,1)S(1)}, u32[]{:S(2)}, u32[]{:S(2)}) async-start(bf16[32,40,512]{2,1,0:T(8,128)(2,1)} %bitcast.18), calls=%async_computation.3 | async-start | bytes 2621440 | tf_op jit(solution)/shard_map/all_to_all | solution.py:16
  308.0 53.9 %all-to-all-start.4 = ((bf16[8,48,512]{2,1,0:T(8,128)(2,1)}), bf16[8,48,512]{2,1,0:T(8,128)(2,1)S(1)}, u32[]{:S(2)}, u32[]{:S(2)}) async-start(bf16[8,48,512]{2,1,0:T(8,128)(2,1)} %bitcast.21), calls=%async_computation.4 | async-start | bytes 786432 | tf_op jit(solution)/shard_map/all_to_all | solution.py:16
where the time goes:
time: 366 us; the launch traced here: 364 us
  waiting for transfers between devices  201 us (55%)
  starting transfers between devices  122 us (33%)
  matrix products  23.9 us (7%)
  local copies, waits for them, and re-layouts  11.6 us (3%)
  other arithmetic  5.53 us (2%)
    all_to_all x5, waiting for transfers between devices, exchange(): return lax.all_to_all(array, axis, 0, 0, tiled=True)  115 us
    all_to_all x5, starting transfers between devices, exchange(): return lax.all_to_all(array, axis, 0, 0, tiled=True)  95.8 us
    ppermute x8, waiting for transfers between devices, shifted(): lax.ppermute(array, axis, [(a, (a + by) % length) for a in range(length)])  85.2 us
    ppermute x8, starting transfers between devices, shifted(): lax.ppermute(array, axis, [(a, (a + by) % length) for a in range(length)])  26.2 us
    dot_general x19, matrix products, dot(): return jnp.dot(a, b, preferred_element_type=jnp.float32)  23.9 us
  transfers between devices with their start and end apart: 13, of which 5 were waited for; matrix products, arithmetic and copies ran while one was open for 7% of the time, Pallas kernels for 0%

commit v1 on v0

--- a/solution.py
+++ b/solution.py
@@ -70,16 +70,8 @@
     units = w_gate.shape[2]
     width = per_group + TILE
 
-    fused = jnp.concatenate([w_gate[0], w_up[0]], 1)
-    ring_in = around(fused, "tp")
     ring_out = around(w_down[0], "tp")
-
-    values = tokens.astype(jnp.float32)
-    own_squares = jnp.sum(values * values, -1)
-    all_squares = exchange(jnp.broadcast_to(own_squares[None, None], (tp_count, 1, tok_rows)), "tp")
-    all_squares = jnp.sum(all_squares, (0, 1))
-    inv_rms = lax.rsqrt(all_squares / model_width + 1e-06)
-    gain_piece = lax.dynamic_slice_in_dim(norm_gain, me * piece_width, piece_width, 0)
+    ring_in = around(jnp.concatenate([w_gate[0], w_up[0]], 1), "tp")
 
     in_group = group_choice[:, None] == jnp.arange(groups, dtype=jnp.int32)[None, :]
     before = jnp.tril(jnp.ones((tok_rows, tok_rows), jnp.bfloat16), -1)
@@ -100,11 +92,9 @@
     columns = rank[:, None] == jnp.arange(piece_width, dtype=jnp.int32)[None, :]
     told = dot(spoken.astype(jnp.bfloat16), columns.astype(jnp.bfloat16)).astype(jnp.bfloat16)
 
-    normed = (values * inv_rms[:, None] * gain_piece[None, :]).astype(jnp.bfloat16)
     seating = lines[:, None] == (group_choice * width + rank)[None, :]
-    seated = (dot(seating.astype(jnp.bfloat16), normed) + told.astype(jnp.float32)).astype(
-        jnp.bfloat16
-    )
+    seated = dot(seating.astype(jnp.bfloat16), tokens) + told.astype(jnp.float32)
+    seated = seated.astype(jnp.bfloat16)
     landed = exchange(seated.reshape(groups, width, piece_width), "g")
 
     heard = landed[:, per_group:, :width].astype(jnp.float32)
@@ -134,18 +124,22 @@
     ).astype(jnp.bfloat16)
 
     rows = exchange(buffer.reshape(tp_count * members, depth, piece_width), BLOCK)
-    rows = rows.reshape(tp_count, members * depth, piece_width)
-    rows = jnp.concatenate([rows[t] for t in range(tp_count)], 1)
-    hidden = []
-    for parts in ring_in:
-        both = dot_parts(rows, parts)
-        hidden.append((jax.nn.silu(both[:, :units]) * both[:, units:]).astype(jnp.bfloat16))
-    start = lax.rem(tp_count - me, tp_count)
-    hidden = lax.dynamic_slice_in_dim(
-        jnp.concatenate(hidden + hidden[:-1], 1), start * units, tp_count * units, 1
-    )
-    results = [dot_parts(hidden, parts).astype(jnp.bfloat16) for parts in ring_out]
-    results = lax.dynamic_slice_in_dim(jnp.stack(results + results[:-1]), start, tp_count, 0)
+    values = rows.reshape(tp_count, members * depth, piece_width).astype(jnp.float32)
+    inv_rms = lax.rsqrt(jnp.sum(values * values, (0, 2)) / model_width + 1e-06)
+    gains = norm_gain.reshape(tp_count, 1, piece_width)
+    normed = (values * inv_rms[None, :, None] * gains).astype(jnp.bfloat16)
+    normed = jnp.concatenate([normed[t] for t in range(tp_count)], 1)
+    hidden = jnp.zeros((members * depth, tp_count * units), jnp.bfloat16)
+    for i, parts in enumerate(ring_in):
+        both = dot_parts(normed, parts)
+        piece = (jax.nn.silu(both[:, :units]) * both[:, units:]).astype(jnp.bfloat16)
+        owner = lax.rem(me + i, tp_count)
+        hidden = lax.dynamic_update_slice_in_dim(hidden, piece, owner * units, 1)
+    results = jnp.zeros((tp_count, members * depth, piece_width), jnp.bfloat16)
+    for i, parts in enumerate(ring_out):
+        piece = dot_parts(hidden, parts).astype(jnp.bfloat16)
+        owner = lax.rem(me + i, tp_count)
+        results = lax.dynamic_update_slice_in_dim(results, piece[None], owner, 0)
 
     returned = exchange(results.reshape(tp_count * members, depth, piece_width), BLOCK)
     returned = returned.reshape(-1, piece_width)

time: 366 us -> 360 us (0.984)
  starting transfers between devices: 122 us -> 116 us
  waiting for transfers between devices: 201 us -> 197 us
    all_to_all x5 -> x4, starting transfers between devices: 95.8 us -> 90 us  [exchange(): return lax.all_to_all(array, axis, 0, 0, tiled=True)]
    all_to_all x5 -> x4, waiting for transfers between devices: 115 us -> 115 us  [exchange(): return lax.all_to_all(array, axis, 0, 0, tiled=True)]
  transfers between devices with their start and end apart: 13 -> 12, of which waited for: 5 -> 5; matrix products, arithmetic and copies ran while one was open for 7% -> 8% of each run, Pallas kernels for 0% -> 0%
where the time goes in v1:
time: 360 us; the launch traced here: 359 us
  waiting for transfers between devices  197 us (55%)
  starting transfers between devices  116 us (32%)
  matrix products  27 us (8%)
  local copies, waits for them, and re-layouts  11.2 us (3%)
  other arithmetic  7.32 us (2%)
    all_to_all x4, waiting for transfers between devices, exchange(): return lax.all_to_all(array, axis, 0, 0, tiled=True)  115 us
    all_to_all x4, starting transfers between devices, exchange(): return lax.all_to_all(array, axis, 0, 0, tiled=True)  90 us
    ppermute x8, waiting for transfers between devices, shifted(): lax.ppermute(array, axis, [(a, (a + by) % length) for a in range(length)])  81.9 us
    dot_general x19, matrix products, dot(): return jnp.dot(a, b, preferred_element_type=jnp.float32)  27 us
    ppermute x8, starting transfers between devices, shifted(): lax.ppermute(array, axis, [(a, (a + by) % length) for a in range(length)])  26.2 us
  transfers between devices with their start and end apart: 12, of which 5 were waited for; matrix products, arithmetic and copies ran while one was open for 8% of the time, Pallas kernels for 0%

profile of v1, /device:TPU:33, one launch (start us, length us, event | category | flops | bytes accessed | tf_op | source)
XLA Modules:
  0.0 359.1 jit_solution(3291657510035690840)
XLA Ops:
  6.8 44.0 %all-to-all-start = ((bf16[8,56,512]{2,1,0:T(8,128)(2,1)}), bf16[8,56,512]{2,1,0:T(8,128)(2,1)S(1)}, u32[]{:S(2)}, u32[]{:S(2)}) async-start(bf16[8,56,512]{2,1,0:T(8,128)(2,1)} %bitcast), calls=%async_computation | async-start | bytes 917504 | tf_op jit(solution)/shard_map/all_to_all | solution.py:16
  51.2 31.9 %all-to-all-done = bf16[8,56,512]{2,1,0:T(8,128)(2,1)S(1)} async-done(((bf16[8,56,512]{2,1,0:T(8,128)(2,1)}), bf16[8,56,512]{2,1,0:T(8,128)(2,1)S(1)}, u32[]{:S(2)}, u32[]{:S(2)}) %all-to-all-start) | async-done | bytes 458784 | tf_op jit(solution)/shard_map/all_to_all | solution.py:16
  83.7 2.0 convolution_convert_fusion
  85.6 34.0 %all-to-all-start.1 = ((bf16[32,40,512]{2,1,0:T(8,128)(2,1)}), bf16[32,40,512]{2,1,0:T(8,128)(2,1)S(1)}, u32[]{:S(2)}, u32[]{:S(2)}) async-start(bf16[32,40,512]{2,1,0:T(8,128)(2,1)} %bitcast.6), calls=%async_computation.1 | async-start | bytes 2621440 | tf_op jit(solution)/shard_map/all_to_all | solution.py:16
  119.7 2.7 pad_maximum_fusion
  122.4 3.3 collective-permute-start.2
  125.7 3.3 collective-permute-start
  129.0 2.0 collective-permute-start.6
  131.0 4.5 %collective-permute-start.4 = (bf16[1024,512]{1,0:T(8,128)(2,1)}, bf16[1024,512]{1,0:T(8,128)(2,1)}, u32[]{:S(2)}, u32[]{:S(2)}) collective-permute-start(bf16[1024,512]{1,0:T(8,128)(2,1)} %bitcast.14), channel_id=1, source_target_pairs={{0,3},{1,0},{2,1},{3,2},{4,7},{5,4},{6,5},{7,6},{8,11},{9,8},{10,9... | collective-permute-start | bytes 3145736 | tf_op jit(solution)/shard_map/ppermute | solution.py:21
  135.7 69.0 %collective-permute-done.6 = bf16[1024,512]{1,0:T(8,128)(2,1)S(1)} collective-permute-done((bf16[1024,512]{1,0:T(8,128)(2,1)}, bf16[1024,512]{1,0:T(8,128)(2,1)S(1)}, u32[]{:S(2)}, u32[]{:S(2)}) %collective-permute-start.6) | collective-permute-done | bytes 1048608 | tf_op jit(solution)/shard_map/ppermute | solution.py:21
  209.4 4.6 %collective-permute-start.5 = (bf16[512,512]{1,0:T(8,128)(2,1)}, bf16[512,512]{1,0:T(8,128)(2,1)}, u32[]{:S(2)}, u32[]{:S(2)}) collective-permute-start(bf16[512,512]{1,0:T(8,128)(2,1)} %slice.170), channel_id=1, source_target_pairs={{0,3},{1,0},{2,1},{3,2},{4,7},{5,4},{6,5},{7,6},{8,11},{9,8},{10,9... | collective-permute-start | bytes 1572872 | tf_op jit(solution)/shard_map/ppermute | solution.py:21
  214.0 2.3 slice.164
  218.2 2.3 slice.163
  220.5 4.6 %collective-permute-start.1 = (bf16[1024,512]{1,0:T(8,128)(2,1)}, bf16[1024,512]{1,0:T(8,128)(2,1)S(1)}, u32[]{:S(2)}, u32[]{:S(2)}) collective-permute-start(bf16[1024,512]{1,0:T(8,128)(2,1)} %slice.163), channel_id=1, source_target_pairs={{0,3},{1,0},{2,1},{3,2},{4,7},{5,4},{6,5},{7,6},{8,11},{9,8},{10,9... | collective-permute-start | bytes 3145736 | tf_op jit(solution)/shard_map/ppermute | solution.py:21
  228.6 2.4 fusion.112
  231.4 12.9 %collective-permute-done.3 = bf16[1024,512]{1,0:T(8,128)(2,1)} collective-permute-done((bf16[1024,512]{1,0:T(8,128)(2,1)}, bf16[1024,512]{1,0:T(8,128)(2,1)}, u32[]{:S(2)}, u32[]{:S(2)}) %collective-permute-start.3) | collective-permute-done | bytes 1048608 | tf_op jit(solution)/shard_map/ppermute | solution.py:21
  246.0 2.4 fusion.111
  250.3 2.5 fusion.19
  253.1 2.6 fusion.21
  255.7 2.1 fusion.17
  259.1 8.4 %all-to-all-start.2 = ((bf16[32,40,512]{2,1,0:T(8,128)(2,1)}), bf16[32,40,512]{2,1,0:T(8,128)(2,1)S(1)}, u32[]{:S(2)}, u32[]{:S(2)}) async-start(bf16[32,40,512]{2,1,0:T(8,128)(2,1)} %bitcast.19), calls=%async_computation.2 | async-start | bytes 2621440 | tf_op jit(solution)/shard_map/all_to_all | solution.py:16
  267.9 32.8 %all-to-all-done.2 = bf16[32,40,512]{2,1,0:T(8,128)(2,1)S(1)} async-done(((bf16[32,40,512]{2,1,0:T(8,128)(2,1)}), bf16[32,40,512]{2,1,0:T(8,128)(2,1)S(1)}, u32[]{:S(2)}, u32[]{:S(2)}) %all-to-all-start.2) | async-done | bytes 1310752 | tf_op jit(solution)/shard_map/all_to_all | solution.py:16
  302.9 3.7 %all-to-all-start.3 = ((bf16[8,48,512]{2,1,0:T(8,128)(2,1)}), bf16[8,48,512]{2,1,0:T(8,128)(2,1)S(1)}, u32[]{:S(2)}, u32[]{:S(2)}) async-start(bf16[8,48,512]{2,1,0:T(8,128)(2,1)} %bitcast.22), calls=%async_computation.3 | async-start | bytes 786432 | tf_op jit(solution)/shard_map/all_to_all | solution.py:16
  306.6 50.2 %all-to-all-done.3 = bf16[8,48,512]{2,1,0:T(8,128)(2,1)S(1)} async-done(((bf16[8,48,512]{2,1,0:T(8,128)(2,1)}), bf16[8,48,512]{2,1,0:T(8,128)(2,1)S(1)}, u32[]{:S(2)}, u32[]{:S(2)}) %all-to-all-start.3) | async-done | bytes 393248 | tf_op jit(solution)/shard_map/all_to_all | solution.py:16
  (93 shorter events, 28.2 us)
Async XLA Ops:
  0.0 5.6 %copy-start = (bf16[384,512]{1,0:T(8,128)(2,1)S(1)}, bf16[384,512]{1,0:T(8,128)(2,1)}, u32[]{:S(2)}) copy-start(bf16[384,512]{1,0:T(8,128)(2,1)} %param.9) | copy-start | bytes 1179652
  6.8 76.3 %all-to-all-start = ((bf16[8,56,512]{2,1,0:T(8,128)(2,1)}), bf16[8,56,512]{2,1,0:T(8,128)(2,1)S(1)}, u32[]{:S(2)}, u32[]{:S(2)}) async-start(bf16[8,56,512]{2,1,0:T(8,128)(2,1)} %bitcast), calls=%async_computation | async-start | bytes 917504 | tf_op jit(solution)/shard_map/all_to_all | solution.py:16
  85.6 34.0 %copy-start.1 = (bf16[1,2048,256]{2,1,0:T(8,128)(2,1)S(1)}, bf16[1,2048,256]{2,1,0:T(8,128)(2,1)}, u32[]{:S(2)}) copy-start(bf16[1,2048,256]{2,1,0:T(8,128)(2,1)} %param.16) | copy-start | bytes 3145732
  85.6 139.4 %all-to-all-start.1 = ((bf16[32,40,512]{2,1,0:T(8,128)(2,1)}), bf16[32,40,512]{2,1,0:T(8,128)(2,1)S(1)}, u32[]{:S(2)}, u32[]{:S(2)}) async-start(bf16[32,40,512]{2,1,0:T(8,128)(2,1)} %bitcast.6), calls=%async_computation.1 | async-start | bytes 2621440 | tf_op jit(solution)/shard_map/all_to_all | solution.py:16
  119.6 16.0 %copy-start.7 = (f32[2048]{0:T(1024)S(1)}, f32[2048]{0:T(1024)}, u32[]{:S(2)}) copy-start(f32[2048]{0:T(1024)} %param.14) | copy-start | bytes 24580
  122.4 91.6 %collective-permute-start.2 = (bf16[2048,512]{1,0:T(8,128)(2,1)}, bf16[2048,512]{1,0:T(8,128)(2,1)}, u32[]{:S(2)}, u32[]{:S(2)}) collective-permute-start(bf16[2048,512]{1,0:T(8,128)(2,1)} %pad_maximum_fusion), channel_id=1, source_target_pairs={{0,1},{1,2},{2,3},{3,0},{4,5},{5,6},{6,7},{7,4},{8,9},{9,10},{10,1... | collective-permute-start | bytes 6291464 | tf_op jit(solution)/shard_map/ppermute | solution.py:21
  125.7 92.5 %collective-permute-start = (bf16[2048,512]{1,0:T(8,128)(2,1)}, bf16[2048,512]{1,0:T(8,128)(2,1)}, u32[]{:S(2)}, u32[]{:S(2)}) collective-permute-start(bf16[2048,512]{1,0:T(8,128)(2,1)} %pad_maximum_fusion), channel_id=1, source_target_pairs={{0,3},{1,0},{2,1},{3,2},{4,7},{5,4},{6,5},{7,6},{8,11},{9,8},{10,9... | collective-permute-start | bytes 6291464 | tf_op jit(solution)/shard_map/ppermute | solution.py:21
  129.0 75.7 %collective-permute-start.6 = (bf16[1024,512]{1,0:T(8,128)(2,1)}, bf16[1024,512]{1,0:T(8,128)(2,1)S(1)}, u32[]{:S(2)}, u32[]{:S(2)}) collective-permute-start(bf16[1024,512]{1,0:T(8,128)(2,1)} %bitcast.14), channel_id=1, source_target_pairs={{0,1},{1,2},{2,3},{3,0},{4,5},{5,6},{6,7},{7,4},{8,9},{9,10},{10,1... | collective-permute-start | bytes 3145736 | tf_op jit(solution)/shard_map/ppermute | solution.py:21
  131.0 76.5 %collective-permute-start.4 = (bf16[1024,512]{1,0:T(8,128)(2,1)}, bf16[1024,512]{1,0:T(8,128)(2,1)}, u32[]{:S(2)}, u32[]{:S(2)}) collective-permute-start(bf16[1024,512]{1,0:T(8,128)(2,1)} %bitcast.14), channel_id=1, source_target_pairs={{0,3},{1,0},{2,1},{3,2},{4,7},{5,4},{6,5},{7,6},{8,11},{9,8},{10,9... | collective-permute-start | bytes 3145736 | tf_op jit(solution)/shard_map/ppermute | solution.py:21
  204.6 11.6 %copy-start.4 = (bf16[1024,512]{1,0:T(8,128)(2,1)}, bf16[1024,512]{1,0:T(8,128)(2,1)S(1)}, u32[]{:S(2)}) copy-start(bf16[1024,512]{1,0:T(8,128)(2,1)S(1)} %collective-permute-done.6) | copy-start | bytes 3145732
  205.6 47.2 %collective-permute-start.7 = (bf16[512,512]{1,0:T(8,128)(2,1)}, bf16[512,512]{1,0:T(8,128)(2,1)S(1)}, u32[]{:S(2)}, u32[]{:S(2)}) collective-permute-start(bf16[512,512]{1,0:T(8,128)(2,1)} %slice.172), channel_id=1, source_target_pairs={{0,1},{1,2},{2,3},{3,0},{4,5},{5,6},{6,7},{7,4},{8,9},{9,10},{10,1... | collective-permute-start | bytes 1572872 | tf_op jit(solution)/shard_map/ppermute | solution.py:21
  209.4 46.3 %collective-permute-start.5 = (bf16[512,512]{1,0:T(8,128)(2,1)}, bf16[512,512]{1,0:T(8,128)(2,1)}, u32[]{:S(2)}, u32[]{:S(2)}) collective-permute-start(bf16[512,512]{1,0:T(8,128)(2,1)} %slice.170), channel_id=1, source_target_pairs={{0,3},{1,0},{2,1},{3,2},{4,7},{5,4},{6,5},{7,6},{8,11},{9,8},{10,9... | collective-permute-start | bytes 1572872 | tf_op jit(solution)/shard_map/ppermute | solution.py:21
  216.3 28.0 %collective-permute-start.3 = (bf16[1024,512]{1,0:T(8,128)(2,1)}, bf16[1024,512]{1,0:T(8,128)(2,1)}, u32[]{:S(2)}, u32[]{:S(2)}) collective-permute-start(bf16[1024,512]{1,0:T(8,128)(2,1)} %slice.164), channel_id=1, source_target_pairs={{0,1},{1,2},{2,3},{3,0},{4,5},{5,6},{6,7},{7,4},{8,9},{9,10},{10,1... | collective-permute-start | bytes 3145736 | tf_op jit(solution)/shard_map/ppermute | solution.py:21
  220.5 27.9 %collective-permute-start.1 = (bf16[1024,512]{1,0:T(8,128)(2,1)}, bf16[1024,512]{1,0:T(8,128)(2,1)S(1)}, u32[]{:S(2)}, u32[]{:S(2)}) collective-permute-start(bf16[1024,512]{1,0:T(8,128)(2,1)} %slice.163), channel_id=1, source_target_pairs={{0,3},{1,0},{2,1},{3,2},{4,7},{5,4},{6,5},{7,6},{8,11},{9,8},{10,9... | collective-permute-start | bytes 3145736 | tf_op jit(solution)/shard_map/ppermute | solution.py:21
  226.2 1.2 copy-start.2
  226.3 1.5 copy-start.3
  253.1 4.7 %copy-start.5 = (bf16[1024,512]{1,0:T(8,128)(2,1)S(1)}, bf16[1024,512]{1,0:T(8,128)(2,1)}, u32[]{:S(2)}) copy-start(bf16[1024,512]{1,0:T(8,128)(2,1)} %copy-done.4) | copy-start | bytes 3145732
  259.1 41.6 %all-to-all-start.2 = ((bf16[32,40,512]{2,1,0:T(8,128)(2,1)}), bf16[32,40,512]{2,1,0:T(8,128)(2,1)S(1)}, u32[]{:S(2)}, u32[]{:S(2)}) async-start(bf16[32,40,512]{2,1,0:T(8,128)(2,1)} %bitcast.19), calls=%async_computation.2 | async-start | bytes 2621440 | tf_op jit(solution)/shard_map/all_to_all | solution.py:16
  301.4 5.1 %copy-start.6 = (s32[384]{0:T(512)S(1)}, s32[384]{0:T(512)}, u32[]{:S(2)}) copy-start(s32[384]{0:T(512)} %param.10) | copy-start | bytes 4612
  302.9 53.9 %all-to-all-start.3 = ((bf16[8,48,512]{2,1,0:T(8,128)(2,1)}), bf16[8,48,512]{2,1,0:T(8,128)(2,1)S(1)}, u32[]{:S(2)}, u32[]{:S(2)}) async-start(bf16[8,48,512]{2,1,0:T(8,128)(2,1)} %bitcast.22), calls=%async_computation.3 | async-start | bytes 786432 | tf_op jit(solution)/shard_map/all_to_all | solution.py:16

commit v2 on v1

--- a/solution.py
+++ b/solution.py
@@ -1,6 +1,8 @@
 import jax
 import jax.numpy as jnp
 from jax import lax
+from jax.experimental import pallas as pl
+from jax.experimental.pallas import tpu as pltpu
 from jax.sharding import Mesh
 from jax.sharding import PartitionSpec as P
 
@@ -38,13 +40,110 @@
     return jnp.dot(a, b, preferred_element_type=jnp.float32)
 
 
-def dot_parts(a, parts):
-    total, at = None, 0
-    for part in parts:
-        product = dot(a[:, at : at + part.shape[0]], part)
-        total = product if total is None else total + product
-        at += part.shape[0]
-    return total
+def fetch(sources, slots, semaphores):
+    copies = [
+        pltpu.make_async_copy(source, slot, semaphores.at[i])
+        for i, (source, slot) in enumerate(zip(sources, slots, strict=True))
+    ]
+    for copy in copies:
+        copy.start()
+    return copies
+
+
+def gated(both, units):
+    gate, up = both[:, :units], both[:, units:]
+    return (gate / (1.0 + jnp.exp(-gate)) * up).astype(jnp.bfloat16)
+
+
+def first_half(gains, given, gate, up, one, three, normed, hidden, rows, *scratch):
+    slots, semaphores = scratch[:-1], scratch[-1]
+    arrived, *copies = fetch((given, gate, up, one, three), (rows, *slots), semaphores)
+    parts, _, width = rows.shape
+    units = gate.shape[1]
+    total = None
+    arrived.wait()
+    for t in range(parts):
+        values = rows[t].astype(jnp.float32)
+        squares = jnp.sum(values * values, -1, keepdims=True)
+        total = squares if total is None else total + squares
+    inv_rms = lax.rsqrt(total / (parts * width) + 1e-06)
+    for t in range(parts):
+        scaled = rows[t].astype(jnp.float32) * inv_rms * gains[t][None, :]
+        normed[:, t * width : (t + 1) * width] = scaled.astype(jnp.bfloat16)
+    copies[0].wait()
+    copies[1].wait()
+    both = jnp.concatenate([dot(normed[...], s[...]) for s in slots[:2]], 1)
+    hidden[0] = gated(both, units)
+    for i in (2, 3):
+        copies[i].wait()
+        hidden[i - 1] = gated(dot(normed[...], slots[i][...]), units)
+
+
+def second_half(me, *refs):
+    sources, results, slots = refs[:9], refs[9], refs[10:19]
+    whole, semaphores = refs[19], refs[20]
+    copies = fetch(sources, slots, semaphores)
+    normed, hidden, in_top, in_bottom, own, one, three, out_top, out_bottom = slots
+    parts, _, _ = results.shape
+    units = hidden.shape[2]
+
+    def owner(offset):
+        return lax.rem(me[0] + offset, parts)
+
+    def place(offset, piece):
+        whole[:, pl.ds(pl.multiple_of(owner(offset) * units, units), units)] = piece
+
+    def halves(whole, top, bottom):
+        half = top.shape[0]
+        return dot(whole[:, :half], top[...]) + dot(whole[:, half:], bottom[...])
+
+    for copy in copies[:4]:
+        copy.wait()
+    for i, offset in enumerate((0, 1, 3)):
+        place(offset, hidden[i])
+    place(2, gated(halves(normed, in_top, in_bottom), units))
+    for copy, slot, offset in zip(copies[4:7], (own, one, three), (0, 1, 3), strict=True):
+        copy.wait()
+        results[owner(offset)] = dot(whole[...], slot[...]).astype(results.dtype)
+    copies[7].wait()
+    copies[8].wait()
+    results[owner(2)] = halves(whole, out_top, out_bottom).astype(results.dtype)
+
+
+def expert(rows, norm_gain, gate, up, ring_in, ring_out, me):
+    parts, count, width = rows.shape
+    units = gate.shape[1]
+    vmem = pl.BlockSpec(memory_space=pltpu.VMEM)
+    hbm = pl.BlockSpec(memory_space=pltpu.HBM)
+    smem = pl.BlockSpec(memory_space=pltpu.SMEM)
+
+    def slots(arrays):
+        return [pltpu.VMEM(a.shape, a.dtype) for a in arrays]
+
+    _, (one,), far, (three,) = ring_in
+    given = [rows, gate, up, one, three]
+    normed, hidden = pl.pallas_call(
+        first_half,
+        out_shape=(
+            jax.ShapeDtypeStruct((count, parts * width), jnp.bfloat16),
+            jax.ShapeDtypeStruct((3, count, units), jnp.bfloat16),
+        ),
+        in_specs=[vmem] + [hbm] * 5,
+        out_specs=(vmem, vmem),
+        scratch_shapes=slots(given) + [pltpu.SemaphoreType.DMA((5,))],
+        name="first_half",
+    )(norm_gain.reshape(parts, width), *given)
+    (own,), (one,), far_out, (three,) = ring_out
+    given = [normed, hidden, *far, own, one, three, *far_out]
+    return pl.pallas_call(
+        second_half,
+        out_shape=jax.ShapeDtypeStruct((parts, count, width), jnp.bfloat16),
+        in_specs=[smem] + [hbm] * 9,
+        out_specs=vmem,
+        scratch_shapes=slots(given)
+        + [pltpu.VMEM((count, parts * units), jnp.bfloat16), pltpu.SemaphoreType.DMA((9,))],
+        name="second_half",
+    )(me.reshape(1), *given)
 
 
 def layer(
@@ -66,12 +165,10 @@
     per_group = tok_rows // groups
     mean_load = 2 * tok_rows // (groups * members)
     capacity = mean_load + min(mean_load // 2, per_group - mean_load)
-    model_width = norm_gain.shape[0]
-    units = w_gate.shape[2]
     width = per_group + TILE
 
+    ring_in = around(jnp.concatenate([w_gate[0], w_up[0]], 1), "tp")
     ring_out = around(w_down[0], "tp")
-    ring_in = around(jnp.concatenate([w_gate[0], w_up[0]], 1), "tp")
 
     in_group = group_choice[:, None] == jnp.arange(groups, dtype=jnp.int32)[None, :]
     before = jnp.tril(jnp.ones((tok_rows, tok_rows), jnp.bfloat16), -1)
@@ -124,22 +221,8 @@
     ).astype(jnp.bfloat16)
 
     rows = exchange(buffer.reshape(tp_count * members, depth, piece_width), BLOCK)
-    values = rows.reshape(tp_count, members * depth, piece_width).astype(jnp.float32)
-    inv_rms = lax.rsqrt(jnp.sum(values * values, (0, 2)) / model_width + 1e-06)
-    gains = norm_gain.reshape(tp_count, 1, piece_width)
-    normed = (values * inv_rms[None, :, None] * gains).astype(jnp.bfloat16)
-    normed = jnp.concatenate([normed[t] for t in range(tp_count)], 1)
-    hidden = jnp.zeros((members * depth, tp_count * units), jnp.bfloat16)
-    for i, parts in enumerate(ring_in):
-        both = dot_parts(normed, parts)
-        piece = (jax.nn.silu(both[:, :units]) * both[:, units:]).astype(jnp.bfloat16)
-        owner = lax.rem(me + i, tp_count)
-        hidden = lax.dynamic_update_slice_in_dim(hidden, piece, owner * units, 1)
-    results = jnp.zeros((tp_count, members * depth, piece_width), jnp.bfloat16)
-    for i, parts in enumerate(ring_out):
-        piece = dot_parts(hidden, parts).astype(jnp.bfloat16)
-        owner = lax.rem(me + i, tp_count)
-        results = lax.dynamic_update_slice_in_dim(results, piece[None], owner, 0)
+    rows = rows.reshape(tp_count, members * depth, piece_width)
+    results = expert(rows, norm_gain, w_gate[0], w_up[0], ring_in, ring_out, me)
 
     returned = exchange(results.reshape(tp_count * members, depth, piece_width), BLOCK)
     returned = returned.reshape(-1, piece_width)

time: 360 us -> 344 us (0.956)
  matrix products: 27 us -> 10.3 us
  Pallas kernels: 0 us -> 12.2 us
    dot_general x19 -> x9, matrix products: 27 us -> 10.3 us  [dot(): return jnp.dot(a, b, preferred_element_type=jnp.float32)]
    pallas_call x0 -> x2, Pallas kernels: none -> 12.2 us  [the longest x1 6.13 us: expert(): pl.pallas_call(second_half, out_shape=jax.ShapeDtypeStruct((parts, count,...]
  transfers between devices with their start and end apart: 12 -> 12, of which waited for: 5 -> 7; matrix products, arithmetic and copies ran while one was open for 8% -> 2% of each run, Pallas kernels for 0% -> 2%
where the time goes in v2:
time: 344 us; the launch traced here: 343 us
  waiting for transfers between devices  194 us (56%)
  starting transfers between devices  114 us (33%)
  Pallas kernels  12.2 us (4%)
  matrix products  10.3 us (3%)
  local copies, waits for them, and re-layouts  7.8 us (2%)
  other arithmetic  4.58 us (1%)
    all_to_all x4, waiting for transfers between devices, exchange(): return lax.all_to_all(array, axis, 0, 0, tiled=True)  115 us
    all_to_all x4, starting transfers between devices, exchange(): return lax.all_to_all(array, axis, 0, 0, tiled=True)  87.8 us
    ppermute x8, waiting for transfers between devices, shifted(): lax.ppermute(array, axis, [(a, (a + by) % length) for a in range(length)])  79.2 us
    ppermute x8, starting transfers between devices, shifted(): lax.ppermute(array, axis, [(a, (a + by) % length) for a in range(length)])  26.2 us
    dot_general x9, matrix products, dot(): return jnp.dot(a, b, preferred_element_type=jnp.float32)  10.3 us
  transfers between devices with their start and end apart: 12, of which 7 were waited for; matrix products, arithmetic and copies ran while one was open for 2% of the time, Pallas kernels for 2%

profile of v2, /device:TPU:33, one launch (start us, length us, event | category | flops | bytes accessed | tf_op | source)
XLA Modules:
  0.0 343.4 jit_solution(10812090269567050701)
XLA Ops:
  4.1 1.5 fusion.10
  6.8 44.0 %all-to-all-start = ((bf16[8,56,512]{2,1,0:T(8,128)(2,1)}), bf16[8,56,512]{2,1,0:T(8,128)(2,1)S(1)}, u32[]{:S(2)}, u32[]{:S(2)}) async-start(bf16[8,56,512]{2,1,0:T(8,128)(2,1)} %bitcast), calls=%async_computation | async-start | bytes 917504 | tf_op jit(solution)/shard_map/all_to_all | solution.py:18
  51.2 31.9 %all-to-all-done = bf16[8,56,512]{2,1,0:T(8,128)(2,1)S(1)} async-done(((bf16[8,56,512]{2,1,0:T(8,128)(2,1)}), bf16[8,56,512]{2,1,0:T(8,128)(2,1)S(1)}, u32[]{:S(2)}, u32[]{:S(2)}) %all-to-all-start) | async-done | bytes 458784 | tf_op jit(solution)/shard_map/all_to_all | solution.py:18
  83.7 1.9 convolution_convert_fusion
  85.6 34.0 %all-to-all-start.1 = ((bf16[32,40,512]{2,1,0:T(8,128)(2,1)}), bf16[32,40,512]{2,1,0:T(8,128)(2,1)S(1)}, u32[]{:S(2)}, u32[]{:S(2)}) async-start(bf16[32,40,512]{2,1,0:T(8,128)(2,1)} %bitcast.42), calls=%async_computation.1 | async-start | bytes 2621440 | tf_op jit(solution)/shard_map/all_to_all | solution.py:18
  121.1 4.6 %collective-permute-start = (bf16[2048,512]{1,0:T(8,128)(2,1)S(1)}, bf16[2048,512]{1,0:T(8,128)(2,1)S(1)}, u32[]{:S(2)}, u32[]{:S(2)}) collective-permute-start(bf16[2048,512]{1,0:T(8,128)(2,1)S(1)} %pad_maximum_fusion), channel_id=1, source_target_pairs={{0,3},{1,0},{2,1},{3,2},{4,7},{5,4},{6,5},{7,6},{8,11},{9,8},{10,9... | collective-permute-start | bytes 6291464 | tf_op jit(solution)/shard_map/ppermute | solution.py:23
  125.7 2.0 collective-permute-start.1
  127.7 4.6 %collective-permute-start.4 = (bf16[1024,512]{1,0:T(8,128)(2,1)S(1)}, bf16[1024,512]{1,0:T(8,128)(2,1)S(1)}, u32[]{:S(2)}, u32[]{:S(2)}) collective-permute-start(bf16[1024,512]{1,0:T(8,128)(2,1)S(1)} %bitcast.46), channel_id=1, source_target_pairs={{0,3},{1,0},{2,1},{3,2},{4,7},{5,4},{6,5},{7,6},{8,11},{9,8},{10,9... | collective-permute-start | bytes 3145736 | tf_op jit(solution)/shard_map/ppermute | solution.py:23
  132.3 2.0 collective-permute-start.5
  134.3 46.2 %collective-permute-done.one = bf16[2048,512]{1,0:T(8,128)(2,1)S(1)} collective-permute-done((bf16[2048,512]{1,0:T(8,128)(2,1)S(1)}, bf16[2048,512]{1,0:T(8,128)(2,1)S(1)}, u32[]{:S(2)}, u32[]{:S(2)}) %collective-permute-start) | collective-permute-done | bytes 2097184 | tf_op jit(solution)/shard_map/ppermute | solution.py:23
  181.7 4.6 %collective-permute-start.2 = (bf16[1024,512]{1,0:T(8,128)(2,1)}, bf16[1024,512]{1,0:T(8,128)(2,1)}, u32[]{:S(2)}, u32[]{:S(2)}) collective-permute-start(bf16[1024,512]{1,0:T(8,128)(2,1)} %slice.95), channel_id=1, source_target_pairs={{0,3},{1,0},{2,1},{3,2},{4,7},{5,4},{6,5},{7,6},{8,11},{9,8},{10,9... | collective-permute-start | bytes 3145736 | tf_op jit(solution)/shard_map/ppermute | solution.py:23
  187.5 1.9 collective-permute-start.3
  189.5 13.5 %collective-permute-done.4.refs_5_ = bf16[1024,512]{1,0:T(8,128)(2,1)S(1)} collective-permute-done((bf16[1024,512]{1,0:T(8,128)(2,1)S(1)}, bf16[1024,512]{1,0:T(8,128)(2,1)S(1)}, u32[]{:S(2)}, u32[]{:S(2)}) %collective-permute-start.4) | collective-permute-done | bytes 1048608 | tf_op jit(solution)/shard_map/ppermute | solution.py:23
  203.8 4.5 %collective-permute-start.6 = (bf16[512,512]{1,0:T(8,128)(2,1)}, bf16[512,512]{1,0:T(8,128)(2,1)S(1)}, u32[]{:S(2)}, u32[]{:S(2)}) collective-permute-start(bf16[512,512]{1,0:T(8,128)(2,1)} %slice.97), channel_id=1, source_target_pairs={{0,3},{1,0},{2,1},{3,2},{4,7},{5,4},{6,5},{7,6},{8,11},{9,8},{10,9... | collective-permute-start | bytes 1572872 | tf_op jit(solution)/shard_map/ppermute | solution.py:23
  210.1 1.9 collective-permute-start.7
  213.8 6.1 %first_half.1 = (bf16[320,2048]{1,0:T(8,128)(2,1)}, bf16[3,320,256]{2,1,0:T(8,128)(2,1)}) custom-call(f32[4,512]{1,0:T(4,128)} %reshape.286.gains, bf16[4,320,512]{2,1,0:T(8,128)(2,1)} %bitcast.36, bf16[2048,256]{1,0:T(8,128)(2,1)} %bitcast.37, bf16[2048,256]{1,0:T(8,128)(2,1)} %bitcast.40, bf16[2048,512]{1,0:T(8,128)(2,1)} %copy-done.2, ...), custom_call_target="tpu_custom_call" | custom-call | tf_op jit(solution)/shard_map/first_half/pallas_call | solution.py:125
  219.9 16.9 %collective-permute-done.6.refs_7_ = bf16[512,512]{1,0:T(8,128)(2,1)S(1)} collective-permute-done((bf16[512,512]{1,0:T(8,128)(2,1)}, bf16[512,512]{1,0:T(8,128)(2,1)S(1)}, u32[]{:S(2)}, u32[]{:S(2)}) %collective-permute-start.6) | collective-permute-done | bytes 524320 | tf_op jit(solution)/shard_map/ppermute | solution.py:23
  236.8 2.6 collective-permute-done.7.refs_8_
  239.4 6.1 %second_half.1 = bf16[4,320,512]{2,1,0:T(8,128)(2,1)} custom-call(s32[1]{0:T(128)} %bitcast.5.me, bf16[320,2048]{1,0:T(8,128)(2,1)} %get-tuple-element.7.refs_0_, bf16[3,320,256]{2,1,0:T(8,128)(2,1)} %get-tuple-element.8.refs_1_, bf16[1024,512]{1,0:T(8,128)(2,1)} %collective-permute-done.2.refs_2_, bf16[1024,512]{1,0:T(8,128)(2,1)} %collective-permute-done.3.refs_3_, ...), custom_call_target="tpu_custom_call" | custom-call | tf_op jit(solution)/shard_map/second_half/pallas_call | solution.py:138
  245.5 6.2 %all-to-all-start.2 = ((bf16[32,40,512]{2,1,0:T(8,128)(2,1)}), bf16[32,40,512]{2,1,0:T(8,128)(2,1)S(1)}, u32[]{:S(2)}, u32[]{:S(2)}) async-start(bf16[32,40,512]{2,1,0:T(8,128)(2,1)} %bitcast.35), calls=%async_computation.2 | async-start | bytes 2621440 | tf_op jit(solution)/shard_map/all_to_all | solution.py:18
  252.1 32.8 %all-to-all-done.2 = bf16[32,40,512]{2,1,0:T(8,128)(2,1)S(1)} async-done(((bf16[32,40,512]{2,1,0:T(8,128)(2,1)}), bf16[32,40,512]{2,1,0:T(8,128)(2,1)S(1)}, u32[]{:S(2)}, u32[]{:S(2)}) %all-to-all-start.2) | async-done | bytes 1310752 | tf_op jit(solution)/shard_map/all_to_all | solution.py:18
  287.1 3.7 %all-to-all-start.3 = ((bf16[8,48,512]{2,1,0:T(8,128)(2,1)}), bf16[8,48,512]{2,1,0:T(8,128)(2,1)S(1)}, u32[]{:S(2)}, u32[]{:S(2)}) async-start(bf16[8,48,512]{2,1,0:T(8,128)(2,1)} %bitcast.15), calls=%async_computation.3 | async-start | bytes 786432 | tf_op jit(solution)/shard_map/all_to_all | solution.py:18
  290.8 50.2 %all-to-all-done.3 = bf16[8,48,512]{2,1,0:T(8,128)(2,1)S(1)} async-done(((bf16[8,48,512]{2,1,0:T(8,128)(2,1)}), bf16[8,48,512]{2,1,0:T(8,128)(2,1)S(1)}, u32[]{:S(2)}, u32[]{:S(2)}) %all-to-all-start.3) | async-done | bytes 393248 | tf_op jit(solution)/shard_map/all_to_all | solution.py:18
  341.5 1.9 fusion.11
  (78 shorter events, 17.4 us)
Async XLA Ops:
  0.0 5.6 %copy-start = (bf16[384,512]{1,0:T(8,128)(2,1)S(1)}, bf16[384,512]{1,0:T(8,128)(2,1)}, u32[]{:S(2)}) copy-start(bf16[384,512]{1,0:T(8,128)(2,1)} %param.9) | copy-start | bytes 1179652
  6.8 76.3 %all-to-all-start = ((bf16[8,56,512]{2,1,0:T(8,128)(2,1)}), bf16[8,56,512]{2,1,0:T(8,128)(2,1)S(1)}, u32[]{:S(2)}, u32[]{:S(2)}) async-start(bf16[8,56,512]{2,1,0:T(8,128)(2,1)} %bitcast), calls=%async_computation | async-start | bytes 917504 | tf_op jit(solution)/shard_map/all_to_all | solution.py:18
  85.6 34.0 %copy-start.4 = (bf16[1,2048,256]{2,1,0:T(8,128)(2,1)S(1)}, bf16[1,2048,256]{2,1,0:T(8,128)(2,1)}, u32[]{:S(2)}) copy-start(bf16[1,2048,256]{2,1,0:T(8,128)(2,1)} %param.15) | copy-start | bytes 3145732
  85.6 127.1 %all-to-all-start.1 = ((bf16[32,40,512]{2,1,0:T(8,128)(2,1)}), bf16[32,40,512]{2,1,0:T(8,128)(2,1)S(1)}, u32[]{:S(2)}, u32[]{:S(2)}) async-start(bf16[32,40,512]{2,1,0:T(8,128)(2,1)} %bitcast.42), calls=%async_computation.1 | async-start | bytes 2621440 | tf_op jit(solution)/shard_map/all_to_all | solution.py:18
  119.6 8.1 %copy-start.7 = (bf16[1,1024,512]{2,1,0:T(8,128)(2,1)S(1)}, bf16[1,1024,512]{2,1,0:T(8,128)(2,1)}, u32[]{:S(2)}) copy-start(bf16[1,1024,512]{2,1,0:T(8,128)(2,1)} %param.17) | copy-start | bytes 3145732
  121.1 59.4 %collective-permute-start = (bf16[2048,512]{1,0:T(8,128)(2,1)S(1)}, bf16[2048,512]{1,0:T(8,128)(2,1)S(1)}, u32[]{:S(2)}, u32[]{:S(2)}) collective-permute-start(bf16[2048,512]{1,0:T(8,128)(2,1)S(1)} %pad_maximum_fusion), channel_id=1, source_target_pairs={{0,3},{1,0},{2,1},{3,2},{4,7},{5,4},{6,5},{7,6},{8,11},{9,8},{10,9... | collective-permute-start | bytes 6291464 | tf_op jit(solution)/shard_map/ppermute | solution.py:23
  125.7 60.6 %collective-permute-start.1 = (bf16[2048,512]{1,0:T(8,128)(2,1)S(1)}, bf16[2048,512]{1,0:T(8,128)(2,1)S(1)}, u32[]{:S(2)}, u32[]{:S(2)}) collective-permute-start(bf16[2048,512]{1,0:T(8,128)(2,1)S(1)} %pad_maximum_fusion), channel_id=1, source_target_pairs={{0,1},{1,2},{2,3},{3,0},{4,5},{5,6},{6,7},{7,4},{8,9},{9,10},{10,1... | collective-permute-start | bytes 6291464 | tf_op jit(solution)/shard_map/ppermute | solution.py:23
  127.7 75.2 %collective-permute-start.4 = (bf16[1024,512]{1,0:T(8,128)(2,1)S(1)}, bf16[1024,512]{1,0:T(8,128)(2,1)S(1)}, u32[]{:S(2)}, u32[]{:S(2)}) collective-permute-start(bf16[1024,512]{1,0:T(8,128)(2,1)S(1)} %bitcast.46), channel_id=1, source_target_pairs={{0,3},{1,0},{2,1},{3,2},{4,7},{5,4},{6,5},{7,6},{8,11},{9,8},{10,9... | collective-permute-start | bytes 3145736 | tf_op jit(solution)/shard_map/ppermute | solution.py:23
  132.3 76.0 %collective-permute-start.5 = (bf16[1024,512]{1,0:T(8,128)(2,1)S(1)}, bf16[1024,512]{1,0:T(8,128)(2,1)S(1)}, u32[]{:S(2)}, u32[]{:S(2)}) collective-permute-start(bf16[1024,512]{1,0:T(8,128)(2,1)S(1)} %bitcast.47), channel_id=1, source_target_pairs={{0,1},{1,2},{2,3},{3,0},{4,5},{5,6},{6,7},{7,4},{8,9},{9,10},{10,1... | collective-permute-start | bytes 3145736 | tf_op jit(solution)/shard_map/ppermute | solution.py:23
  180.5 7.0 %copy-start.2 = (bf16[2048,512]{1,0:T(8,128)(2,1)}, bf16[2048,512]{1,0:T(8,128)(2,1)S(1)}, u32[]{:S(2)}) copy-start(bf16[2048,512]{1,0:T(8,128)(2,1)S(1)} %collective-permute-done.one) | copy-start | bytes 6291460
  181.7 30.4 %copy-start.10 = (f32[2048]{0:T(1024)S(1)}, f32[2048]{0:T(1024)}, u32[]{:S(2)}) copy-start(f32[2048]{0:T(1024)} %param.14) | copy-start | bytes 24580
  181.7 57.7 %collective-permute-start.2 = (bf16[1024,512]{1,0:T(8,128)(2,1)}, bf16[1024,512]{1,0:T(8,128)(2,1)}, u32[]{:S(2)}, u32[]{:S(2)}) collective-permute-start(bf16[1024,512]{1,0:T(8,128)(2,1)} %slice.95), channel_id=1, source_target_pairs={{0,3},{1,0},{2,1},{3,2},{4,7},{5,4},{6,5},{7,6},{8,11},{9,8},{10,9... | collective-permute-start | bytes 3145736 | tf_op jit(solution)/shard_map/ppermute | solution.py:23
  186.4 23.8 %copy-start.3 = (bf16[2048,512]{1,0:T(8,128)(2,1)}, bf16[2048,512]{1,0:T(8,128)(2,1)S(1)}, u32[]{:S(2)}) copy-start(bf16[2048,512]{1,0:T(8,128)(2,1)S(1)} %collective-permute-done.1.three) | copy-start | bytes 6291460
  187.5 51.8 %collective-permute-start.3 = (bf16[1024,512]{1,0:T(8,128)(2,1)}, bf16[1024,512]{1,0:T(8,128)(2,1)}, u32[]{:S(2)}, u32[]{:S(2)}) collective-permute-start(bf16[1024,512]{1,0:T(8,128)(2,1)} %slice.96), channel_id=1, source_target_pairs={{0,1},{1,2},{2,3},{3,0},{4,5},{5,6},{6,7},{7,4},{8,9},{9,10},{10,1... | collective-permute-start | bytes 3145736 | tf_op jit(solution)/shard_map/ppermute | solution.py:23
  203.0 16.9 %copy-start.5 = (bf16[1024,512]{1,0:T(8,128)(2,1)}, bf16[1024,512]{1,0:T(8,128)(2,1)S(1)}, u32[]{:S(2)}) copy-start(bf16[1024,512]{1,0:T(8,128)(2,1)S(1)} %collective-permute-done.4.refs_5_) | copy-start | bytes 3145732
  203.8 32.9 %collective-permute-start.6 = (bf16[512,512]{1,0:T(8,128)(2,1)}, bf16[512,512]{1,0:T(8,128)(2,1)S(1)}, u32[]{:S(2)}, u32[]{:S(2)}) collective-permute-start(bf16[512,512]{1,0:T(8,128)(2,1)} %slice.97), channel_id=1, source_target_pairs={{0,3},{1,0},{2,1},{3,2},{4,7},{5,4},{6,5},{7,6},{8,11},{9,8},{10,9... | collective-permute-start | bytes 1572872 | tf_op jit(solution)/shard_map/ppermute | solution.py:23
  208.4 1.0 copy-start.6
  210.1 29.2 %collective-permute-start.7 = (bf16[512,512]{1,0:T(8,128)(2,1)}, bf16[512,512]{1,0:T(8,128)(2,1)}, u32[]{:S(2)}, u32[]{:S(2)}) collective-permute-start(bf16[512,512]{1,0:T(8,128)(2,1)} %slice.98), channel_id=1, source_target_pairs={{0,1},{1,2},{2,3},{3,0},{4,5},{5,6},{6,7},{7,4},{8,9},{9,10},{10,1... | collective-permute-start | bytes 1572872 | tf_op jit(solution)/shard_map/ppermute | solution.py:23
  212.7 1.1 copy-start.1
  236.8 2.6 copy-start.8
  245.5 39.4 %all-to-all-start.2 = ((bf16[32,40,512]{2,1,0:T(8,128)(2,1)}), bf16[32,40,512]{2,1,0:T(8,128)(2,1)S(1)}, u32[]{:S(2)}, u32[]{:S(2)}) async-start(bf16[32,40,512]{2,1,0:T(8,128)(2,1)} %bitcast.35), calls=%async_computation.2 | async-start | bytes 2621440 | tf_op jit(solution)/shard_map/all_to_all | solution.py:18
  285.7 5.1 %copy-start.9 = (s32[384]{0:T(512)S(1)}, s32[384]{0:T(512)}, u32[]{:S(2)}) copy-start(s32[384]{0:T(512)} %param.10) | copy-start | bytes 4612
  287.1 53.9 %all-to-all-start.3 = ((bf16[8,48,512]{2,1,0:T(8,128)(2,1)}), bf16[8,48,512]{2,1,0:T(8,128)(2,1)S(1)}, u32[]{:S(2)}, u32[]{:S(2)}) async-start(bf16[8,48,512]{2,1,0:T(8,128)(2,1)} %bitcast.15), calls=%async_computation.3 | async-start | bytes 786432 | tf_op jit(solution)/shard_map/all_to_all | solution.py:18

commit v3 on v1

--- a/solution.py
+++ b/solution.py
@@ -1,6 +1,8 @@
 import jax
 import jax.numpy as jnp
 from jax import lax
+from jax.experimental import pallas as pl
+from jax.experimental.pallas import tpu as pltpu
 from jax.sharding import Mesh
 from jax.sharding import PartitionSpec as P
 
@@ -25,26 +27,113 @@
     return -(-length // tile) * tile
 
 
-def around(array, axis):
-    one = shifted(array, axis, 3)
-    three = shifted(array, axis, 1)
-    half = array.shape[0] // 2
+def ring_in(gate, up, axis):
+    gate_one = shifted(gate, axis, 3)
+    up_three = shifted(up, axis, 1)
+    up_one = shifted(up, axis, 3)
+    gate_three = shifted(gate, axis, 1)
+    gate_two = shifted(gate_one, axis, 3)
+    up_two = shifted(up_three, axis, 1)
+    return [gate, up, gate_one, up_one, gate_two, up_two, gate_three, up_three]
+
+
+def ring_out(down, axis):
+    one = shifted(down, axis, 3)
+    three = shifted(down, axis, 1)
+    half = down.shape[0] // 2
     top = shifted(one[:half], axis, 3)
     bottom = shifted(three[half:], axis, 1)
-    return [(array,), (one,), (top, bottom), (three,)]
+    return [down, one, three, top, bottom]
 
 
 def dot(a, b):
     return jnp.dot(a, b, preferred_element_type=jnp.float32)
 
 
-def dot_parts(a, parts):
-    total, at = None, 0
-    for part in parts:
-        product = dot(a[:, at : at + part.shape[0]], part)
-        total = product if total is None else total + product
-        at += part.shape[0]
-    return total
+def fetch(sources, slots, semaphores):
+    copies = [
+        pltpu.make_async_copy(source, slot, semaphores.at[i])
+        for i, (source, slot) in enumerate(zip(sources, slots, strict=True))
+    ]
+    for copy in copies:
+        copy.start()
+    return copies
+
+
+def to_hidden(me, gains, *refs):
+    hidden, scratch = refs[9], refs[10:]
+    rows, *slots = scratch[:9]
+    normed, semaphores = scratch[9:]
+    arrived, *copies = fetch(refs[:9], (rows, *slots), semaphores)
+    parts, _, width = rows.shape
+    units = slots[0].shape[1]
+    total = None
+    arrived.wait()
+    for t in range(parts):
+        values = rows[t].astype(jnp.float32)
+        squares = jnp.sum(values * values, -1, keepdims=True)
+        total = squares if total is None else total + squares
+    inv_rms = lax.rsqrt(total / (parts * width) + 1e-06)
+    for t in range(parts):
+        scaled = rows[t].astype(jnp.float32) * inv_rms * gains[t][None, :]
+        normed[:, t * width : (t + 1) * width] = scaled.astype(jnp.bfloat16)
+    for i in range(parts):
+        copies[2 * i].wait()
+        copies[2 * i + 1].wait()
+        gate = dot(normed[...], slots[2 * i][...])
+        up = dot(normed[...], slots[2 * i + 1][...])
+        piece = (gate / (1.0 + jnp.exp(-gate)) * up).astype(jnp.bfloat16)
+        at = lax.rem(me[0] + i, parts) * units
+        hidden[:, pl.ds(pl.multiple_of(at, units), units)] = piece
+
+
+def from_hidden(me, *refs):
+    results, slots, semaphores = refs[6], refs[7:13], refs[13]
+    copies = fetch(refs[:6], slots, semaphores)
+    hidden, own, one, three, top, bottom = slots
+    parts = results.shape[0]
+    copies[0].wait()
+    for copy, slot, offset in zip(copies[1:4], (own, one, three), (0, 1, 3), strict=True):
+        copy.wait()
+        piece = dot(hidden[...], slot[...])
+        results[lax.rem(me[0] + offset, parts)] = piece.astype(results.dtype)
+    copies[4].wait()
+    copies[5].wait()
+    half = top.shape[0]
+    piece = dot(hidden[:, :half], top[...]) + dot(hidden[:, half:], bottom[...])
+    results[lax.rem(me[0] + 2, parts)] = piece.astype(results.dtype)
+
+
+def expert(rows, norm_gain, weights_in, weights_out, me):
+    parts, count, width = rows.shape
+    units = weights_in[0].shape[1]
+    vmem = pl.BlockSpec(memory_space=pltpu.VMEM)
+    hbm = pl.BlockSpec(memory_space=pltpu.HBM)
+    smem = pl.BlockSpec(memory_space=pltpu.SMEM)
+
+    def slots(arrays):
+        return [pltpu.VMEM(a.shape, a.dtype) for a in arrays]
+
+    me = me.reshape(1)
+    given = [rows, *weights_in]
+    hidden = pl.pallas_call(
+        to_hidden,
+        out_shape=jax.ShapeDtypeStruct((count, parts * units), jnp.bfloat16),
+        in_specs=[smem, vmem] + [hbm] * 9,
+        out_specs=vmem,
+        scratch_shapes=slots(given)
+        + [pltpu.VMEM((count, parts * width), jnp.bfloat16), pltpu.SemaphoreType.DMA((9,))],
+        name="to_hidden",
+    )(me, norm_gain.reshape(parts, width), *given)
+    given = [hidden, *weights_out]
+    return pl.pallas_call(
+        from_hidden,
+        out_shape=jax.ShapeDtypeStruct((parts, count, width), jnp.bfloat16),
+        in_specs=[smem] + [hbm] * 6,
+        out_specs=vmem,
+        scratch_shapes=slots(given) + [pltpu.SemaphoreType.DMA((6,))],
+        name="from_hidden",
+    )(me, *given)
 
 
 def layer(
@@ -66,12 +155,10 @@
     per_group = tok_rows // groups
     mean_load = 2 * tok_rows // (groups * members)
     capacity = mean_load + min(mean_load // 2, per_group - mean_load)
-    model_width = norm_gain.shape[0]
-    units = w_gate.shape[2]
     width = per_group + TILE
 
-    ring_out = around(w_down[0], "tp")
-    ring_in = around(jnp.concatenate([w_gate[0], w_up[0]], 1), "tp")
+    weights_in = ring_in(w_gate[0], w_up[0], "tp")
+    weights_out = ring_out(w_down[0], "tp")
 
     in_group = group_choice[:, None] == jnp.arange(groups, dtype=jnp.int32)[None, :]
     before = jnp.tril(jnp.ones((tok_rows, tok_rows), jnp.bfloat16), -1)
@@ -124,22 +211,8 @@
     ).astype(jnp.bfloat16)
 
     rows = exchange(buffer.reshape(tp_count * members, depth, piece_width), BLOCK)
-    values = rows.reshape(tp_count, members * depth, piece_width).astype(jnp.float32)
-    inv_rms = lax.rsqrt(jnp.sum(values * values, (0, 2)) / model_width + 1e-06)
-    gains = norm_gain.reshape(tp_count, 1, piece_width)
-    normed = (values * inv_rms[None, :, None] * gains).astype(jnp.bfloat16)
-    normed = jnp.concatenate([normed[t] for t in range(tp_count)], 1)
-    hidden = jnp.zeros((members * depth, tp_count * units), jnp.bfloat16)
-    for i, parts in enumerate(ring_in):
-        both = dot_parts(normed, parts)
-        piece = (jax.nn.silu(both[:, :units]) * both[:, units:]).astype(jnp.bfloat16)
-        owner = lax.rem(me + i, tp_count)
-        hidden = lax.dynamic_update_slice_in_dim(hidden, piece, owner * units, 1)
-    results = jnp.zeros((tp_count, members * depth, piece_width), jnp.bfloat16)
-    for i, parts in enumerate(ring_out):
-        piece = dot_parts(hidden, parts).astype(jnp.bfloat16)
-        owner = lax.rem(me + i, tp_count)
-        results = lax.dynamic_update_slice_in_dim(results, piece[None], owner, 0)
+    rows = rows.reshape(tp_count, members * depth, piece_width)
+    results = expert(rows, norm_gain, weights_in, weights_out, me)
 
     returned = exchange(results.reshape(tp_count * members, depth, piece_width), BLOCK)
     returned = returned.reshape(-1, piece_width)

time: 360 us -> 342 us (0.950)
  matrix products: 27 us -> 10.3 us
  Pallas kernels: 0 us -> 11.6 us
  local copies, waits for them, and re-layouts: 11.2 us -> 5.22 us
  other arithmetic: 7.32 us -> 3.12 us
    dot_general x19 -> x9, matrix products: 27 us -> 10.3 us  [dot(): return jnp.dot(a, b, preferred_element_type=jnp.float32)]
    pallas_call x0 -> x2, Pallas kernels: none -> 11.6 us  [the longest x1 7.01 us: expert(): pl.pallas_call(to_hidden, out_shape=jax.ShapeDtypeStruct((count, parts *...]
    slice x4 -> x2, local copies, waits for them, and re-layouts: 7.31 us -> 1.66 us  [the longest x1 0.84 us: ring_out(): top = shifted(one[:half], axis, 3)]
    ppermute x8 -> x10, starting transfers between devices: 26.2 us -> 27.7 us  [shifted(): lax.ppermute(array, axis, [(a, (a + by) % length) for a in range(length)])]
    ppermute x8 -> x10, waiting for transfers between devices: 81.9 us -> 80.7 us  [shifted(): lax.ppermute(array, axis, [(a, (a + by) % length) for a in range(length)])]
  transfers between devices with their start and end apart: 12 -> 14, of which waited for: 5 -> 9; matrix products, arithmetic and copies ran while one was open for 8% -> 1% of each run, Pallas kernels for 0% -> 2%
where the time goes in v3:
time: 342 us; the launch traced here: 341 us
  waiting for transfers between devices  196 us (57%)
  starting transfers between devices  115 us (34%)
  Pallas kernels  11.6 us (3%)
  matrix products  10.3 us (3%)
  local copies, waits for them, and re-layouts  5.22 us (2%)
    all_to_all x4, waiting for transfers between devices, exchange(): return lax.all_to_all(array, axis, 0, 0, tiled=True)  115 us
    all_to_all x4, starting transfers between devices, exchange(): return lax.all_to_all(array, axis, 0, 0, tiled=True)  87.2 us
    ppermute x10, waiting for transfers between devices, shifted(): lax.ppermute(array, axis, [(a, (a + by) % length) for a in range(length)])  80.7 us
    ppermute x10, starting transfers between devices, shifted(): lax.ppermute(array, axis, [(a, (a + by) % length) for a in range(length)])  27.7 us
    dot_general x9, matrix products, dot(): return jnp.dot(a, b, preferred_element_type=jnp.float32)  10.3 us
    pallas_call x1, Pallas kernels, expert(): pl.pallas_call(to_hidden, out_shape=jax.ShapeDtypeStruct((count, parts *...  7.01 us
  transfers between devices with their start and end apart: 14, of which 9 were waited for; matrix products, arithmetic and copies ran while one was open for 1% of the time, Pallas kernels for 2%

profile of v3, /device:TPU:33, one launch (start us, length us, event | category | flops | bytes accessed | tf_op | source)
XLA Modules:
  0.0 341.1 jit_solution(9400039493995637365)
XLA Ops:
  6.8 44.0 %all-to-all-start = ((bf16[8,56,512]{2,1,0:T(8,128)(2,1)}), bf16[8,56,512]{2,1,0:T(8,128)(2,1)S(1)}, u32[]{:S(2)}, u32[]{:S(2)}) async-start(bf16[8,56,512]{2,1,0:T(8,128)(2,1)} %bitcast), calls=%async_computation | async-start | bytes 917504 | tf_op jit(solution)/shard_map/all_to_all | solution.py:18
  51.2 31.9 %all-to-all-done = bf16[8,56,512]{2,1,0:T(8,128)(2,1)S(1)} async-done(((bf16[8,56,512]{2,1,0:T(8,128)(2,1)}), bf16[8,56,512]{2,1,0:T(8,128)(2,1)S(1)}, u32[]{:S(2)}, u32[]{:S(2)}) %all-to-all-start) | async-done | bytes 458784 | tf_op jit(solution)/shard_map/all_to_all | solution.py:18
  83.7 2.0 convolution_convert_fusion
  85.6 33.9 %all-to-all-start.1 = ((bf16[32,40,512]{2,1,0:T(8,128)(2,1)}), bf16[32,40,512]{2,1,0:T(8,128)(2,1)S(1)}, u32[]{:S(2)}, u32[]{:S(2)}) async-start(bf16[32,40,512]{2,1,0:T(8,128)(2,1)} %bitcast.7), calls=%async_computation.1 | async-start | bytes 2621440 | tf_op jit(solution)/shard_map/all_to_all | solution.py:18
  119.5 4.6 %collective-permute-start = (bf16[2048,256]{1,0:T(8,128)(2,1)}, bf16[2048,256]{1,0:T(8,128)(2,1)}, u32[]{:S(2)}, u32[]{:S(2)}) collective-permute-start(bf16[2048,256]{1,0:T(8,128)(2,1)} %bitcast.9.refs_1_), channel_id=1, source_target_pairs={{0,3},{1,0},{2,1},{3,2},{4,7},{5,4},{6,5},{7,6},{8,11},{9,8},{10,9... | collective-permute-start | bytes 3145736 | tf_op jit(solution)/shard_map/ppermute | solution.py:23
  124.2 2.0 collective-permute-start.3
  126.1 2.0 collective-permute-start.7
  128.2 4.5 %collective-permute-start.6 = (bf16[1024,512]{1,0:T(8,128)(2,1)}, bf16[1024,512]{1,0:T(8,128)(2,1)S(1)}, u32[]{:S(2)}, u32[]{:S(2)}) collective-permute-start(bf16[1024,512]{1,0:T(8,128)(2,1)} %bitcast.41), channel_id=1, source_target_pairs={{0,3},{1,0},{2,1},{3,2},{4,7},{5,4},{6,5},{7,6},{8,11},{9,8},{10,9... | collective-permute-start | bytes 3145736 | tf_op jit(solution)/shard_map/ppermute | solution.py:23
  132.7 2.0 collective-permute-start.5
  134.7 23.4 %collective-permute-done.refs_3_ = bf16[2048,256]{1,0:T(8,128)(2,1)} collective-permute-done((bf16[2048,256]{1,0:T(8,128)(2,1)}, bf16[2048,256]{1,0:T(8,128)(2,1)}, u32[]{:S(2)}, u32[]{:S(2)}) %collective-permute-start) | collective-permute-done | bytes 1048608 | tf_op jit(solution)/shard_map/ppermute | solution.py:23
  158.0 4.5 %collective-permute-start.1 = (bf16[2048,256]{1,0:T(8,128)(2,1)}, bf16[2048,256]{1,0:T(8,128)(2,1)}, u32[]{:S(2)}, u32[]{:S(2)}) collective-permute-start(bf16[2048,256]{1,0:T(8,128)(2,1)} %bitcast.10.refs_2_), channel_id=1, source_target_pairs={{0,3},{1,0},{2,1},{3,2},{4,7},{5,4},{6,5},{7,6},{8,11},{9,8},{10,9... | collective-permute-start | bytes 3145736 | tf_op jit(solution)/shard_map/ppermute | solution.py:23
  162.5 2.2 collective-permute-start.2
  164.7 17.5 %collective-permute-done.7.refs_3_ = bf16[1024,512]{1,0:T(8,128)(2,1)S(1)} collective-permute-done((bf16[1024,512]{1,0:T(8,128)(2,1)}, bf16[1024,512]{1,0:T(8,128)(2,1)S(1)}, u32[]{:S(2)}, u32[]{:S(2)}) %collective-permute-start.7) | collective-permute-done | bytes 1048608 | tf_op jit(solution)/shard_map/ppermute | solution.py:23
  182.2 1.9 collective-permute-start.4
  187.8 17.0 %collective-permute-done.5.refs_7_ = bf16[2048,256]{1,0:T(8,128)(2,1)} collective-permute-done((bf16[2048,256]{1,0:T(8,128)(2,1)}, bf16[2048,256]{1,0:T(8,128)(2,1)}, u32[]{:S(2)}, u32[]{:S(2)}) %collective-permute-start.5) | collective-permute-done | bytes 1048608 | tf_op jit(solution)/shard_map/ppermute | solution.py:23
  204.8 2.0 collective-permute-start.8
  207.4 18.0 %collective-permute-done.2.refs_5_ = bf16[2048,256]{1,0:T(8,128)(2,1)} collective-permute-done((bf16[2048,256]{1,0:T(8,128)(2,1)}, bf16[2048,256]{1,0:T(8,128)(2,1)}, u32[]{:S(2)}, u32[]{:S(2)}) %collective-permute-start.2) | collective-permute-done | bytes 1048608 | tf_op jit(solution)/shard_map/ppermute | solution.py:23
  228.3 7.0 %to_hidden.1.refs_0_ = bf16[320,1024]{1,0:T(8,128)(2,1)} custom-call(s32[1]{0:T(128)} %bitcast.5.me, f32[4,512]{1,0:T(4,128)} %reshape.286.gains, bf16[4,320,512]{2,1,0:T(8,128)(2,1)} %bitcast.35, bf16[2048,256]{1,0:T(8,128)(2,1)} %bitcast.9.refs_1_, bf16[2048,256]{1,0:T(8,128)(2,1)} %bitcast.10.refs_2_, bf16[2048,256]{1,0:T(8,128)(2,1)} %collective-permute-done.refs_3_, ...), custom_call_target="tpu_custom_call" | custom-call | tf_op jit(solution)/shard_map/to_hidden/pallas_call | solution.py:119
  235.4 3.0 collective-permute-done.9.refs_5_
  239.2 4.6 %from_hidden.1 = bf16[4,320,512]{2,1,0:T(8,128)(2,1)} custom-call(s32[1]{0:T(128)} %bitcast.5.me, bf16[320,1024]{1,0:T(8,128)(2,1)} %to_hidden.1.refs_0_, bf16[1024,512]{1,0:T(8,128)(2,1)} %bitcast.42, bf16[1024,512]{1,0:T(8,128)(2,1)} %copy-done.3, bf16[1024,512]{1,0:T(8,128)(2,1)} %copy-done.2, bf16[512,512]{1,0:T(8,128)(2,1)} %collective-permute-done.8.refs_4_, ...), custom_call_target="tpu_custom_call" | custom-call | tf_op jit(solution)/shard_map/from_hidden/pallas_call | solution.py:129
  243.8 5.7 %all-to-all-start.2 = ((bf16[32,40,512]{2,1,0:T(8,128)(2,1)}), bf16[32,40,512]{2,1,0:T(8,128)(2,1)S(1)}, u32[]{:S(2)}, u32[]{:S(2)}) async-start(bf16[32,40,512]{2,1,0:T(8,128)(2,1)} %bitcast.36), calls=%async_computation.2 | async-start | bytes 2621440 | tf_op jit(solution)/shard_map/all_to_all | solution.py:18
  249.8 32.8 %all-to-all-done.2 = bf16[32,40,512]{2,1,0:T(8,128)(2,1)S(1)} async-done(((bf16[32,40,512]{2,1,0:T(8,128)(2,1)}), bf16[32,40,512]{2,1,0:T(8,128)(2,1)S(1)}, u32[]{:S(2)}, u32[]{:S(2)}) %all-to-all-start.2) | async-done | bytes 1310752 | tf_op jit(solution)/shard_map/all_to_all | solution.py:18
  284.8 3.7 %all-to-all-start.3 = ((bf16[8,48,512]{2,1,0:T(8,128)(2,1)}), bf16[8,48,512]{2,1,0:T(8,128)(2,1)S(1)}, u32[]{:S(2)}, u32[]{:S(2)}) async-start(bf16[8,48,512]{2,1,0:T(8,128)(2,1)} %bitcast.15), calls=%async_computation.3 | async-start | bytes 786432 | tf_op jit(solution)/shard_map/all_to_all | solution.py:18
  288.5 50.2 %all-to-all-done.3 = bf16[8,48,512]{2,1,0:T(8,128)(2,1)S(1)} async-done(((bf16[8,48,512]{2,1,0:T(8,128)(2,1)}), bf16[8,48,512]{2,1,0:T(8,128)(2,1)S(1)}, u32[]{:S(2)}, u32[]{:S(2)}) %all-to-all-start.3) | async-done | bytes 393248 | tf_op jit(solution)/shard_map/all_to_all | solution.py:18
  (71 shorter events, 20.5 us)
Async XLA Ops:
  0.0 5.6 %copy-start = (bf16[384,512]{1,0:T(8,128)(2,1)S(1)}, bf16[384,512]{1,0:T(8,128)(2,1)}, u32[]{:S(2)}) copy-start(bf16[384,512]{1,0:T(8,128)(2,1)} %param.9) | copy-start | bytes 1179652
  6.8 76.3 %all-to-all-start = ((bf16[8,56,512]{2,1,0:T(8,128)(2,1)}), bf16[8,56,512]{2,1,0:T(8,128)(2,1)S(1)}, u32[]{:S(2)}, u32[]{:S(2)}) async-start(bf16[8,56,512]{2,1,0:T(8,128)(2,1)} %bitcast), calls=%async_computation | async-start | bytes 917504 | tf_op jit(solution)/shard_map/all_to_all | solution.py:18
  85.6 141.6 %all-to-all-start.1 = ((bf16[32,40,512]{2,1,0:T(8,128)(2,1)}), bf16[32,40,512]{2,1,0:T(8,128)(2,1)S(1)}, u32[]{:S(2)}, u32[]{:S(2)}) async-start(bf16[32,40,512]{2,1,0:T(8,128)(2,1)} %bitcast.7), calls=%async_computation.1 | async-start | bytes 2621440 | tf_op jit(solution)/shard_map/all_to_all | solution.py:18
  119.5 87.3 %copy-start.6 = (f32[2048]{0:T(1024)S(1)}, f32[2048]{0:T(1024)}, u32[]{:S(2)}) copy-start(f32[2048]{0:T(1024)} %param.14) | copy-start | bytes 24580
  119.5 38.5 %collective-permute-start = (bf16[2048,256]{1,0:T(8,128)(2,1)}, bf16[2048,256]{1,0:T(8,128)(2,1)}, u32[]{:S(2)}, u32[]{:S(2)}) collective-permute-start(bf16[2048,256]{1,0:T(8,128)(2,1)} %bitcast.9.refs_1_), channel_id=1, source_target_pairs={{0,3},{1,0},{2,1},{3,2},{4,7},{5,4},{6,5},{7,6},{8,11},{9,8},{10,9... | collective-permute-start | bytes 3145736 | tf_op jit(solution)/shard_map/ppermute | solution.py:23
  124.2 38.4 %collective-permute-start.3 = (bf16[2048,256]{1,0:T(8,128)(2,1)}, bf16[2048,256]{1,0:T(8,128)(2,1)}, u32[]{:S(2)}, u32[]{:S(2)}) collective-permute-start(bf16[2048,256]{1,0:T(8,128)(2,1)} %bitcast.10.refs_2_), channel_id=1, source_target_pairs={{0,1},{1,2},{2,3},{3,0},{4,5},{5,6},{6,7},{7,4},{8,9},{9,10},{10,1... | collective-permute-start | bytes 3145736 | tf_op jit(solution)/shard_map/ppermute | solution.py:23
  126.1 56.1 %collective-permute-start.7 = (bf16[1024,512]{1,0:T(8,128)(2,1)}, bf16[1024,512]{1,0:T(8,128)(2,1)S(1)}, u32[]{:S(2)}, u32[]{:S(2)}) collective-permute-start(bf16[1024,512]{1,0:T(8,128)(2,1)} %bitcast.40), channel_id=1, source_target_pairs={{0,1},{1,2},{2,3},{3,0},{4,5},{5,6},{6,7},{7,4},{8,9},{9,10},{10,1... | collective-permute-start | bytes 3145736 | tf_op jit(solution)/shard_map/ppermute | solution.py:23
  128.2 56.8 %collective-permute-start.6 = (bf16[1024,512]{1,0:T(8,128)(2,1)}, bf16[1024,512]{1,0:T(8,128)(2,1)S(1)}, u32[]{:S(2)}, u32[]{:S(2)}) collective-permute-start(bf16[1024,512]{1,0:T(8,128)(2,1)} %bitcast.41), channel_id=1, source_target_pairs={{0,3},{1,0},{2,1},{3,2},{4,7},{5,4},{6,5},{7,6},{8,11},{9,8},{10,9... | collective-permute-start | bytes 3145736 | tf_op jit(solution)/shard_map/ppermute | solution.py:23
  132.7 72.1 %collective-permute-start.5 = (bf16[2048,256]{1,0:T(8,128)(2,1)}, bf16[2048,256]{1,0:T(8,128)(2,1)}, u32[]{:S(2)}, u32[]{:S(2)}) collective-permute-start(bf16[2048,256]{1,0:T(8,128)(2,1)} %bitcast.9.refs_1_), channel_id=1, source_target_pairs={{0,1},{1,2},{2,3},{3,0},{4,5},{5,6},{6,7},{7,4},{8,9},{9,10},{10,1... | collective-permute-start | bytes 3145736 | tf_op jit(solution)/shard_map/ppermute | solution.py:23
  158.0 49.4 %collective-permute-start.1 = (bf16[2048,256]{1,0:T(8,128)(2,1)}, bf16[2048,256]{1,0:T(8,128)(2,1)}, u32[]{:S(2)}, u32[]{:S(2)}) collective-permute-start(bf16[2048,256]{1,0:T(8,128)(2,1)} %bitcast.10.refs_2_), channel_id=1, source_target_pairs={{0,3},{1,0},{2,1},{3,2},{4,7},{5,4},{6,5},{7,6},{8,11},{9,8},{10,9... | collective-permute-start | bytes 3145736 | tf_op jit(solution)/shard_map/ppermute | solution.py:23
  162.5 62.9 %collective-permute-start.2 = (bf16[2048,256]{1,0:T(8,128)(2,1)}, bf16[2048,256]{1,0:T(8,128)(2,1)}, u32[]{:S(2)}, u32[]{:S(2)}) collective-permute-start(bf16[2048,256]{1,0:T(8,128)(2,1)} %collective-permute-done.refs_3_), channel_id=1, source_target_pairs={{0,3},{1,0},{2,1},{3,2},{4,7},{5,4},{6,5},{7,6},{8,11},{9,8},{10,9... | collective-permute-start | bytes 3145736 | tf_op jit(solution)/shard_map/ppermute | solution.py:23
  182.2 53.1 %copy-start.2 = (bf16[1024,512]{1,0:T(8,128)(2,1)}, bf16[1024,512]{1,0:T(8,128)(2,1)S(1)}, u32[]{:S(2)}) copy-start(bf16[1024,512]{1,0:T(8,128)(2,1)S(1)} %collective-permute-done.7.refs_3_) | copy-start | bytes 3145732
  182.2 45.0 %collective-permute-start.4 = (bf16[2048,256]{1,0:T(8,128)(2,1)}, bf16[2048,256]{1,0:T(8,128)(2,1)}, u32[]{:S(2)}, u32[]{:S(2)}) collective-permute-start(bf16[2048,256]{1,0:T(8,128)(2,1)} %collective-permute-done.3.refs_8_), channel_id=1, source_target_pairs={{0,1},{1,2},{2,3},{3,0},{4,5},{5,6},{6,7},{7,4},{8,9},{9,10},{10,1... | collective-permute-start | bytes 3145736 | tf_op jit(solution)/shard_map/ppermute | solution.py:23
  185.0 2.0 copy-start.3
  185.0 53.4 %collective-permute-start.9 = (bf16[512,512]{1,0:T(8,128)(2,1)}, bf16[512,512]{1,0:T(8,128)(2,1)S(1)}, u32[]{:S(2)}, u32[]{:S(2)}) collective-permute-start(bf16[512,512]{1,0:T(8,128)(2,1)} %slice.88), channel_id=1, source_target_pairs={{0,1},{1,2},{2,3},{3,0},{4,5},{5,6},{6,7},{7,4},{8,9},{9,10},{10,1... | collective-permute-start | bytes 1572872 | tf_op jit(solution)/shard_map/ppermute | solution.py:23
  204.8 33.6 %collective-permute-start.8 = (bf16[512,512]{1,0:T(8,128)(2,1)}, bf16[512,512]{1,0:T(8,128)(2,1)}, u32[]{:S(2)}, u32[]{:S(2)}) collective-permute-start(bf16[512,512]{1,0:T(8,128)(2,1)} %slice.87), channel_id=1, source_target_pairs={{0,3},{1,0},{2,1},{3,2},{4,7},{5,4},{6,5},{7,6},{8,11},{9,8},{10,9... | collective-permute-start | bytes 1572872 | tf_op jit(solution)/shard_map/ppermute | solution.py:23
  227.3 1.1 copy-start.1
  238.4 0.8 copy-start.4
  243.8 38.9 %all-to-all-start.2 = ((bf16[32,40,512]{2,1,0:T(8,128)(2,1)}), bf16[32,40,512]{2,1,0:T(8,128)(2,1)S(1)}, u32[]{:S(2)}, u32[]{:S(2)}) async-start(bf16[32,40,512]{2,1,0:T(8,128)(2,1)} %bitcast.36), calls=%async_computation.2 | async-start | bytes 2621440 | tf_op jit(solution)/shard_map/all_to_all | solution.py:18
  283.3 5.2 %copy-start.5 = (s32[384]{0:T(512)S(1)}, s32[384]{0:T(512)}, u32[]{:S(2)}) copy-start(s32[384]{0:T(512)} %param.10) | copy-start | bytes 4612
  284.8 53.9 %all-to-all-start.3 = ((bf16[8,48,512]{2,1,0:T(8,128)(2,1)}), bf16[8,48,512]{2,1,0:T(8,128)(2,1)S(1)}, u32[]{:S(2)}, u32[]{:S(2)}) async-start(bf16[8,48,512]{2,1,0:T(8,128)(2,1)} %bitcast.15), calls=%async_computation.3 | async-start | bytes 786432 | tf_op jit(solution)/shard_map/all_to_all | solution.py:18

commit v4 on v3

v4 whole, which is shorter than its diff:
```python
import functools

import jax
import jax.numpy as jnp
from jax import lax
from jax.experimental import pallas as pl
from jax.experimental.pallas import tpu as pltpu
from jax.sharding import Mesh
from jax.sharding import PartitionSpec as P


GROUP_SIZE = 8
TILE = 8
LANES = 128
EP = ("g", "m")
GRP_EP = ("grp", "g", "m")
BLOCK = ("tp", "m")


def exchange(array, axis):
    return lax.all_to_all(array, axis, 0, 0, tiled=True)


def shifted(array, axis, by):
    length = lax.axis_size(axis)
    return lax.ppermute(array, axis, [(a, (a + by) % length) for a in range(length)])


def up_to(length, tile):
    return -(-length // tile) * tile


def ring(gate, up, down, axis):
    down_one = shifted(down, axis, 3)
    down_three = shifted(down, axis, 1)
    gate_one = shifted(gate, axis, 3)
    up_three = shifted(up, axis, 1)
    up_one = shifted(up, axis, 3)
    gate_three = shifted(gate, axis, 1)
    half = down.shape[0] // 2
    top = shifted(down_one[:half], axis, 3)
    bottom = shifted(down_three[half:], axis, 1)
    gate_two = shifted(gate_one, axis, 3)
    up_two = shifted(up_three, axis, 1)
    near = [gate, up, gate_one, up_one, gate_three, up_three]
    far = [gate_two, up_two, down, down_one, down_three, top, bottom]
    return near, far


def dot(a, b):
    return jnp.dot(a, b, preferred_element_type=jnp.float32)


def fetch(sources, slots, semaphores):
    copies = [
        pltpu.make_async_copy(source, slot, semaphores.at[i])
        for i, (source, slot) in enumerate(zip(sources, slots, strict=True))
    ]
    for copy in copies:
        copy.start()
    return copies


def iota(shape, dim):
    return lax.broadcasted_iota(jnp.int32, shape, dim)


def ones(condition):
    return jnp.where(condition, 1.0, 0.0).astype(jnp.bfloat16)


def depart(group, choice, group_share, expert_share, tokens, blocks, ranks):
    groups, _, lanes = blocks.shape
    count, width = tokens.shape
    chunks, per_group = width // lanes, count // groups
    group = group[...]
    member = group == iota((groups, count), 0)
    earlier = dot(ones(member), ones(iota((count, count), 0) < iota((count, count), 1)))
    rank = jnp.sum(jnp.where(member, earlier, 0.0), 0, keepdims=True).astype(jnp.int32)
    ranks[...] = rank
    seating = ones(iota((count, count), 0) == group * per_group + rank)
    seated = dot(seating, tokens[...]).astype(jnp.bfloat16)
    mixing = group_share[...] * expert_share[...]
    mixing = mixing / jnp.sum(expert_share[...], 0, keepdims=True)
    coarse = mixing.astype(jnp.bfloat16).astype(jnp.float32)
    fine = mixing - coarse
    choice = choice[...].astype(jnp.float32)
    facts = jnp.zeros((TILE, count), jnp.float32)
    for i, pair in enumerate((choice, coarse, fine)):
        for k in range(2):
            facts = jnp.where(iota((TILE, count), 0) == 2 * i + k, pair[k : k + 1], facts)
    spoken = [jnp.where(group == g, facts, 0.0) for g in range(groups)]
    spoken = jnp.concatenate(spoken, 0).astype(jnp.bfloat16)
    columns = ones(iota((lanes, count), 0) == rank)
    told = lax.dot_general(
        spoken, columns, (((1,), (1,)), ((), ())), preferred_element_type=jnp.float32
    ).astype(jnp.bfloat16)
    for g in range(groups):
        for c in range(chunks):
            piece = seated[g * per_group : (g + 1) * per_group, c * lanes : (c + 1) * lanes]
            blocks[g, c * per_group : (c + 1) * per_group, :] = piece
        blocks[g, chunks * per_group :, :] = told[g * TILE : (g + 1) * TILE]


def arrive(capacity, landed, buffer, places, shares, seats):
    groups, lines, lanes = landed.shape
    parts, count, width = buffer.shape
    chunks = width // lanes
    per_group = (lines - TILE) // chunks
    members = GROUP_SIZE
    depth = count // members
    sources = groups // parts
    told = landed[:, chunks * per_group :, :].astype(jnp.float32)
    told = told.reshape(groups * TILE, lanes).astype(jnp.bfloat16)
    wanted = (6 * groups, groups * TILE)
    row = iota(wanted, 0)
    pick = iota(wanted, 1) == lax.rem(row, groups) * TILE + lax.div(row, groups)
    heard = dot(ones(pick), told)
    facts = [heard[i * groups : (i + 1) * groups] for i in range(6)]
    choices = [fact.astype(jnp.int32) for fact in facts[:2]]
    inside = iota((groups, lanes), 1) < per_group
    named = []
    for e in range(members):
        hit = (choices[0] == e) | (choices[1] == e)
        named.append(jnp.where(hit & inside, 1.0, 0.0))
    named = jnp.concatenate(named, 0).astype(jnp.bfloat16)
    earlier = dot(named, ones(iota((lanes, lanes), 0) < iota((lanes, lanes), 1)))
    source = iota((groups, lanes), 0)
    local = []
    for k in range(2):
        seat = jnp.zeros((groups, lanes), jnp.float32)
        for e in range(members):
            seat = jnp.where(choices[k] == e, earlier[e * groups : (e + 1) * groups], seat)
        place = choices[k] * depth + lax.rem(source, sources) * capacity + seat.astype(jnp.int32)
        local.append(jnp.where(inside, place, -1))
        places[k] = jnp.where(inside, lax.div(source, sources) * count + place, -1)
        shares[k] = facts[2 + k] + facts[4 + k]
    for g in range(groups):
        seats[g, per_group:, :] = jnp.zeros((lanes - per_group, width), jnp.bfloat16)
        for c in range(chunks):
            piece = landed[g, c * per_group : (c + 1) * per_group, :]
            seats[g, :per_group, c * lanes : (c + 1) * lanes] = piece
    rows = iota((count, lanes), 0)
    for p in range(parts):
        spread = []
        for g in range(p * sources, (p + 1) * sources):
            hit = (rows == local[0][g : g + 1]) | (rows == local[1][g : g + 1])
            spread.append(ones(hit))
        spread = jnp.concatenate(spread, 1)
        held = seats[p * sources : (p + 1) * sources].reshape(sources * lanes, width)
        buffer[p] = dot(spread, held).astype(jnp.bfloat16)


def gate_up(normed, gate, up):
    gate, up = dot(normed[...], gate[...]), dot(normed[...], up[...])
    return (gate / (1.0 + jnp.exp(-gate)) * up).astype(jnp.bfloat16)


def columns_of(me, offset, parts, units):
    return pl.ds(pl.multiple_of(lax.rem(me[0] + offset, parts) * units, units), units)


def first_half(me, gains, *refs):
    given, (normed, hidden), (rows, *slots), semaphores = refs[:7], refs[7:9], refs[9:16], refs[16]
    arrived, *copies = fetch(given, (rows, *slots), semaphores)
    parts, _, width = rows.shape
    units = slots[0].shape[1]
    total = None
    arrived.wait()
    for t in range(parts):
        values = rows[t].astype(jnp.float32)
        squares = jnp.sum(values * values, -1, keepdims=True)
        total = squares if total is None else total + squares
    inv_rms = lax.rsqrt(total / (parts * width) + 1e-06)
    for t in range(parts):
        scaled = rows[t].astype(jnp.float32) * inv_rms * gains[t][None, :]
        normed[:, t * width : (t + 1) * width] = scaled.astype(jnp.bfloat16)
    for i, offset in enumerate((0, 1, 3)):
        copies[2 * i].wait()
        copies[2 * i + 1].wait()
        piece = gate_up(normed, slots[2 * i], slots[2 * i + 1])
        hidden[:, columns_of(me, offset, parts, units)] = piece


def second_half(me, *refs):
    given, results, slots, semaphores = refs[:9], refs[9], refs[10:19], refs[19]
    copies = fetch(given, slots, semaphores)
    normed, hidden, gate, up, own, one, three, top, bottom = slots
    parts, units = results.shape[0], gate.shape[1]
    for copy in copies[:4]:
        copy.wait()
    hidden[:, columns_of(me, 2, parts, units)] = gate_up(normed, gate, up)
    for copy, slot, offset in zip(copies[4:7], (own, one, three), (0, 1, 3), strict=True):
        copy.wait()
        piece = dot(hidden[...], slot[...])
        results[lax.rem(me[0] + offset, parts)] = piece.astype(results.dtype)
    copies[7].wait()
    copies[8].wait()
    half = top.shape[0]
    piece = dot(hidden[:, :half], top[...]) + dot(hidden[:, half:], bottom[...])
    results[lax.rem(me[0] + 2, parts)] = piece.astype(results.dtype)


VMEM = pl.BlockSpec(memory_space=pltpu.VMEM)
HBM = pl.BlockSpec(memory_space=pltpu.HBM)
SMEM = pl.BlockSpec(memory_space=pltpu.SMEM)


def shaped(shape, dtype=jnp.bfloat16):
    return jax.ShapeDtypeStruct(shape, dtype)


def slots_for(arrays):
    slots = [pltpu.VMEM(a.shape, a.dtype) for a in arrays]
    return slots + [pltpu.SemaphoreType.DMA((len(arrays),))]


def expert(rows, norm_gain, near, far, me):
    parts, count, width = rows.shape
    units = near[0].shape[1]
    me = me.reshape(1)
    given = [rows, *near]
    normed, hidden = pl.pallas_call(
        first_half,
        out_shape=(shaped((count, parts * width)), shaped((count, parts * units))),
        in_specs=[SMEM, VMEM] + [HBM] * len(given),
        out_specs=(VMEM, VMEM),
        scratch_shapes=slots_for(given),
        name="first_half",
    )(me, norm_gain.reshape(parts, width), *given)
    given = [normed, hidden, *far]
    return pl.pallas_call(
        second_half,
        out_shape=shaped((parts, count, width)),
        in_specs=[SMEM] + [HBM] * len(given),
        out_specs=VMEM,
        scratch_shapes=slots_for(given),
        name="second_half",
    )(me, *given)


def layer(
    tokens,
    group_choice,
    expert_choice,
    group_weight,
    expert_weight,
    norm_gain,
    w_gate,
    w_up,
    w_down,
):
    tok_rows, piece_width = tokens.shape
    groups = lax.axis_size("g")
    members = lax.axis_size("m")
    tp_count = lax.axis_size("tp")
    me = lax.axis_index("tp")
    per_group = tok_rows // groups
    mean_load = 2 * tok_rows // (groups * members)
    capacity = mean_load + min(mean_load // 2, per_group - mean_load)
    chunks = piece_width // LANES
    depth = up_to(groups // tp_count * capacity, TILE)

    near, far = ring(w_gate[0], w_up[0], w_down[0], "tp")

    blocks, rank = pl.pallas_call(
        depart,
        out_shape=(
            shaped((groups, chunks * per_group + TILE, LANES)),
            shaped((1, tok_rows), jnp.int32),
        ),
        in_specs=[VMEM] * 5,
        out_specs=(VMEM, VMEM),
        name="depart",
    )(group_choice[None], expert_choice.T, group_weight[None], expert_weight.T, tokens)
    rank = rank[0]
    landed = exchange(blocks, "g")

    facts_shape = (2, groups, LANES)
    buffer, targets, shares = pl.pallas_call(
        functools.partial(arrive, capacity),
        out_shape=(
            shaped((tp_count, members * depth, piece_width)),
            shaped(facts_shape, jnp.int32),
            shaped(facts_shape, jnp.float32),
        ),
        in_specs=[VMEM],
        out_specs=(VMEM, VMEM, VMEM),
        scratch_shapes=[pltpu.VMEM((groups, LANES, piece_width), jnp.bfloat16)],
        name="arrive",
    )(landed)
    rows = exchange(buffer.reshape(tp_count * members, depth, piece_width), BLOCK)
    rows = rows.reshape(tp_count, members * depth, piece_width)
    results = expert(rows, norm_gain, near, far, me)

    returned = exchange(results.reshape(tp_count * members, depth, piece_width), BLOCK)
    returned = returned.reshape(-1, piece_width)
    places = jnp.arange(returned.shape[0], dtype=jnp.int32)
    combined = jnp.zeros((tok_rows, piece_width), jnp.float32)
    for k in range(2):
        back = targets[k][:, :per_group].reshape(-1)
        share = shares[k][:, :per_group].reshape(-1)
        picker = (back[:, None] == places[None, :]).astype(jnp.bfloat16)
        combined = combined + share[:, None] * dot(picker, returned)
    combined = combined.astype(jnp.bfloat16)
    home = exchange(combined.reshape(groups, per_group, piece_width), "g")
    home = home.reshape(tok_rows, piece_width)
    here = lax.axis_index("g")
    seats = jnp.arange(per_group, dtype=jnp.int32)[None, :]
    stayed = (group_choice == here)[:, None] & (rank[:, None] == seats)
    own = lax.dynamic_slice_in_dim(combined, here * per_group, per_group, 0)
    kept = dot(stayed.astype(jnp.bfloat16), own)
    slot = jnp.where(group_choice == here, -1, group_choice * per_group + rank)
    unseating = slot[:, None] == jnp.arange(tok_rows, dtype=jnp.int32)[None, :]
    return (dot(unseating.astype(jnp.bfloat16), home) + kept).astype(jnp.bfloat16)


def solution(mesh):
    groups = mesh.shape["ep"] // GROUP_SIZE
    split = Mesh(
        mesh.devices.reshape(mesh.shape["grp"], groups, GROUP_SIZE, mesh.shape["tp"]),
        ("grp", "g", "m", "tp"),
    )
    placed = (
        P(GRP_EP, "tp"),
        P(GRP_EP),
        P(GRP_EP, None),
        P(GRP_EP),
        P(GRP_EP, None),
        P(),
        P(EP, None, "tp"),
        P(EP, None, "tp"),
        P(EP, None, "tp"),
    )
    return jax.shard_map(
        layer, mesh=split, in_specs=placed, out_specs=P(GRP_EP, "tp"), check_vma=False
    )
```

time: 342 us -> 339 us (level)
  blocking collectives: 0 us -> 78.7 us
  starting transfers between devices: 115 us -> 72.2 us
  waiting for transfers between devices: 196 us -> 158 us
  matrix products: 10.3 us -> 4.47 us
  Pallas kernels: 11.6 us -> 17.4 us
    all_to_all x0 -> x1, blocking collectives: none -> 78.7 us  [exchange(): return lax.all_to_all(array, axis, 0, 0, tiled=True)]
    all_to_all x4 -> x3, starting transfers between devices: 87.2 us -> 37.6 us  [exchange(): return lax.all_to_all(array, axis, 0, 0, tiled=True)]
    all_to_all x4 -> x3, waiting for transfers between devices: 115 us -> 83.4 us  [exchange(): return lax.all_to_all(array, axis, 0, 0, tiled=True)]
    ppermute x10, starting transfers between devices: 27.7 us -> 34.6 us  [shifted(): lax.ppermute(array, axis, [(a, (a + by) % length) for a in range(length)])]
    ppermute x10, waiting for transfers between devices: 80.7 us -> 74.8 us  [shifted(): lax.ppermute(array, axis, [(a, (a + by) % length) for a in range(length)])]
    dot_general x9 -> x4, matrix products: 10.3 us -> 4.47 us  [dot(): return jnp.dot(a, b, preferred_element_type=jnp.float32)]
    pallas_call x2 -> x4, Pallas kernels: 11.6 us -> 17.4 us  [the longest x1 6.15 us: expert(): pl.pallas_call(second_half, out_shape=shaped((parts, count, width)), in_s...]
  transfers between devices with their start and end apart: 14 -> 13, of which waited for: 9 -> 7; matrix products, arithmetic and copies ran while one was open for 1% -> 1% of each run, Pallas kernels for 2% -> 2%
where the time goes in v4:
time: 339 us; the launch traced here: 338 us
  waiting for transfers between devices  158 us (47%)
  blocking collectives  78.7 us (23%)
  starting transfers between devices  72.2 us (21%)
  Pallas kernels  17.4 us (5%)
  local copies, waits for them, and re-layouts  6.2 us (2%)
  matrix products  4.47 us (1%)
    all_to_all x3, waiting for transfers between devices, exchange(): return lax.all_to_all(array, axis, 0, 0, tiled=True)  83.4 us
    all_to_all x1, blocking collectives, exchange(): return lax.all_to_all(array, axis, 0, 0, tiled=True)  78.7 us
    ppermute x10, waiting for transfers between devices, shifted(): lax.ppermute(array, axis, [(a, (a + by) % length) for a in range(length)])  74.8 us
    all_to_all x3, starting transfers between devices, exchange(): return lax.all_to_all(array, axis, 0, 0, tiled=True)  37.6 us
    ppermute x10, starting transfers between devices, shifted(): lax.ppermute(array, axis, [(a, (a + by) % length) for a in range(length)])  34.6 us
  transfers between devices with their start and end apart: 13, of which 7 were waited for; matrix products, arithmetic and copies ran while one was open for 1% of the time, Pallas kernels for 2%

profile of v4, /device:TPU:33, one launch (start us, length us, event | category | flops | bytes accessed | tf_op | source)
XLA Modules:
  0.0 337.5 jit_solution(14775107689072840486)
XLA Ops:
  2.5 2.3 depart.1
  4.8 78.7 %all_to_all.20.landed = bf16[8,200,128]{2,1,0:T(8,128)(2,1)} all-to-all(bf16[8,200,128]{2,1,0:T(8,128)(2,1)} %get-tuple-element.13), channel_id=1, replica_groups=mesh['grp'=2,'g'=8,'m'=8,'tp'=4] {'g'}, dimensions={0} | all-to-all | bytes 819200 | tf_op jit(solution)/shard_map/all_to_all | solution.py:21
  83.5 2.8 arrive.1
  86.3 27.5 %all-to-all-start.1 = ((bf16[32,40,512]{2,1,0:T(8,128)(2,1)}), bf16[32,40,512]{2,1,0:T(8,128)(2,1)S(1)}, u32[]{:S(2)}, u32[]{:S(2)}) async-start(bf16[32,40,512]{2,1,0:T(8,128)(2,1)} %bitcast.30), calls=%async_computation.1 | async-start | bytes 2621440 | tf_op jit(solution)/shard_map/all_to_all | solution.py:21
  113.9 4.6 %collective-permute-start = (bf16[2048,256]{1,0:T(8,128)(2,1)}, bf16[2048,256]{1,0:T(8,128)(2,1)}, u32[]{:S(2)}, u32[]{:S(2)}) collective-permute-start(bf16[2048,256]{1,0:T(8,128)(2,1)} %bitcast.7.refs_1_), channel_id=1, source_target_pairs={{0,3},{1,0},{2,1},{3,2},{4,7},{5,4},{6,5},{7,6},{8,11},{9,8},{10,9... | collective-permute-start | bytes 3145736 | tf_op jit(solution)/shard_map/ppermute | solution.py:26
  118.5 2.0 collective-permute-start.3
  120.5 4.6 %collective-permute-start.6 = (bf16[1024,512]{1,0:T(8,128)(2,1)}, bf16[1024,512]{1,0:T(8,128)(2,1)S(1)}, u32[]{:S(2)}, u32[]{:S(2)}) collective-permute-start(bf16[1024,512]{1,0:T(8,128)(2,1)} %bitcast.9.refs_4_), channel_id=1, source_target_pairs={{0,3},{1,0},{2,1},{3,2},{4,7},{5,4},{6,5},{7,6},{8,11},{9,8},{10,9... | collective-permute-start | bytes 3145736 | tf_op jit(solution)/shard_map/ppermute | solution.py:26
  125.1 2.0 collective-permute-start.7
  127.0 4.6 %collective-permute-start.1 = (bf16[2048,256]{1,0:T(8,128)(2,1)}, bf16[2048,256]{1,0:T(8,128)(2,1)}, u32[]{:S(2)}, u32[]{:S(2)}) collective-permute-start(bf16[2048,256]{1,0:T(8,128)(2,1)} %bitcast.8.refs_2_), channel_id=1, source_target_pairs={{0,3},{1,0},{2,1},{3,2},{4,7},{5,4},{6,5},{7,6},{8,11},{9,8},{10,9... | collective-permute-start | bytes 3145736 | tf_op jit(solution)/shard_map/ppermute | solution.py:26
  131.7 20.7 %collective-permute-done.refs_3_ = bf16[2048,256]{1,0:T(8,128)(2,1)} collective-permute-done((bf16[2048,256]{1,0:T(8,128)(2,1)}, bf16[2048,256]{1,0:T(8,128)(2,1)}, u32[]{:S(2)}, u32[]{:S(2)}) %collective-permute-start) | collective-permute-done | bytes 1048608 | tf_op jit(solution)/shard_map/ppermute | solution.py:26
  152.4 3.7 %collective-permute-start.2 = (bf16[2048,256]{1,0:T(8,128)(2,1)}, bf16[2048,256]{1,0:T(8,128)(2,1)}, u32[]{:S(2)}, u32[]{:S(2)}) collective-permute-start(bf16[2048,256]{1,0:T(8,128)(2,1)} %bitcast.7.refs_1_), channel_id=1, source_target_pairs={{0,1},{1,2},{2,3},{3,0},{4,5},{5,6},{6,7},{7,4},{8,9},{9,10},{10,1... | collective-permute-start | bytes 3145736 | tf_op jit(solution)/shard_map/ppermute | solution.py:26
  156.1 2.8 collective-permute-start.4
  158.9 15.8 %collective-permute-done.6.refs_5_ = bf16[1024,512]{1,0:T(8,128)(2,1)S(1)} collective-permute-done((bf16[1024,512]{1,0:T(8,128)(2,1)}, bf16[1024,512]{1,0:T(8,128)(2,1)S(1)}, u32[]{:S(2)}, u32[]{:S(2)}) %collective-permute-start.6) | collective-permute-done | bytes 1048608 | tf_op jit(solution)/shard_map/ppermute | solution.py:26
  174.7 3.8 %collective-permute-start.5 = (bf16[2048,256]{1,0:T(8,128)(2,1)}, bf16[2048,256]{1,0:T(8,128)(2,1)}, u32[]{:S(2)}, u32[]{:S(2)}) collective-permute-start(bf16[2048,256]{1,0:T(8,128)(2,1)} %collective-permute-done.3.refs_6_), channel_id=1, source_target_pairs={{0,1},{1,2},{2,3},{3,0},{4,5},{5,6},{6,7},{7,4},{8,9},{9,10},{10,1... | collective-permute-start | bytes 3145736 | tf_op jit(solution)/shard_map/ppermute | solution.py:26
  179.4 2.7 collective-permute-start.8
  183.0 14.3 %collective-permute-done.1.refs_4_ = bf16[2048,256]{1,0:T(8,128)(2,1)} collective-permute-done((bf16[2048,256]{1,0:T(8,128)(2,1)}, bf16[2048,256]{1,0:T(8,128)(2,1)}, u32[]{:S(2)}, u32[]{:S(2)}) %collective-permute-start.1) | collective-permute-done | bytes 1048608 | tf_op jit(solution)/shard_map/ppermute | solution.py:26
  197.3 3.7 %collective-permute-start.9 = (bf16[512,512]{1,0:T(8,128)(2,1)}, bf16[512,512]{1,0:T(8,128)(2,1)}, u32[]{:S(2)}, u32[]{:S(2)}) collective-permute-start(bf16[512,512]{1,0:T(8,128)(2,1)} %slice.41), channel_id=1, source_target_pairs={{0,1},{1,2},{2,3},{3,0},{4,5},{5,6},{6,7},{7,4},{8,9},{9,10},{10,1... | collective-permute-start | bytes 1572872 | tf_op jit(solution)/shard_map/ppermute | solution.py:26
  202.7 6.1 %first_half.1 = (bf16[320,2048]{1,0:T(8,128)(2,1)}, bf16[320,1024]{1,0:T(8,128)(2,1)}) custom-call(s32[1]{0:T(128)} %bitcast.4.me, f32[4,512]{1,0:T(4,128)} %reshape.32.gains, bf16[4,320,512]{2,1,0:T(8,128)(2,1)} %bitcast.28, bf16[2048,256]{1,0:T(8,128)(2,1)} %bitcast.7.refs_1_, bf16[2048,256]{1,0:T(8,128)(2,1)} %bitcast.8.refs_2_, ...), custom_call_target="tpu_custom_call" | custom-call | tf_op jit(solution)/shard_map/first_half/pallas_call | solution.py:223
  208.9 22.2 %collective-permute-done.8.refs_7_ = bf16[512,512]{1,0:T(8,128)(2,1)} collective-permute-done((bf16[512,512]{1,0:T(8,128)(2,1)}, bf16[512,512]{1,0:T(8,128)(2,1)}, u32[]{:S(2)}, u32[]{:S(2)}) %collective-permute-start.8) | collective-permute-done | bytes 524320 | tf_op jit(solution)/shard_map/ppermute | solution.py:26
  232.9 6.1 %second_half.1 = bf16[4,320,512]{2,1,0:T(8,128)(2,1)} custom-call(s32[1]{0:T(128)} %bitcast.4.me, bf16[320,2048]{1,0:T(8,128)(2,1)} %get-tuple-element.17.refs_0_, bf16[320,1024]{1,0:T(8,128)(2,1)} %get-tuple-element.18.refs_1_, bf16[2048,256]{1,0:T(8,128)(2,1)} %collective-permute-done.4.refs_2_, bf16[2048,256]{1,0:T(8,128)(2,1)} %collective-permute-done.5.refs_3_, ...), custom_call_target="tpu_custom_call" | custom-call | tf_op jit(solution)/shard_map/second_half/pallas_call | solution.py:232
  239.0 6.4 %all-to-all-start.2 = ((bf16[32,40,512]{2,1,0:T(8,128)(2,1)}), bf16[32,40,512]{2,1,0:T(8,128)(2,1)S(1)}, u32[]{:S(2)}, u32[]{:S(2)}) async-start(bf16[32,40,512]{2,1,0:T(8,128)(2,1)} %bitcast.27), calls=%async_computation.2 | async-start | bytes 2621440 | tf_op jit(solution)/shard_map/all_to_all | solution.py:21
  245.9 32.8 %all-to-all-done.2 = bf16[32,40,512]{2,1,0:T(8,128)(2,1)S(1)} async-done(((bf16[32,40,512]{2,1,0:T(8,128)(2,1)}), bf16[32,40,512]{2,1,0:T(8,128)(2,1)S(1)}, u32[]{:S(2)}, u32[]{:S(2)}) %all-to-all-start.2) | async-done | bytes 1310752 | tf_op jit(solution)/shard_map/all_to_all | solution.py:21
  280.9 3.7 %all-to-all-start.3 = ((bf16[8,48,512]{2,1,0:T(8,128)(2,1)}), bf16[8,48,512]{2,1,0:T(8,128)(2,1)S(1)}, u32[]{:S(2)}, u32[]{:S(2)}) async-start(bf16[8,48,512]{2,1,0:T(8,128)(2,1)} %bitcast.14), calls=%async_computation.3 | async-start | bytes 786432 | tf_op jit(solution)/shard_map/all_to_all | solution.py:21
  284.6 50.6 %all-to-all-done.3 = bf16[8,48,512]{2,1,0:T(8,128)(2,1)S(1)} async-done(((bf16[8,48,512]{2,1,0:T(8,128)(2,1)}), bf16[8,48,512]{2,1,0:T(8,128)(2,1)S(1)}, u32[]{:S(2)}, u32[]{:S(2)}) %all-to-all-start.3) | async-done | bytes 393248 | tf_op jit(solution)/shard_map/all_to_all | solution.py:21
  (41 shorter events, 12.6 us)
Async XLA Ops:
  86.3 115.3 %all-to-all-start.1 = ((bf16[32,40,512]{2,1,0:T(8,128)(2,1)}), bf16[32,40,512]{2,1,0:T(8,128)(2,1)S(1)}, u32[]{:S(2)}, u32[]{:S(2)}) async-start(bf16[32,40,512]{2,1,0:T(8,128)(2,1)} %bitcast.30), calls=%async_computation.1 | async-start | bytes 2621440 | tf_op jit(solution)/shard_map/all_to_all | solution.py:21
  113.8 87.2 %copy-start.4 = (f32[2048]{0:T(1024)S(1)}, f32[2048]{0:T(1024)}, u32[]{:S(2)}) copy-start(f32[2048]{0:T(1024)} %param.14) | copy-start | bytes 24580
  113.9 38.5 %collective-permute-start = (bf16[2048,256]{1,0:T(8,128)(2,1)}, bf16[2048,256]{1,0:T(8,128)(2,1)}, u32[]{:S(2)}, u32[]{:S(2)}) collective-permute-start(bf16[2048,256]{1,0:T(8,128)(2,1)} %bitcast.7.refs_1_), channel_id=1, source_target_pairs={{0,3},{1,0},{2,1},{3,2},{4,7},{5,4},{6,5},{7,6},{8,11},{9,8},{10,9... | collective-permute-start | bytes 3145736 | tf_op jit(solution)/shard_map/ppermute | solution.py:26
  118.5 37.6 %collective-permute-start.3 = (bf16[2048,256]{1,0:T(8,128)(2,1)}, bf16[2048,256]{1,0:T(8,128)(2,1)}, u32[]{:S(2)}, u32[]{:S(2)}) collective-permute-start(bf16[2048,256]{1,0:T(8,128)(2,1)} %bitcast.8.refs_2_), channel_id=1, source_target_pairs={{0,1},{1,2},{2,3},{3,0},{4,5},{5,6},{6,7},{7,4},{8,9},{9,10},{10,1... | collective-permute-start | bytes 3145736 | tf_op jit(solution)/shard_map/ppermute | solution.py:26
  120.5 54.3 %collective-permute-start.6 = (bf16[1024,512]{1,0:T(8,128)(2,1)}, bf16[1024,512]{1,0:T(8,128)(2,1)S(1)}, u32[]{:S(2)}, u32[]{:S(2)}) collective-permute-start(bf16[1024,512]{1,0:T(8,128)(2,1)} %bitcast.9.refs_4_), channel_id=1, source_target_pairs={{0,3},{1,0},{2,1},{3,2},{4,7},{5,4},{6,5},{7,6},{8,11},{9,8},{10,9... | collective-permute-start | bytes 3145736 | tf_op jit(solution)/shard_map/ppermute | solution.py:26
  125.1 54.4 %collective-permute-start.7 = (bf16[1024,512]{1,0:T(8,128)(2,1)}, bf16[1024,512]{1,0:T(8,128)(2,1)S(1)}, u32[]{:S(2)}, u32[]{:S(2)}) collective-permute-start(bf16[1024,512]{1,0:T(8,128)(2,1)} %bitcast.9.refs_4_), channel_id=1, source_target_pairs={{0,1},{1,2},{2,3},{3,0},{4,5},{5,6},{6,7},{7,4},{8,9},{9,10},{10,1... | collective-permute-start | bytes 3145736 | tf_op jit(solution)/shard_map/ppermute | solution.py:26
  127.0 70.3 %collective-permute-start.1 = (bf16[2048,256]{1,0:T(8,128)(2,1)}, bf16[2048,256]{1,0:T(8,128)(2,1)}, u32[]{:S(2)}, u32[]{:S(2)}) collective-permute-start(bf16[2048,256]{1,0:T(8,128)(2,1)} %bitcast.8.refs_2_), channel_id=1, source_target_pairs={{0,3},{1,0},{2,1},{3,2},{4,7},{5,4},{6,5},{7,6},{8,11},{9,8},{10,9... | collective-permute-start | bytes 3145736 | tf_op jit(solution)/shard_map/ppermute | solution.py:26
  152.4 49.3 %collective-permute-start.2 = (bf16[2048,256]{1,0:T(8,128)(2,1)}, bf16[2048,256]{1,0:T(8,128)(2,1)}, u32[]{:S(2)}, u32[]{:S(2)}) collective-permute-start(bf16[2048,256]{1,0:T(8,128)(2,1)} %bitcast.7.refs_1_), channel_id=1, source_target_pairs={{0,1},{1,2},{2,3},{3,0},{4,5},{5,6},{6,7},{7,4},{8,9},{9,10},{10,1... | collective-permute-start | bytes 3145736 | tf_op jit(solution)/shard_map/ppermute | solution.py:26
  156.1 76.8 %collective-permute-start.4 = (bf16[2048,256]{1,0:T(8,128)(2,1)}, bf16[2048,256]{1,0:T(8,128)(2,1)}, u32[]{:S(2)}, u32[]{:S(2)}) collective-permute-start(bf16[2048,256]{1,0:T(8,128)(2,1)} %collective-permute-done.refs_3_), channel_id=1, source_target_pairs={{0,3},{1,0},{2,1},{3,2},{4,7},{5,4},{6,5},{7,6},{8,11},{9,8},{10,9... | collective-permute-start | bytes 3145736 | tf_op jit(solution)/shard_map/ppermute | solution.py:26
  174.7 34.1 %copy-start.1 = (bf16[1024,512]{1,0:T(8,128)(2,1)}, bf16[1024,512]{1,0:T(8,128)(2,1)S(1)}, u32[]{:S(2)}) copy-start(bf16[1024,512]{1,0:T(8,128)(2,1)S(1)} %collective-permute-done.6.refs_5_) | copy-start | bytes 3145732
  174.7 58.1 %collective-permute-start.5 = (bf16[2048,256]{1,0:T(8,128)(2,1)}, bf16[2048,256]{1,0:T(8,128)(2,1)}, u32[]{:S(2)}, u32[]{:S(2)}) collective-permute-start(bf16[2048,256]{1,0:T(8,128)(2,1)} %collective-permute-done.3.refs_6_), channel_id=1, source_target_pairs={{0,1},{1,2},{2,3},{3,0},{4,5},{5,6},{6,7},{7,4},{8,9},{9,10},{10,1... | collective-permute-start | bytes 3145736 | tf_op jit(solution)/shard_map/ppermute | solution.py:26
  179.4 29.4 %copy-start.2 = (bf16[1024,512]{1,0:T(8,128)(2,1)}, bf16[1024,512]{1,0:T(8,128)(2,1)S(1)}, u32[]{:S(2)}) copy-start(bf16[1024,512]{1,0:T(8,128)(2,1)S(1)} %collective-permute-done.7.refs_6_) | copy-start | bytes 3145732
  179.4 51.6 %collective-permute-start.8 = (bf16[512,512]{1,0:T(8,128)(2,1)}, bf16[512,512]{1,0:T(8,128)(2,1)}, u32[]{:S(2)}, u32[]{:S(2)}) collective-permute-start(bf16[512,512]{1,0:T(8,128)(2,1)} %slice.40), channel_id=1, source_target_pairs={{0,3},{1,0},{2,1},{3,2},{4,7},{5,4},{6,5},{7,6},{8,11},{9,8},{10,9... | collective-permute-start | bytes 1572872 | tf_op jit(solution)/shard_map/ppermute | solution.py:26
  197.3 35.6 %collective-permute-start.9 = (bf16[512,512]{1,0:T(8,128)(2,1)}, bf16[512,512]{1,0:T(8,128)(2,1)}, u32[]{:S(2)}, u32[]{:S(2)}) collective-permute-start(bf16[512,512]{1,0:T(8,128)(2,1)} %slice.41), channel_id=1, source_target_pairs={{0,1},{1,2},{2,3},{3,0},{4,5},{5,6},{6,7},{7,4},{8,9},{9,10},{10,1... | collective-permute-start | bytes 1572872 | tf_op jit(solution)/shard_map/ppermute | solution.py:26
  201.7 1.1 copy-start
  239.0 6.5 %copy-start.6 = (s32[2,8,128]{2,1,0:T(8,128)S(1)}, s32[2,8,128]{2,1,0:T(8,128)}, u32[]{:S(2)}) copy-start(s32[2,8,128]{2,1,0:T(8,128)} %get-tuple-element.15) | copy-start | bytes 24580
  239.0 6.6 %copy-start.5 = (f32[2,8,128]{2,1,0:T(8,128)S(1)}, f32[2,8,128]{2,1,0:T(8,128)}, u32[]{:S(2)}) copy-start(f32[2,8,128]{2,1,0:T(8,128)} %get-tuple-element.14) | copy-start | bytes 24580
  239.0 39.6 %all-to-all-start.2 = ((bf16[32,40,512]{2,1,0:T(8,128)(2,1)}), bf16[32,40,512]{2,1,0:T(8,128)(2,1)S(1)}, u32[]{:S(2)}, u32[]{:S(2)}) async-start(bf16[32,40,512]{2,1,0:T(8,128)(2,1)} %bitcast.27), calls=%async_computation.2 | async-start | bytes 2621440 | tf_op jit(solution)/shard_map/all_to_all | solution.py:21
  279.4 5.2 %copy-start.7 = (s32[1,384]{1,0:T(1,128)S(1)}, s32[1,384]{1,0:T(1,128)}, u32[]{:S(2)}) copy-start(s32[1,384]{1,0:T(1,128)} %get-tuple-element.12) | copy-start | bytes 4612
  279.4 5.2 %copy-start.3 = (s32[384]{0:T(512)S(1)}, s32[384]{0:T(512)}, u32[]{:S(2)}) copy-start(s32[384]{0:T(512)} %param.10) | copy-start | bytes 4612
  280.9 54.3 %all-to-all-start.3 = ((bf16[8,48,512]{2,1,0:T(8,128)(2,1)}), bf16[8,48,512]{2,1,0:T(8,128)(2,1)S(1)}, u32[]{:S(2)}, u32[]{:S(2)}) async-start(bf16[8,48,512]{2,1,0:T(8,128)(2,1)} %bitcast.14), calls=%async_computation.3 | async-start | bytes 786432 | tf_op jit(solution)/shard_map/all_to_all | solution.py:21

commit v5 on v4

--- a/solution.py
+++ b/solution.py
@@ -30,21 +30,13 @@
     return -(-length // tile) * tile
 
 
-def ring(gate, up, down, axis):
-    down_one = shifted(down, axis, 3)
-    down_three = shifted(down, axis, 1)
-    gate_one = shifted(gate, axis, 3)
-    up_three = shifted(up, axis, 1)
-    up_one = shifted(up, axis, 3)
-    gate_three = shifted(gate, axis, 1)
-    half = down.shape[0] // 2
-    top = shifted(down_one[:half], axis, 3)
-    bottom = shifted(down_three[half:], axis, 1)
-    gate_two = shifted(gate_one, axis, 3)
-    up_two = shifted(up_three, axis, 1)
-    near = [gate, up, gate_one, up_one, gate_three, up_three]
-    far = [gate_two, up_two, down, down_one, down_three, top, bottom]
-    return near, far
+def around(array, axis):
+    one = shifted(array, axis, 3)
+    three = shifted(array, axis, 1)
+    half = array.shape[0] // 2
+    top = shifted(one[:half], axis, 3)
+    bottom = shifted(three[half:], axis, 1)
+    return [one, three], [top, bottom]
 
 
 def dot(a, b):
@@ -61,6 +53,11 @@
     return copies
 
 
+def gated(both, units):
+    gate, up = both[:, :units], both[:, units:]
+    return (gate / (1.0 + jnp.exp(-gate)) * up).astype(jnp.bfloat16)
+
+
 def iota(shape, dim):
     return lax.broadcasted_iota(jnp.int32, shape, dim)
 
@@ -73,14 +70,14 @@
     groups, _, lanes = blocks.shape
     count, width = tokens.shape
     chunks, per_group = width // lanes, count // groups
-    group = group[...]
+    group = group[...].reshape(1, count)
     member = group == iota((groups, count), 0)
     earlier = dot(ones(member), ones(iota((count, count), 0) < iota((count, count), 1)))
     rank = jnp.sum(jnp.where(member, earlier, 0.0), 0, keepdims=True).astype(jnp.int32)
     ranks[...] = rank
     seating = ones(iota((count, count), 0) == group * per_group + rank)
     seated = dot(seating, tokens[...]).astype(jnp.bfloat16)
-    mixing = group_share[...] * expert_share[...]
+    mixing = group_share[...].reshape(1, count) * expert_share[...]
     mixing = mixing / jnp.sum(expert_share[...], 0, keepdims=True)
     coarse = mixing.astype(jnp.bfloat16).astype(jnp.float32)
     fine = mixing - coarse
@@ -151,20 +148,27 @@
         buffer[p] = dot(spread, held).astype(jnp.bfloat16)
 
 
-def gate_up(normed, gate, up):
-    gate, up = dot(normed[...], gate[...]), dot(normed[...], up[...])
+def gated(gate, up):
     return (gate / (1.0 + jnp.exp(-gate)) * up).astype(jnp.bfloat16)
 
 
-def columns_of(me, offset, parts, units):
-    return pl.ds(pl.multiple_of(lax.rem(me[0] + offset, parts) * units, units), units)
+def place(hidden, me, offset, parts, piece):
+    units = piece.shape[1]
+    at = pl.multiple_of(lax.rem(me[0] + offset, parts) * units, units)
+    hidden[:, pl.ds(at, units)] = piece
+
+
+def by_halves(whole, top, bottom):
+    half = top.shape[0]
+    return dot(whole[:, :half], top[...]) + dot(whole[:, half:], bottom[...])
 
 
 def first_half(me, gains, *refs):
-    given, (normed, hidden), (rows, *slots), semaphores = refs[:7], refs[7:9], refs[9:16], refs[16]
+    given, (normed, hidden), (rows, *slots), semaphores = refs[:5], refs[5:7], refs[7:12], refs[12]
+    gate, up, one, three = slots
     arrived, *copies = fetch(given, (rows, *slots), semaphores)
     parts, _, width = rows.shape
-    units = slots[0].shape[1]
+    units = gate.shape[1]
     total = None
     arrived.wait()
     for t in range(parts):
@@ -175,30 +179,34 @@
     for t in range(parts):
         scaled = rows[t].astype(jnp.float32) * inv_rms * gains[t][None, :]
         normed[:, t * width : (t + 1) * width] = scaled.astype(jnp.bfloat16)
-    for i, offset in enumerate((0, 1, 3)):
-        copies[2 * i].wait()
-        copies[2 * i + 1].wait()
-        piece = gate_up(normed, slots[2 * i], slots[2 * i + 1])
-        hidden[:, columns_of(me, offset, parts, units)] = piece
+    copies[0].wait()
+    copies[1].wait()
+    piece = gated(dot(normed[...], gate[...]), dot(normed[...], up[...]))
+    place(hidden, me, 0, parts, piece)
+    for copy, slot, offset in zip(copies[2:], (one, three), (1, 3), strict=True):
+        copy.wait()
+        both = dot(normed[...], slot[...])
+        place(hidden, me, offset, parts, gated(both[:, :units], both[:, units:]))
 
 
 def second_half(me, *refs):
     given, results, slots, semaphores = refs[:9], refs[9], refs[10:19], refs[19]
     copies = fetch(given, slots, semaphores)
-    normed, hidden, gate, up, own, one, three, top, bottom = slots
-    parts, units = results.shape[0], gate.shape[1]
+    normed, hidden, top, bottom, own, one, three, down_top, down_bottom = slots
+    parts = results.shape[0]
+    units = hidden.shape[1] // parts
     for copy in copies[:4]:
         copy.wait()
-    hidden[:, columns_of(me, 2, parts, units)] = gate_up(normed, gate, up)
+    both = by_halves(normed, top, bottom)
+    place(hidden, me, 2, parts, gated(both[:, :units], both[:, units:]))
     for copy, slot, offset in zip(copies[4:7], (own, one, three), (0, 1, 3), strict=True):
         copy.wait()
-        piece = dot(hidden[...], slot[...])
-        results[lax.rem(me[0] + offset, parts)] = piece.astype(results.dtype)
+        owner = lax.rem(me[0] + offset, parts)
+        results[owner] = dot(hidden[...], slot[...]).astype(results.dtype)
     copies[7].wait()
     copies[8].wait()
-    half = top.shape[0]
-    piece = dot(hidden[:, :half], top[...]) + dot(hidden[:, half:], bottom[...])
-    results[lax.rem(me[0] + 2, parts)] = piece.astype(results.dtype)
+    owner = lax.rem(me[0] + 2, parts)
+    results[owner] = by_halves(hidden, down_top, down_bottom).astype(results.dtype)
 
 
 VMEM = pl.BlockSpec(memory_space=pltpu.VMEM)
@@ -211,30 +219,31 @@
 
 
 def slots_for(arrays):
-    slots = [pltpu.VMEM(a.shape, a.dtype) for a in arrays]
-    return slots + [pltpu.SemaphoreType.DMA((len(arrays),))]
-
-
-def expert(rows, norm_gain, near, far, me):
+    return [pltpu.VMEM(a.shape, a.dtype) for a in arrays]
+
+
+def expert(rows, norm_gain, gate, up, down, gate_up_ring, down_ring, me):
     parts, count, width = rows.shape
-    units = near[0].shape[1]
+    units = gate.shape[1]
     me = me.reshape(1)
-    given = [rows, *near]
+    near, far = gate_up_ring
+    given = [rows, gate, up, *near]
     normed, hidden = pl.pallas_call(
         first_half,
         out_shape=(shaped((count, parts * width)), shaped((count, parts * units))),
         in_specs=[SMEM, VMEM] + [HBM] * len(given),
         out_specs=(VMEM, VMEM),
-        scratch_shapes=slots_for(given),
+        scratch_shapes=slots_for(given) + [pltpu.SemaphoreType.DMA((len(given),))],
         name="first_half",
     )(me, norm_gain.reshape(parts, width), *given)
-    given = [normed, hidden, *far]
+    near, far_down = down_ring
+    given = [normed, hidden, *far, down, *near, *far_down]
     return pl.pallas_call(
         second_half,
         out_shape=shaped((parts, count, width)),
         in_specs=[SMEM] + [HBM] * len(given),
         out_specs=VMEM,
-        scratch_shapes=slots_for(given),
+        scratch_shapes=slots_for(given) + [pltpu.SemaphoreType.DMA((len(given),))],
         name="second_half",
     )(me, *given)
 
@@ -261,7 +270,8 @@
     chunks = piece_width // LANES
     depth = up_to(groups // tp_count * capacity, TILE)
 
-    near, far = ring(w_gate[0], w_up[0], w_down[0], "tp")
+    gate_up_ring = around(jnp.concatenate([w_gate[0], w_up[0]], 1), "tp")
+    down_ring = around(w_down[0], "tp")
 
     blocks, rank = pl.pallas_call(
         depart,
@@ -272,7 +282,7 @@
         in_specs=[VMEM] * 5,
         out_specs=(VMEM, VMEM),
         name="depart",
-    )(group_choice[None], expert_choice.T, group_weight[None], expert_weight.T, tokens)
+    )(group_choice, expert_choice.T, group_weight, expert_weight.T, tokens)
     rank = rank[0]
     landed = exchange(blocks, "g")
 
@@ -291,7 +301,9 @@
     )(landed)
     rows = exchange(buffer.reshape(tp_count * members, depth, piece_width), BLOCK)
     rows = rows.reshape(tp_count, members * depth, piece_width)
-    results = expert(rows, norm_gain, near, far, me)
+    results = expert(
+        rows, norm_gain, w_gate[0], w_up[0], w_down[0], gate_up_ring, down_ring, me
+    )
 
     returned = exchange(results.reshape(tp_count * members, depth, piece_width), BLOCK)
     returned = returned.reshape(-1, piece_width)

time: 339 us -> 338 us (level)
  starting transfers between devices: 72.2 us -> 64 us
  waiting for transfers between devices: 158 us -> 164 us
    ppermute x10 -> x8, starting transfers between devices: 34.6 us -> 26.3 us  [shifted(): lax.ppermute(array, axis, [(a, (a + by) % length) for a in range(length)])]
    ppermute x10 -> x8, waiting for transfers between devices: 74.8 us -> 80.5 us  [shifted(): lax.ppermute(array, axis, [(a, (a + by) % length) for a in range(length)])]
  transfers between devices with their start and end apart: 13 -> 11, of which waited for: 7 -> 6; matrix products, arithmetic and copies ran while one was open for 1% -> 2% of each run, Pallas kernels for 2% -> 2%
where the time goes in v5:
time: 338 us; the launch traced here: 337 us
  waiting for transfers between devices  164 us (49%)
  blocking collectives  78.8 us (23%)
  starting transfers between devices  64 us (19%)
  Pallas kernels  17.5 us (5%)
  local copies, waits for them, and re-layouts  7.43 us (2%)
  matrix products  4.48 us (1%)
    all_to_all x3, waiting for transfers between devices, exchange(): return lax.all_to_all(array, axis, 0, 0, tiled=True)  83.4 us
    ppermute x8, waiting for transfers between devices, shifted(): lax.ppermute(array, axis, [(a, (a + by) % length) for a in range(length)])  80.5 us
    all_to_all x1, blocking collectives, exchange(): return lax.all_to_all(array, axis, 0, 0, tiled=True)  78.8 us
    all_to_all x3, starting transfers between devices, exchange(): return lax.all_to_all(array, axis, 0, 0, tiled=True)  37.6 us
    ppermute x8, starting transfers between devices, shifted(): lax.ppermute(array, axis, [(a, (a + by) % length) for a in range(length)])  26.3 us
  transfers between devices with their start and end apart: 11, of which 6 were waited for; matrix products, arithmetic and copies ran while one was open for 2% of the time, Pallas kernels for 2%

profile of v5, /device:TPU:33, one launch (start us, length us, event | category | flops | bytes accessed | tf_op | source)
XLA Modules:
  0.0 336.6 jit_solution(14581366130302169692)
XLA Ops:
  0.0 2.4 depart.1
  2.4 78.8 %all_to_all.20.landed = bf16[8,200,128]{2,1,0:T(8,128)(2,1)} all-to-all(bf16[8,200,128]{2,1,0:T(8,128)(2,1)} %get-tuple-element.13), channel_id=1, replica_groups=mesh['grp'=2,'g'=8,'m'=8,'tp'=4] {'g'}, dimensions={0} | all-to-all | bytes 819200 | tf_op jit(solution)/shard_map/all_to_all | solution.py:21
  81.2 2.9 arrive.1
  84.1 27.5 %all-to-all-start.1 = ((bf16[32,40,512]{2,1,0:T(8,128)(2,1)}), bf16[32,40,512]{2,1,0:T(8,128)(2,1)S(1)}, u32[]{:S(2)}, u32[]{:S(2)}) async-start(bf16[32,40,512]{2,1,0:T(8,128)(2,1)} %bitcast.34), calls=%async_computation.1 | async-start | bytes 2621440 | tf_op jit(solution)/shard_map/all_to_all | solution.py:21
  111.8 4.8 %collective-permute-start = (bf16[2048,512]{1,0:T(8,128)(2,1)S(1)}, bf16[2048,512]{1,0:T(8,128)(2,1)S(1)}, u32[]{:S(2)}, u32[]{:S(2)}) collective-permute-start(bf16[2048,512]{1,0:T(8,128)(2,1)S(1)} %pad_maximum_fusion), channel_id=1, source_target_pairs={{0,3},{1,0},{2,1},{3,2},{4,7},{5,4},{6,5},{7,6},{8,11},{9,8},{10,9... | collective-permute-start | bytes 6291464 | tf_op jit(solution)/shard_map/ppermute | solution.py:26
  116.5 2.0 collective-permute-start.1
  118.5 4.6 %collective-permute-start.4 = (bf16[1024,512]{1,0:T(8,128)(2,1)S(1)}, bf16[1024,512]{1,0:T(8,128)(2,1)S(1)}, u32[]{:S(2)}, u32[]{:S(2)}) collective-permute-start(bf16[1024,512]{1,0:T(8,128)(2,1)S(1)} %bitcast.38), channel_id=1, source_target_pairs={{0,3},{1,0},{2,1},{3,2},{4,7},{5,4},{6,5},{7,6},{8,11},{9,8},{10,9... | collective-permute-start | bytes 3145736 | tf_op jit(solution)/shard_map/ppermute | solution.py:26
  123.1 2.0 collective-permute-start.5
  125.1 47.4 %collective-permute-done.refs_3_ = bf16[2048,512]{1,0:T(8,128)(2,1)S(1)} collective-permute-done((bf16[2048,512]{1,0:T(8,128)(2,1)S(1)}, bf16[2048,512]{1,0:T(8,128)(2,1)S(1)}, u32[]{:S(2)}, u32[]{:S(2)}) %collective-permute-start) | collective-permute-done | bytes 2097184 | tf_op jit(solution)/shard_map/ppermute | solution.py:26
  173.6 4.6 %collective-permute-start.2 = (bf16[1024,512]{1,0:T(8,128)(2,1)}, bf16[1024,512]{1,0:T(8,128)(2,1)S(1)}, u32[]{:S(2)}, u32[]{:S(2)}) collective-permute-start(bf16[1024,512]{1,0:T(8,128)(2,1)} %slice.48), channel_id=1, source_target_pairs={{0,3},{1,0},{2,1},{3,2},{4,7},{5,4},{6,5},{7,6},{8,11},{9,8},{10,9... | collective-permute-start | bytes 3145736 | tf_op jit(solution)/shard_map/ppermute | solution.py:26
  179.3 1.9 collective-permute-start.3
  181.3 13.6 %collective-permute-done.4.refs_5_ = bf16[1024,512]{1,0:T(8,128)(2,1)S(1)} collective-permute-done((bf16[1024,512]{1,0:T(8,128)(2,1)S(1)}, bf16[1024,512]{1,0:T(8,128)(2,1)S(1)}, u32[]{:S(2)}, u32[]{:S(2)}) %collective-permute-start.4) | collective-permute-done | bytes 1048608 | tf_op jit(solution)/shard_map/ppermute | solution.py:26
  195.8 4.5 %collective-permute-start.6 = (bf16[512,512]{1,0:T(8,128)(2,1)}, bf16[512,512]{1,0:T(8,128)(2,1)}, u32[]{:S(2)}, u32[]{:S(2)}) collective-permute-start(bf16[512,512]{1,0:T(8,128)(2,1)} %slice.50), channel_id=1, source_target_pairs={{0,3},{1,0},{2,1},{3,2},{4,7},{5,4},{6,5},{7,6},{8,11},{9,8},{10,9... | collective-permute-start | bytes 1572872 | tf_op jit(solution)/shard_map/ppermute | solution.py:26
  201.3 1.9 collective-permute-start.7
  205.0 6.1 %first_half.1 = (bf16[320,2048]{1,0:T(8,128)(2,1)}, bf16[320,1024]{1,0:T(8,128)(2,1)}) custom-call(s32[1]{0:T(128)} %bitcast.4.me, f32[4,512]{1,0:T(4,128)} %reshape.32.gains, bf16[4,320,512]{2,1,0:T(8,128)(2,1)} %bitcast.28, bf16[2048,256]{1,0:T(8,128)(2,1)} %bitcast.29, bf16[2048,256]{1,0:T(8,128)(2,1)} %bitcast.31, bf16[2048,512]{1,0:T(8,128)(2,1)} %copy-done.1, ...), custom_call_target="tpu_custom_call" | custom-call | tf_op jit(solution)/shard_map/first_half/pallas_call | solution.py:231
  211.1 17.6 %collective-permute-done.6.refs_7_ = bf16[512,512]{1,0:T(8,128)(2,1)} collective-permute-done((bf16[512,512]{1,0:T(8,128)(2,1)}, bf16[512,512]{1,0:T(8,128)(2,1)}, u32[]{:S(2)}, u32[]{:S(2)}) %collective-permute-start.6) | collective-permute-done | bytes 524320 | tf_op jit(solution)/shard_map/ppermute | solution.py:26
  228.7 1.8 collective-permute-done.7.refs_8_
  231.9 6.2 %second_half.1 = bf16[4,320,512]{2,1,0:T(8,128)(2,1)} custom-call(s32[1]{0:T(128)} %bitcast.4.me, bf16[320,2048]{1,0:T(8,128)(2,1)} %get-tuple-element.17.refs_0_, bf16[320,1024]{1,0:T(8,128)(2,1)} %get-tuple-element.18.refs_1_, bf16[1024,512]{1,0:T(8,128)(2,1)} %copy-done.8, bf16[1024,512]{1,0:T(8,128)(2,1)} %copy-done.9, bf16[1024,512]{1,0:T(8,128)(2,1)} %bitcast.37, ...), custom_call_target="tpu_custom_call" | custom-call | tf_op jit(solution)/shard_map/second_half/pallas_call | solution.py:241
  238.1 6.5 %all-to-all-start.2 = ((bf16[32,40,512]{2,1,0:T(8,128)(2,1)}), bf16[32,40,512]{2,1,0:T(8,128)(2,1)S(1)}, u32[]{:S(2)}, u32[]{:S(2)}) async-start(bf16[32,40,512]{2,1,0:T(8,128)(2,1)} %bitcast.27), calls=%async_computation.2 | async-start | bytes 2621440 | tf_op jit(solution)/shard_map/all_to_all | solution.py:21
  244.9 32.8 %all-to-all-done.2 = bf16[32,40,512]{2,1,0:T(8,128)(2,1)S(1)} async-done(((bf16[32,40,512]{2,1,0:T(8,128)(2,1)}), bf16[32,40,512]{2,1,0:T(8,128)(2,1)S(1)}, u32[]{:S(2)}, u32[]{:S(2)}) %all-to-all-start.2) | async-done | bytes 1310752 | tf_op jit(solution)/shard_map/all_to_all | solution.py:21
  278.5 1.5 fusion.6
  280.0 3.7 %all-to-all-start.3 = ((bf16[8,48,512]{2,1,0:T(8,128)(2,1)}), bf16[8,48,512]{2,1,0:T(8,128)(2,1)S(1)}, u32[]{:S(2)}, u32[]{:S(2)}) async-start(bf16[8,48,512]{2,1,0:T(8,128)(2,1)} %bitcast.14), calls=%async_computation.3 | async-start | bytes 786432 | tf_op jit(solution)/shard_map/all_to_all | solution.py:21
  283.7 50.6 %all-to-all-done.3 = bf16[8,48,512]{2,1,0:T(8,128)(2,1)S(1)} async-done(((bf16[8,48,512]{2,1,0:T(8,128)(2,1)}), bf16[8,48,512]{2,1,0:T(8,128)(2,1)S(1)}, u32[]{:S(2)}, u32[]{:S(2)}) %all-to-all-start.3) | async-done | bytes 393248 | tf_op jit(solution)/shard_map/all_to_all | solution.py:21
  334.7 1.9 fusion.5
  (52 shorter events, 8.8 us)
Async XLA Ops:
  2.4 109.2 %copy-start.3 = (bf16[1,2048,256]{2,1,0:T(8,128)(2,1)S(1)}, bf16[1,2048,256]{2,1,0:T(8,128)(2,1)}, u32[]{:S(2)}) copy-start(bf16[1,2048,256]{2,1,0:T(8,128)(2,1)} %param.15) | copy-start | bytes 3145732
  2.4 109.2 %copy-start.4 = (bf16[1,2048,256]{2,1,0:T(8,128)(2,1)S(1)}, bf16[1,2048,256]{2,1,0:T(8,128)(2,1)}, u32[]{:S(2)}) copy-start(bf16[1,2048,256]{2,1,0:T(8,128)(2,1)} %param.16) | copy-start | bytes 3145732
  84.1 119.8 %all-to-all-start.1 = ((bf16[32,40,512]{2,1,0:T(8,128)(2,1)}), bf16[32,40,512]{2,1,0:T(8,128)(2,1)S(1)}, u32[]{:S(2)}, u32[]{:S(2)}) async-start(bf16[32,40,512]{2,1,0:T(8,128)(2,1)} %bitcast.34), calls=%async_computation.1 | async-start | bytes 2621440 | tf_op jit(solution)/shard_map/all_to_all | solution.py:21
  111.6 6.9 %copy-start.7 = (bf16[1,1024,512]{2,1,0:T(8,128)(2,1)S(1)}, bf16[1,1024,512]{2,1,0:T(8,128)(2,1)}, u32[]{:S(2)}) copy-start(bf16[1,1024,512]{2,1,0:T(8,128)(2,1)} %param.17) | copy-start | bytes 3145732
  111.8 60.7 %collective-permute-start = (bf16[2048,512]{1,0:T(8,128)(2,1)S(1)}, bf16[2048,512]{1,0:T(8,128)(2,1)S(1)}, u32[]{:S(2)}, u32[]{:S(2)}) collective-permute-start(bf16[2048,512]{1,0:T(8,128)(2,1)S(1)} %pad_maximum_fusion), channel_id=1, source_target_pairs={{0,3},{1,0},{2,1},{3,2},{4,7},{5,4},{6,5},{7,6},{8,11},{9,8},{10,9... | collective-permute-start | bytes 6291464 | tf_op jit(solution)/shard_map/ppermute | solution.py:26
  116.5 61.7 %collective-permute-start.1 = (bf16[2048,512]{1,0:T(8,128)(2,1)S(1)}, bf16[2048,512]{1,0:T(8,128)(2,1)S(1)}, u32[]{:S(2)}, u32[]{:S(2)}) collective-permute-start(bf16[2048,512]{1,0:T(8,128)(2,1)S(1)} %pad_maximum_fusion), channel_id=1, source_target_pairs={{0,1},{1,2},{2,3},{3,0},{4,5},{5,6},{6,7},{7,4},{8,9},{9,10},{10,1... | collective-permute-start | bytes 6291464 | tf_op jit(solution)/shard_map/ppermute | solution.py:26
  118.5 76.4 %collective-permute-start.4 = (bf16[1024,512]{1,0:T(8,128)(2,1)S(1)}, bf16[1024,512]{1,0:T(8,128)(2,1)S(1)}, u32[]{:S(2)}, u32[]{:S(2)}) collective-permute-start(bf16[1024,512]{1,0:T(8,128)(2,1)S(1)} %bitcast.38), channel_id=1, source_target_pairs={{0,3},{1,0},{2,1},{3,2},{4,7},{5,4},{6,5},{7,6},{8,11},{9,8},{10,9... | collective-permute-start | bytes 3145736 | tf_op jit(solution)/shard_map/ppermute | solution.py:26
  123.1 77.3 %collective-permute-start.5 = (bf16[1024,512]{1,0:T(8,128)(2,1)S(1)}, bf16[1024,512]{1,0:T(8,128)(2,1)S(1)}, u32[]{:S(2)}, u32[]{:S(2)}) collective-permute-start(bf16[1024,512]{1,0:T(8,128)(2,1)S(1)} %bitcast.39), channel_id=1, source_target_pairs={{0,1},{1,2},{2,3},{3,0},{4,5},{5,6},{6,7},{7,4},{8,9},{9,10},{10,1... | collective-permute-start | bytes 3145736 | tf_op jit(solution)/shard_map/ppermute | solution.py:26
  172.4 6.9 %copy-start.1 = (bf16[2048,512]{1,0:T(8,128)(2,1)}, bf16[2048,512]{1,0:T(8,128)(2,1)S(1)}, u32[]{:S(2)}) copy-start(bf16[2048,512]{1,0:T(8,128)(2,1)S(1)} %collective-permute-done.refs_3_) | copy-start | bytes 6291460
  173.6 29.7 %copy-start.11 = (f32[2048]{0:T(1024)S(1)}, f32[2048]{0:T(1024)}, u32[]{:S(2)}) copy-start(f32[2048]{0:T(1024)} %param.14) | copy-start | bytes 24580
  173.6 57.0 %collective-permute-start.2 = (bf16[1024,512]{1,0:T(8,128)(2,1)}, bf16[1024,512]{1,0:T(8,128)(2,1)S(1)}, u32[]{:S(2)}, u32[]{:S(2)}) collective-permute-start(bf16[1024,512]{1,0:T(8,128)(2,1)} %slice.48), channel_id=1, source_target_pairs={{0,3},{1,0},{2,1},{3,2},{4,7},{5,4},{6,5},{7,6},{8,11},{9,8},{10,9... | collective-permute-start | bytes 3145736 | tf_op jit(solution)/shard_map/ppermute | solution.py:26
  178.2 23.1 %copy-start.2 = (bf16[2048,512]{1,0:T(8,128)(2,1)}, bf16[2048,512]{1,0:T(8,128)(2,1)S(1)}, u32[]{:S(2)}) copy-start(bf16[2048,512]{1,0:T(8,128)(2,1)S(1)} %collective-permute-done.1.refs_4_) | copy-start | bytes 6291460
  179.3 51.2 %collective-permute-start.3 = (bf16[1024,512]{1,0:T(8,128)(2,1)}, bf16[1024,512]{1,0:T(8,128)(2,1)S(1)}, u32[]{:S(2)}, u32[]{:S(2)}) collective-permute-start(bf16[1024,512]{1,0:T(8,128)(2,1)} %slice.49), channel_id=1, source_target_pairs={{0,1},{1,2},{2,3},{3,0},{4,5},{5,6},{6,7},{7,4},{8,9},{9,10},{10,1... | collective-permute-start | bytes 3145736 | tf_op jit(solution)/shard_map/ppermute | solution.py:26
  194.9 8.3 %copy-start.5 = (bf16[1024,512]{1,0:T(8,128)(2,1)}, bf16[1024,512]{1,0:T(8,128)(2,1)S(1)}, u32[]{:S(2)}) copy-start(bf16[1024,512]{1,0:T(8,128)(2,1)S(1)} %collective-permute-done.4.refs_5_) | copy-start | bytes 3145732
  195.8 32.9 %collective-permute-start.6 = (bf16[512,512]{1,0:T(8,128)(2,1)}, bf16[512,512]{1,0:T(8,128)(2,1)}, u32[]{:S(2)}, u32[]{:S(2)}) collective-permute-start(bf16[512,512]{1,0:T(8,128)(2,1)} %slice.50), channel_id=1, source_target_pairs={{0,3},{1,0},{2,1},{3,2},{4,7},{5,4},{6,5},{7,6},{8,11},{9,8},{10,9... | collective-permute-start | bytes 1572872 | tf_op jit(solution)/shard_map/ppermute | solution.py:26
  200.4 2.9 copy-start.6
  201.3 29.3 %collective-permute-start.7 = (bf16[512,512]{1,0:T(8,128)(2,1)}, bf16[512,512]{1,0:T(8,128)(2,1)}, u32[]{:S(2)}, u32[]{:S(2)}) collective-permute-start(bf16[512,512]{1,0:T(8,128)(2,1)} %slice.51), channel_id=1, source_target_pairs={{0,1},{1,2},{2,3},{3,0},{4,5},{5,6},{6,7},{7,4},{8,9},{9,10},{10,1... | collective-permute-start | bytes 1572872 | tf_op jit(solution)/shard_map/ppermute | solution.py:26
  230.5 1.3 copy-start.9
  238.1 6.5 %copy-start.13 = (s32[2,8,128]{2,1,0:T(8,128)S(1)}, s32[2,8,128]{2,1,0:T(8,128)}, u32[]{:S(2)}) copy-start(s32[2,8,128]{2,1,0:T(8,128)} %get-tuple-element.15) | copy-start | bytes 24580
  238.1 6.6 %copy-start.12 = (f32[2,8,128]{2,1,0:T(8,128)S(1)}, f32[2,8,128]{2,1,0:T(8,128)}, u32[]{:S(2)}) copy-start(f32[2,8,128]{2,1,0:T(8,128)} %get-tuple-element.14) | copy-start | bytes 24580
  238.1 39.7 %all-to-all-start.2 = ((bf16[32,40,512]{2,1,0:T(8,128)(2,1)}), bf16[32,40,512]{2,1,0:T(8,128)(2,1)S(1)}, u32[]{:S(2)}, u32[]{:S(2)}) async-start(bf16[32,40,512]{2,1,0:T(8,128)(2,1)} %bitcast.27), calls=%async_computation.2 | async-start | bytes 2621440 | tf_op jit(solution)/shard_map/all_to_all | solution.py:21
  278.5 5.2 %copy-start.14 = (s32[1,384]{1,0:T(1,128)S(1)}, s32[1,384]{1,0:T(1,128)}, u32[]{:S(2)}) copy-start(s32[1,384]{1,0:T(1,128)} %get-tuple-element.12) | copy-start | bytes 4612
  278.5 5.2 %copy-start.10 = (s32[384]{0:T(512)S(1)}, s32[384]{0:T(512)}, u32[]{:S(2)}) copy-start(s32[384]{0:T(512)} %group.1) | copy-start | bytes 4612
  280.0 54.3 %all-to-all-start.3 = ((bf16[8,48,512]{2,1,0:T(8,128)(2,1)}), bf16[8,48,512]{2,1,0:T(8,128)(2,1)S(1)}, u32[]{:S(2)}, u32[]{:S(2)}) async-start(bf16[8,48,512]{2,1,0:T(8,128)(2,1)} %bitcast.14), calls=%async_computation.3 | async-start | bytes 786432 | tf_op jit(solution)/shard_map/all_to_all | solution.py:21
  (2 other events, 2.1 us)

commit v6 on v5

--- a/solution.py
+++ b/solution.py
@@ -163,9 +163,10 @@
     return dot(whole[:, :half], top[...]) + dot(whole[:, half:], bottom[...])
 
 
-def first_half(me, gains, *refs):
-    given, (normed, hidden), (rows, *slots), semaphores = refs[:5], refs[5:7], refs[7:12], refs[12]
-    gate, up, one, three = slots
+def main_part(me, gains, *refs):
+    given, (hidden_out, results), (rows, *slots) = refs[:10], refs[10:12], refs[12:22]
+    normed, hidden, pieces, semaphores, leaving = refs[22:]
+    gate, up, one, three, top, bottom, *down = slots
     arrived, *copies = fetch(given, (rows, *slots), semaphores)
     parts, _, width = rows.shape
     units = gate.shape[1]
@@ -183,30 +184,36 @@
     copies[1].wait()
     piece = gated(dot(normed[...], gate[...]), dot(normed[...], up[...]))
     place(hidden, me, 0, parts, piece)
-    for copy, slot, offset in zip(copies[2:], (one, three), (1, 3), strict=True):
+    for copy, slot, offset in zip(copies[2:4], (one, three), (1, 3), strict=True):
         copy.wait()
         both = dot(normed[...], slot[...])
         place(hidden, me, offset, parts, gated(both[:, :units], both[:, units:]))
-
-
-def second_half(me, *refs):
-    given, results, slots, semaphores = refs[:9], refs[9], refs[10:19], refs[19]
-    copies = fetch(given, slots, semaphores)
-    normed, hidden, top, bottom, own, one, three, down_top, down_bottom = slots
-    parts = results.shape[0]
-    units = hidden.shape[1] // parts
-    for copy in copies[:4]:
-        copy.wait()
+    copies[4].wait()
+    copies[5].wait()
     both = by_halves(normed, top, bottom)
     place(hidden, me, 2, parts, gated(both[:, :units], both[:, units:]))
-    for copy, slot, offset in zip(copies[4:7], (own, one, three), (0, 1, 3), strict=True):
+    out = [pltpu.make_async_copy(hidden, hidden_out, leaving.at[3])]
+    out[0].start()
+    for i, offset in enumerate((0, 1, 3)):
+        copies[6 + i].wait()
+        pieces[i] = dot(hidden[...], down[i][...]).astype(pieces.dtype)
+        owner = lax.rem(me[0] + offset, parts)
+        out.append(pltpu.make_async_copy(pieces.at[i], results.at[owner], leaving.at[i]))
+        out[-1].start()
+    for copy in out:
         copy.wait()
-        owner = lax.rem(me[0] + offset, parts)
-        results[owner] = dot(hidden[...], slot[...]).astype(results.dtype)
-    copies[7].wait()
-    copies[8].wait()
-    owner = lax.rem(me[0] + 2, parts)
-    results[owner] = by_halves(hidden, down_top, down_bottom).astype(results.dtype)
+
+
+def last_part(me, *refs):
+    given, results, slots, piece, semaphores = refs[:3], refs[4], refs[5:8], refs[8], refs[9]
+    for copy in fetch(given, slots, semaphores):
+        copy.wait()
+    hidden, top, bottom = slots
+    piece[...] = by_halves(hidden, top, bottom).astype(piece.dtype)
+    owner = lax.rem(me[0] + 2, results.shape[0])
+    copy = pltpu.make_async_copy(piece, results.at[owner], semaphores.at[3])
+    copy.start()
+    copy.wait()
 
 
 VMEM = pl.BlockSpec(memory_space=pltpu.VMEM)
@@ -227,25 +234,31 @@
     units = gate.shape[1]
     me = me.reshape(1)
     near, far = gate_up_ring
-    given = [rows, gate, up, *near]
-    normed, hidden = pl.pallas_call(
-        first_half,
-        out_shape=(shaped((count, parts * width)), shaped((count, parts * units))),
+    near_down, far_down = down_ring
+    given = [rows, gate, up, *near, *far, down, *near_down]
+    whole = shaped((count, parts * units))
+    hidden, results = pl.pallas_call(
+        main_part,
+        out_shape=(whole, shaped((parts, count, width))),
         in_specs=[SMEM, VMEM] + [HBM] * len(given),
-        out_specs=(VMEM, VMEM),
-        scratch_shapes=slots_for(given) + [pltpu.SemaphoreType.DMA((len(given),))],
-        name="first_half",
+        out_specs=(HBM, HBM),
+        scratch_shapes=slots_for(given)
+        + slots_for([shaped((count, parts * width)), whole, shaped((3, count, width))])
+        + [pltpu.SemaphoreType.DMA((len(given),)), pltpu.SemaphoreType.DMA((4,))],
+        name="main_part",
     )(me, norm_gain.reshape(parts, width), *given)
-    near, far_down = down_ring
-    given = [normed, hidden, *far, down, *near, *far_down]
+    given = [hidden, *far_down]
     return pl.pallas_call(
-        second_half,
+        last_part,
         out_shape=shaped((parts, count, width)),
-        in_specs=[SMEM] + [HBM] * len(given),
-        out_specs=VMEM,
-        scratch_shapes=slots_for(given) + [pltpu.SemaphoreType.DMA((len(given),))],
-        name="second_half",
-    )(me, *given)
+        in_specs=[SMEM] + [HBM] * 4,
+        out_specs=HBM,
+        input_output_aliases={4: 0},
+        scratch_shapes=slots_for(given)
+        + slots_for([shaped((count, width))])
+        + [pltpu.SemaphoreType.DMA((4,))],
+        name="last_part",
+    )(me, *given, results)
 
 
 def layer(

time: 338 us -> 333 us (0.985)
  local copies, waits for them, and re-layouts: 7.43 us -> 4.03 us
  transfers between devices with their start and end apart: 11 -> 11, of which waited for: 6 -> 7; matrix products, arithmetic and copies ran while one was open for 2% -> 1% of each run, Pallas kernels for 2% -> 3%
where the time goes in v6:
time: 333 us; the launch traced here: 332 us
  waiting for transfers between devices  164 us (49%)
  blocking collectives  78.8 us (24%)
  starting transfers between devices  64 us (19%)
  Pallas kernels  16.3 us (5%)
  matrix products  4.48 us (1%)
  local copies, waits for them, and re-layouts  4.03 us (1%)
    all_to_all x3, waiting for transfers between devices, exchange(): return lax.all_to_all(array, axis, 0, 0, tiled=True)  83.4 us
    ppermute x8, waiting for transfers between devices, shifted(): lax.ppermute(array, axis, [(a, (a + by) % length) for a in range(length)])  80.1 us
    all_to_all x1, blocking collectives, exchange(): return lax.all_to_all(array, axis, 0, 0, tiled=True)  78.8 us
    all_to_all x3, starting transfers between devices, exchange(): return lax.all_to_all(array, axis, 0, 0, tiled=True)  37.6 us
    ppermute x8, starting transfers between devices, shifted(): lax.ppermute(array, axis, [(a, (a + by) % length) for a in range(length)])  26.4 us
    pallas_call x1, Pallas kernels, expert(): pl.pallas_call(main_part, out_shape=(whole, shaped((parts, count, width))...  8.46 us
  transfers between devices with their start and end apart: 11, of which 7 were waited for; matrix products, arithmetic and copies ran while one was open for 1% of the time, Pallas kernels for 3%

profile of v6, /device:TPU:33, one launch (start us, length us, event | category | flops | bytes accessed | tf_op | source)
XLA Modules:
  0.0 331.7 jit_solution(9337580677490500721)
XLA Ops:
  0.0 2.3 depart.1
  2.3 78.8 %all_to_all.20.landed = bf16[8,200,128]{2,1,0:T(8,128)(2,1)} all-to-all(bf16[8,200,128]{2,1,0:T(8,128)(2,1)} %get-tuple-element.13), channel_id=1, replica_groups=mesh['grp'=2,'g'=8,'m'=8,'tp'=4] {'g'}, dimensions={0} | all-to-all | bytes 819200 | tf_op jit(solution)/shard_map/all_to_all | solution.py:21
  81.2 2.9 arrive.1
  84.0 27.5 %all-to-all-start.1 = ((bf16[32,40,512]{2,1,0:T(8,128)(2,1)}), bf16[32,40,512]{2,1,0:T(8,128)(2,1)S(1)}, u32[]{:S(2)}, u32[]{:S(2)}) async-start(bf16[32,40,512]{2,1,0:T(8,128)(2,1)} %bitcast.34), calls=%async_computation.1 | async-start | bytes 2621440 | tf_op jit(solution)/shard_map/all_to_all | solution.py:21
  111.7 4.8 %collective-permute-start = (bf16[2048,512]{1,0:T(8,128)(2,1)S(1)}, bf16[2048,512]{1,0:T(8,128)(2,1)S(1)}, u32[]{:S(2)}, u32[]{:S(2)}) collective-permute-start(bf16[2048,512]{1,0:T(8,128)(2,1)S(1)} %pad_maximum_fusion), channel_id=1, source_target_pairs={{0,3},{1,0},{2,1},{3,2},{4,7},{5,4},{6,5},{7,6},{8,11},{9,8},{10,9... | collective-permute-start | bytes 6291464 | tf_op jit(solution)/shard_map/ppermute | solution.py:26
  116.5 2.0 collective-permute-start.1
  118.5 4.6 %collective-permute-start.4 = (bf16[1024,512]{1,0:T(8,128)(2,1)S(1)}, bf16[1024,512]{1,0:T(8,128)(2,1)S(1)}, u32[]{:S(2)}, u32[]{:S(2)}) collective-permute-start(bf16[1024,512]{1,0:T(8,128)(2,1)S(1)} %bitcast.38), channel_id=1, source_target_pairs={{0,3},{1,0},{2,1},{3,2},{4,7},{5,4},{6,5},{7,6},{8,11},{9,8},{10,9... | collective-permute-start | bytes 3145736 | tf_op jit(solution)/shard_map/ppermute | solution.py:26
  123.1 2.0 collective-permute-start.5
  125.1 47.4 %collective-permute-done.refs_3_ = bf16[2048,512]{1,0:T(8,128)(2,1)S(1)} collective-permute-done((bf16[2048,512]{1,0:T(8,128)(2,1)S(1)}, bf16[2048,512]{1,0:T(8,128)(2,1)S(1)}, u32[]{:S(2)}, u32[]{:S(2)}) %collective-permute-start) | collective-permute-done | bytes 2097184 | tf_op jit(solution)/shard_map/ppermute | solution.py:26
  172.5 4.7 %collective-permute-start.2 = (bf16[1024,512]{1,0:T(8,128)(2,1)S(1)}, bf16[1024,512]{1,0:T(8,128)(2,1)}, u32[]{:S(2)}, u32[]{:S(2)}) collective-permute-start(bf16[1024,512]{1,0:T(8,128)(2,1)S(1)} %slice.48), channel_id=1, source_target_pairs={{0,3},{1,0},{2,1},{3,2},{4,7},{5,4},{6,5},{7,6},{8,11},{9,8},{10,9... | collective-permute-start | bytes 3145736 | tf_op jit(solution)/shard_map/ppermute | solution.py:26
  177.3 2.0 collective-permute-start.3
  179.2 15.6 %collective-permute-done.4.refs_8_ = bf16[1024,512]{1,0:T(8,128)(2,1)S(1)} collective-permute-done((bf16[1024,512]{1,0:T(8,128)(2,1)S(1)}, bf16[1024,512]{1,0:T(8,128)(2,1)S(1)}, u32[]{:S(2)}, u32[]{:S(2)}) %collective-permute-start.4) | collective-permute-done | bytes 1048608 | tf_op jit(solution)/shard_map/ppermute | solution.py:26
  195.8 4.5 %collective-permute-start.6 = (bf16[512,512]{1,0:T(8,128)(2,1)}, bf16[512,512]{1,0:T(8,128)(2,1)}, u32[]{:S(2)}, u32[]{:S(2)}) collective-permute-start(bf16[512,512]{1,0:T(8,128)(2,1)} %slice.50), channel_id=1, source_target_pairs={{0,3},{1,0},{2,1},{3,2},{4,7},{5,4},{6,5},{7,6},{8,11},{9,8},{10,9... | collective-permute-start | bytes 1572872 | tf_op jit(solution)/shard_map/ppermute | solution.py:26
  201.3 1.9 collective-permute-start.7
  203.8 13.6 %collective-permute-done.2.refs_5_ = bf16[1024,512]{1,0:T(8,128)(2,1)} collective-permute-done((bf16[1024,512]{1,0:T(8,128)(2,1)S(1)}, bf16[1024,512]{1,0:T(8,128)(2,1)}, u32[]{:S(2)}, u32[]{:S(2)}) %collective-permute-start.2) | collective-permute-done | bytes 1048608 | tf_op jit(solution)/shard_map/ppermute | solution.py:26
  217.5 1.8 collective-permute-done.3.refs_6_
  220.4 8.5 %main_part.1 = (bf16[320,1024]{1,0:T(8,128)(2,1)}, bf16[4,320,512]{2,1,0:T(8,128)(2,1)}) custom-call(s32[1]{0:T(128)} %bitcast.4.me, f32[4,512]{1,0:T(4,128)} %reshape.32.gains, bf16[4,320,512]{2,1,0:T(8,128)(2,1)} %bitcast.28, bf16[2048,256]{1,0:T(8,128)(2,1)} %bitcast.29, bf16[2048,256]{1,0:T(8,128)(2,1)} %bitcast.31, bf16[2048,512]{1,0:T(8,128)(2,1)} %copy-done.1, ...), custom_call_target="tpu_custom_call" | custom-call | tf_op jit(solution)/shard_map/main_part/pallas_call | solution.py:240
  228.9 1.6 collective-permute-done.7.refs_2_
  230.5 2.7 last_part.1
  233.2 6.5 %all-to-all-start.2 = ((bf16[32,40,512]{2,1,0:T(8,128)(2,1)}), bf16[32,40,512]{2,1,0:T(8,128)(2,1)S(1)}, u32[]{:S(2)}, u32[]{:S(2)}) async-start(bf16[32,40,512]{2,1,0:T(8,128)(2,1)} %bitcast.27), calls=%async_computation.2 | async-start | bytes 2621440 | tf_op jit(solution)/shard_map/all_to_all | solution.py:21
  240.0 32.8 %all-to-all-done.2 = bf16[32,40,512]{2,1,0:T(8,128)(2,1)S(1)} async-done(((bf16[32,40,512]{2,1,0:T(8,128)(2,1)}), bf16[32,40,512]{2,1,0:T(8,128)(2,1)S(1)}, u32[]{:S(2)}, u32[]{:S(2)}) %all-to-all-start.2) | async-done | bytes 1310752 | tf_op jit(solution)/shard_map/all_to_all | solution.py:21
  275.1 3.7 %all-to-all-start.3 = ((bf16[8,48,512]{2,1,0:T(8,128)(2,1)}), bf16[8,48,512]{2,1,0:T(8,128)(2,1)S(1)}, u32[]{:S(2)}, u32[]{:S(2)}) async-start(bf16[8,48,512]{2,1,0:T(8,128)(2,1)} %bitcast.14), calls=%async_computation.3 | async-start | bytes 786432 | tf_op jit(solution)/shard_map/all_to_all | solution.py:21
  278.8 50.6 %all-to-all-done.3 = bf16[8,48,512]{2,1,0:T(8,128)(2,1)S(1)} async-done(((bf16[8,48,512]{2,1,0:T(8,128)(2,1)}), bf16[8,48,512]{2,1,0:T(8,128)(2,1)S(1)}, u32[]{:S(2)}, u32[]{:S(2)}) %all-to-all-start.3) | async-done | bytes 393248 | tf_op jit(solution)/shard_map/all_to_all | solution.py:21
  329.9 1.9 fusion.5
  (48 shorter events, 6.8 us)
Async XLA Ops:
  2.3 109.2 %copy-start.3 = (bf16[1,2048,256]{2,1,0:T(8,128)(2,1)S(1)}, bf16[1,2048,256]{2,1,0:T(8,128)(2,1)}, u32[]{:S(2)}) copy-start(bf16[1,2048,256]{2,1,0:T(8,128)(2,1)} %param.15) | copy-start | bytes 3145732
  2.3 109.2 %copy-start.4 = (bf16[1,2048,256]{2,1,0:T(8,128)(2,1)S(1)}, bf16[1,2048,256]{2,1,0:T(8,128)(2,1)}, u32[]{:S(2)}) copy-start(bf16[1,2048,256]{2,1,0:T(8,128)(2,1)} %param.16) | copy-start | bytes 3145732
  84.0 135.2 %all-to-all-start.1 = ((bf16[32,40,512]{2,1,0:T(8,128)(2,1)}), bf16[32,40,512]{2,1,0:T(8,128)(2,1)S(1)}, u32[]{:S(2)}, u32[]{:S(2)}) async-start(bf16[32,40,512]{2,1,0:T(8,128)(2,1)} %bitcast.34), calls=%async_computation.1 | async-start | bytes 2621440 | tf_op jit(solution)/shard_map/all_to_all | solution.py:21
  111.6 6.9 %copy-start.7 = (bf16[1,1024,512]{2,1,0:T(8,128)(2,1)S(1)}, bf16[1,1024,512]{2,1,0:T(8,128)(2,1)}, u32[]{:S(2)}) copy-start(bf16[1,1024,512]{2,1,0:T(8,128)(2,1)} %param.17) | copy-start | bytes 3145732
  111.7 60.7 %collective-permute-start = (bf16[2048,512]{1,0:T(8,128)(2,1)S(1)}, bf16[2048,512]{1,0:T(8,128)(2,1)S(1)}, u32[]{:S(2)}, u32[]{:S(2)}) collective-permute-start(bf16[2048,512]{1,0:T(8,128)(2,1)S(1)} %pad_maximum_fusion), channel_id=1, source_target_pairs={{0,3},{1,0},{2,1},{3,2},{4,7},{5,4},{6,5},{7,6},{8,11},{9,8},{10,9... | collective-permute-start | bytes 6291464 | tf_op jit(solution)/shard_map/ppermute | solution.py:26
  116.5 60.7 %collective-permute-start.1 = (bf16[2048,512]{1,0:T(8,128)(2,1)S(1)}, bf16[2048,512]{1,0:T(8,128)(2,1)S(1)}, u32[]{:S(2)}, u32[]{:S(2)}) collective-permute-start(bf16[2048,512]{1,0:T(8,128)(2,1)S(1)} %pad_maximum_fusion), channel_id=1, source_target_pairs={{0,1},{1,2},{2,3},{3,0},{4,5},{5,6},{6,7},{7,4},{8,9},{9,10},{10,1... | collective-permute-start | bytes 6291464 | tf_op jit(solution)/shard_map/ppermute | solution.py:26
  118.5 76.4 %collective-permute-start.4 = (bf16[1024,512]{1,0:T(8,128)(2,1)S(1)}, bf16[1024,512]{1,0:T(8,128)(2,1)S(1)}, u32[]{:S(2)}, u32[]{:S(2)}) collective-permute-start(bf16[1024,512]{1,0:T(8,128)(2,1)S(1)} %bitcast.38), channel_id=1, source_target_pairs={{0,3},{1,0},{2,1},{3,2},{4,7},{5,4},{6,5},{7,6},{8,11},{9,8},{10,9... | collective-permute-start | bytes 3145736 | tf_op jit(solution)/shard_map/ppermute | solution.py:26
  123.1 77.2 %collective-permute-start.5 = (bf16[1024,512]{1,0:T(8,128)(2,1)S(1)}, bf16[1024,512]{1,0:T(8,128)(2,1)S(1)}, u32[]{:S(2)}, u32[]{:S(2)}) collective-permute-start(bf16[1024,512]{1,0:T(8,128)(2,1)S(1)} %bitcast.39), channel_id=1, source_target_pairs={{0,1},{1,2},{2,3},{3,0},{4,5},{5,6},{6,7},{7,4},{8,9},{9,10},{10,1... | collective-permute-start | bytes 3145736 | tf_op jit(solution)/shard_map/ppermute | solution.py:26
  172.4 4.9 %copy-start.1 = (bf16[2048,512]{1,0:T(8,128)(2,1)}, bf16[2048,512]{1,0:T(8,128)(2,1)S(1)}, u32[]{:S(2)}) copy-start(bf16[2048,512]{1,0:T(8,128)(2,1)S(1)} %collective-permute-done.refs_3_) | copy-start | bytes 6291460
  172.5 30.7 %copy-start.9 = (f32[2048]{0:T(1024)S(1)}, f32[2048]{0:T(1024)}, u32[]{:S(2)}) copy-start(f32[2048]{0:T(1024)} %param.14) | copy-start | bytes 24580
  172.5 45.0 %collective-permute-start.2 = (bf16[1024,512]{1,0:T(8,128)(2,1)S(1)}, bf16[1024,512]{1,0:T(8,128)(2,1)}, u32[]{:S(2)}, u32[]{:S(2)}) collective-permute-start(bf16[1024,512]{1,0:T(8,128)(2,1)S(1)} %slice.48), channel_id=1, source_target_pairs={{0,3},{1,0},{2,1},{3,2},{4,7},{5,4},{6,5},{7,6},{8,11},{9,8},{10,9... | collective-permute-start | bytes 3145736 | tf_op jit(solution)/shard_map/ppermute | solution.py:26
  177.2 24.1 %copy-start.2 = (bf16[2048,512]{1,0:T(8,128)(2,1)}, bf16[2048,512]{1,0:T(8,128)(2,1)S(1)}, u32[]{:S(2)}) copy-start(bf16[2048,512]{1,0:T(8,128)(2,1)S(1)} %collective-permute-done.1.refs_4_) | copy-start | bytes 6291460
  177.3 42.0 %collective-permute-start.3 = (bf16[1024,512]{1,0:T(8,128)(2,1)S(1)}, bf16[1024,512]{1,0:T(8,128)(2,1)}, u32[]{:S(2)}, u32[]{:S(2)}) collective-permute-start(bf16[1024,512]{1,0:T(8,128)(2,1)S(1)} %slice.49), channel_id=1, source_target_pairs={{0,1},{1,2},{2,3},{3,0},{4,5},{5,6},{6,7},{7,4},{8,9},{9,10},{10,1... | collective-permute-start | bytes 3145736 | tf_op jit(solution)/shard_map/ppermute | solution.py:26
  194.9 8.3 %copy-start.5 = (bf16[1024,512]{1,0:T(8,128)(2,1)}, bf16[1024,512]{1,0:T(8,128)(2,1)S(1)}, u32[]{:S(2)}) copy-start(bf16[1024,512]{1,0:T(8,128)(2,1)S(1)} %collective-permute-done.4.refs_8_) | copy-start | bytes 3145732
  195.8 33.1 %collective-permute-start.6 = (bf16[512,512]{1,0:T(8,128)(2,1)}, bf16[512,512]{1,0:T(8,128)(2,1)}, u32[]{:S(2)}, u32[]{:S(2)}) collective-permute-start(bf16[512,512]{1,0:T(8,128)(2,1)} %slice.50), channel_id=1, source_target_pairs={{0,3},{1,0},{2,1},{3,2},{4,7},{5,4},{6,5},{7,6},{8,11},{9,8},{10,9... | collective-permute-start | bytes 1572872 | tf_op jit(solution)/shard_map/ppermute | solution.py:26
  200.3 2.9 copy-start.6
  201.3 29.3 %collective-permute-start.7 = (bf16[512,512]{1,0:T(8,128)(2,1)}, bf16[512,512]{1,0:T(8,128)(2,1)}, u32[]{:S(2)}, u32[]{:S(2)}) collective-permute-start(bf16[512,512]{1,0:T(8,128)(2,1)} %slice.51), channel_id=1, source_target_pairs={{0,1},{1,2},{2,3},{3,0},{4,5},{5,6},{6,7},{7,4},{8,9},{9,10},{10,1... | collective-permute-start | bytes 1572872 | tf_op jit(solution)/shard_map/ppermute | solution.py:26
  219.3 1.1 copy-start
  233.2 6.5 %copy-start.11 = (s32[2,8,128]{2,1,0:T(8,128)S(1)}, s32[2,8,128]{2,1,0:T(8,128)}, u32[]{:S(2)}) copy-start(s32[2,8,128]{2,1,0:T(8,128)} %get-tuple-element.15) | copy-start | bytes 24580
  233.2 6.6 %copy-start.10 = (f32[2,8,128]{2,1,0:T(8,128)S(1)}, f32[2,8,128]{2,1,0:T(8,128)}, u32[]{:S(2)}) copy-start(f32[2,8,128]{2,1,0:T(8,128)} %get-tuple-element.14) | copy-start | bytes 24580
  233.2 39.7 %all-to-all-start.2 = ((bf16[32,40,512]{2,1,0:T(8,128)(2,1)}), bf16[32,40,512]{2,1,0:T(8,128)(2,1)S(1)}, u32[]{:S(2)}, u32[]{:S(2)}) async-start(bf16[32,40,512]{2,1,0:T(8,128)(2,1)} %bitcast.27), calls=%async_computation.2 | async-start | bytes 2621440 | tf_op jit(solution)/shard_map/all_to_all | solution.py:21
  273.6 5.2 %copy-start.12 = (s32[1,384]{1,0:T(1,128)S(1)}, s32[1,384]{1,0:T(1,128)}, u32[]{:S(2)}) copy-start(s32[1,384]{1,0:T(1,128)} %get-tuple-element.12) | copy-start | bytes 4612
  273.6 5.2 %copy-start.8 = (s32[384]{0:T(512)S(1)}, s32[384]{0:T(512)}, u32[]{:S(2)}) copy-start(s32[384]{0:T(512)} %group.1) | copy-start | bytes 4612
  275.1 54.3 %all-to-all-start.3 = ((bf16[8,48,512]{2,1,0:T(8,128)(2,1)}), bf16[8,48,512]{2,1,0:T(8,128)(2,1)S(1)}, u32[]{:S(2)}, u32[]{:S(2)}) async-start(bf16[8,48,512]{2,1,0:T(8,128)(2,1)} %bitcast.14), calls=%async_computation.3 | async-start | bytes 786432 | tf_op jit(solution)/shard_map/all_to_all | solution.py:21

commit v7 on v6

--- a/solution.py
+++ b/solution.py
@@ -66,7 +66,11 @@
     return jnp.where(condition, 1.0, 0.0).astype(jnp.bfloat16)
 
 
-def depart(group, choice, group_share, expert_share, tokens, blocks, ranks):
+def depart(group, choice, group_share, expert_share, tokens, gate, up, *refs):
+    blocks, ranks, joined, semaphores = refs
+    units = gate.shape[1]
+    sides = joined.at[:, pl.ds(0, units)], joined.at[:, pl.ds(units, units)]
+    joining = fetch((gate, up), sides, semaphores)
     groups, _, lanes = blocks.shape
     count, width = tokens.shape
     chunks, per_group = width // lanes, count // groups
@@ -97,6 +101,8 @@
             piece = seated[g * per_group : (g + 1) * per_group, c * lanes : (c + 1) * lanes]
             blocks[g, c * per_group : (c + 1) * per_group, :] = piece
         blocks[g, chunks * per_group :, :] = told[g * TILE : (g + 1) * TILE]
+    for copy in joining:
+        copy.wait()
 
 
 def arrive(capacity, landed, buffer, places, shares, seats):
@@ -283,19 +289,21 @@
     chunks = piece_width // LANES
     depth = up_to(groups // tp_count * capacity, TILE)
 
-    gate_up_ring = around(jnp.concatenate([w_gate[0], w_up[0]], 1), "tp")
-    down_ring = around(w_down[0], "tp")
-
-    blocks, rank = pl.pallas_call(
+    gate, up, down = w_gate[0], w_up[0], w_down[0]
+    blocks, rank, joined = pl.pallas_call(
         depart,
         out_shape=(
             shaped((groups, chunks * per_group + TILE, LANES)),
             shaped((1, tok_rows), jnp.int32),
+            shaped((gate.shape[0], 2 * gate.shape[1])),
         ),
-        in_specs=[VMEM] * 5,
-        out_specs=(VMEM, VMEM),
+        in_specs=[VMEM] * 5 + [HBM] * 2,
+        out_specs=(VMEM, VMEM, HBM),
+        scratch_shapes=[pltpu.SemaphoreType.DMA((2,))],
         name="depart",
-    )(group_choice, expert_choice.T, group_weight, expert_weight.T, tokens)
+    )(group_choice, expert_choice.T, group_weight, expert_weight.T, tokens, gate, up)
+    gate_up_ring = around(joined, "tp")
+    down_ring = around(down, "tp")
     rank = rank[0]
     landed = exchange(blocks, "g")
 
@@ -314,9 +322,7 @@
     )(landed)
     rows = exchange(buffer.reshape(tp_count * members, depth, piece_width), BLOCK)
     rows = rows.reshape(tp_count, members * depth, piece_width)
-    results = expert(
-        rows, norm_gain, w_gate[0], w_up[0], w_down[0], gate_up_ring, down_ring, me
-    )
+    results = expert(rows, norm_gain, gate, up, down, gate_up_ring, down_ring, me)
 
     returned = exchange(results.reshape(tp_count * members, depth, piece_width), BLOCK)
     returned = returned.reshape(-1, piece_width)

time: 333 us -> 397 us (1.19)
  Pallas kernels: 16.3 us -> 80.5 us
    pallas_call x1, Pallas kernels: 2.34 us -> 66.5 us  [layer(): pl.pallas_call(depart, out_shape=(shaped((groups, chunks * per_group + TI...]
  transfers between devices with their start and end apart: 11 -> 11, of which waited for: 7 -> 7; matrix products, arithmetic and copies ran while one was open for 1% -> 1% of each run, Pallas kernels for 3% -> 2%
where the time goes in v7:
time: 397 us; the launch traced here: 396 us
  waiting for transfers between devices  163 us (41%)
  Pallas kernels  80.5 us (20%)
  blocking collectives  78.7 us (20%)
  starting transfers between devices  63.8 us (16%)
  local copies, waits for them, and re-layouts  4.9 us (1%)
  matrix products  4.46 us (1%)
    all_to_all x3, waiting for transfers between devices, exchange(): return lax.all_to_all(array, axis, 0, 0, tiled=True)  83.3 us
    ppermute x8, waiting for transfers between devices, shifted(): lax.ppermute(array, axis, [(a, (a + by) % length) for a in range(length)])  79.6 us
    all_to_all x1, blocking collectives, exchange(): return lax.all_to_all(array, axis, 0, 0, tiled=True)  78.7 us
    pallas_call x1, Pallas kernels, layer(): pl.pallas_call(depart, out_shape=(shaped((groups, chunks * per_group + TI...  66.5 us
    all_to_all x3, starting transfers between devices, exchange(): return lax.all_to_all(array, axis, 0, 0, tiled=True)  37.6 us
    ppermute x8, starting transfers between devices, shifted(): lax.ppermute(array, axis, [(a, (a + by) % length) for a in range(length)])  26.2 us
    pallas_call x1, Pallas kernels, expert(): pl.pallas_call(main_part, out_shape=(whole, shaped((parts, count, width))...  8.46 us
  transfers between devices with their start and end apart: 11, of which 7 were waited for; matrix products, arithmetic and copies ran while one was open for 1% of the time, Pallas kernels for 2%

profile of v7, /device:TPU:33, one launch (start us, length us, event | category | flops | bytes accessed | tf_op | source)
XLA Modules:
  0.0 395.6 jit_solution(2371726299423565720)
XLA Ops:
  0.0 66.5 %depart.1 = (bf16[8,200,128]{2,1,0:T(8,128)(2,1)}, s32[1,384]{1,0:T(1,128)}, bf16[2048,512]{1,0:T(8,128)(2,1)}) custom-call(s32[384]{0:T(512)} %group.1, s32[2,384]{1,0:T(2,128)} %bitcast.41, f32[384]{0:T(512)} %group_share.1, f32[2,384]{1,0:T(2,128)} %bitcast.42, bf16[384,512]{1,0:T(8,128)(2,1)} %tokens.1, bf16[2048,256]{1,0:T(8,128)(2,1)} %bitcast.29, ...), custom_call_target="tpu_custom_call" | custom-call | tf_op jit(solution)/shard_map/depart/pallas_call | solution.py:293
  66.5 78.7 %all_to_all.20.landed = bf16[8,200,128]{2,1,0:T(8,128)(2,1)} all-to-all(bf16[8,200,128]{2,1,0:T(8,128)(2,1)} %get-tuple-element.14), channel_id=1, replica_groups=mesh['grp'=2,'g'=8,'m'=8,'tp'=4] {'g'}, dimensions={0} | all-to-all | bytes 819200 | tf_op jit(solution)/shard_map/all_to_all | solution.py:21
  145.2 2.9 arrive.1
  148.0 27.5 %all-to-all-start.1 = ((bf16[32,40,512]{2,1,0:T(8,128)(2,1)}), bf16[32,40,512]{2,1,0:T(8,128)(2,1)S(1)}, u32[]{:S(2)}, u32[]{:S(2)}) async-start(bf16[32,40,512]{2,1,0:T(8,128)(2,1)} %bitcast.34), calls=%async_computation.1 | async-start | bytes 2621440 | tf_op jit(solution)/shard_map/all_to_all | solution.py:21
  175.5 4.6 %collective-permute-start = (bf16[2048,512]{1,0:T(8,128)(2,1)}, bf16[2048,512]{1,0:T(8,128)(2,1)S(1)}, u32[]{:S(2)}, u32[]{:S(2)}) collective-permute-start(bf16[2048,512]{1,0:T(8,128)(2,1)} %get-tuple-element.18), channel_id=1, source_target_pairs={{0,3},{1,0},{2,1},{3,2},{4,7},{5,4},{6,5},{7,6},{8,11},{9,8},{10,9... | collective-permute-start | bytes 6291464 | tf_op jit(solution)/shard_map/ppermute | solution.py:26
  180.2 2.0 collective-permute-start.1
  182.2 4.6 %collective-permute-start.4 = (bf16[1024,512]{1,0:T(8,128)(2,1)}, bf16[1024,512]{1,0:T(8,128)(2,1)S(1)}, u32[]{:S(2)}, u32[]{:S(2)}) collective-permute-start(bf16[1024,512]{1,0:T(8,128)(2,1)} %bitcast.9.refs_7_), channel_id=1, source_target_pairs={{0,3},{1,0},{2,1},{3,2},{4,7},{5,4},{6,5},{7,6},{8,11},{9,8},{10,9... | collective-permute-start | bytes 3145736 | tf_op jit(solution)/shard_map/ppermute | solution.py:26
  186.8 2.0 collective-permute-start.5
  188.7 47.7 %collective-permute-done.refs_3_ = bf16[2048,512]{1,0:T(8,128)(2,1)S(1)} collective-permute-done((bf16[2048,512]{1,0:T(8,128)(2,1)}, bf16[2048,512]{1,0:T(8,128)(2,1)S(1)}, u32[]{:S(2)}, u32[]{:S(2)}) %collective-permute-start) | collective-permute-done | bytes 2097184 | tf_op jit(solution)/shard_map/ppermute | solution.py:26
  236.5 4.5 %collective-permute-start.2 = (bf16[1024,512]{1,0:T(8,128)(2,1)S(1)}, bf16[1024,512]{1,0:T(8,128)(2,1)}, u32[]{:S(2)}, u32[]{:S(2)}) collective-permute-start(bf16[1024,512]{1,0:T(8,128)(2,1)S(1)} %slice.48), channel_id=1, source_target_pairs={{0,3},{1,0},{2,1},{3,2},{4,7},{5,4},{6,5},{7,6},{8,11},{9,8},{10,9... | collective-permute-start | bytes 3145736 | tf_op jit(solution)/shard_map/ppermute | solution.py:26
  241.2 2.1 collective-permute-start.3
  243.3 15.6 %collective-permute-done.4.refs_8_ = bf16[1024,512]{1,0:T(8,128)(2,1)S(1)} collective-permute-done((bf16[1024,512]{1,0:T(8,128)(2,1)}, bf16[1024,512]{1,0:T(8,128)(2,1)S(1)}, u32[]{:S(2)}, u32[]{:S(2)}) %collective-permute-start.4) | collective-permute-done | bytes 1048608 | tf_op jit(solution)/shard_map/ppermute | solution.py:26
  259.8 4.5 %collective-permute-start.6 = (bf16[512,512]{1,0:T(8,128)(2,1)}, bf16[512,512]{1,0:T(8,128)(2,1)}, u32[]{:S(2)}, u32[]{:S(2)}) collective-permute-start(bf16[512,512]{1,0:T(8,128)(2,1)} %slice.50), channel_id=1, source_target_pairs={{0,3},{1,0},{2,1},{3,2},{4,7},{5,4},{6,5},{7,6},{8,11},{9,8},{10,9... | collective-permute-start | bytes 1572872 | tf_op jit(solution)/shard_map/ppermute | solution.py:26
  266.2 1.9 collective-permute-start.7
  268.7 12.7 %collective-permute-done.2.refs_5_ = bf16[1024,512]{1,0:T(8,128)(2,1)} collective-permute-done((bf16[1024,512]{1,0:T(8,128)(2,1)S(1)}, bf16[1024,512]{1,0:T(8,128)(2,1)}, u32[]{:S(2)}, u32[]{:S(2)}) %collective-permute-start.2) | collective-permute-done | bytes 1048608 | tf_op jit(solution)/shard_map/ppermute | solution.py:26
  281.5 1.9 collective-permute-done.3.refs_6_
  284.4 8.5 %main_part.1 = (bf16[320,1024]{1,0:T(8,128)(2,1)}, bf16[4,320,512]{2,1,0:T(8,128)(2,1)}) custom-call(s32[1]{0:T(128)} %bitcast.6.me, f32[4,512]{1,0:T(4,128)} %reshape.32.gains, bf16[4,320,512]{2,1,0:T(8,128)(2,1)} %bitcast.28, bf16[2048,256]{1,0:T(8,128)(2,1)} %bitcast.30, bf16[2048,256]{1,0:T(8,128)(2,1)} %bitcast.32, bf16[2048,512]{1,0:T(8,128)(2,1)} %copy-done.1, ...), custom_call_target="tpu_custom_call" | custom-call | tf_op jit(solution)/shard_map/main_part/pallas_call | solution.py:246
  292.9 1.7 collective-permute-done.7.refs_2_
  294.6 2.7 last_part.1
  297.3 6.4 %all-to-all-start.2 = ((bf16[32,40,512]{2,1,0:T(8,128)(2,1)}), bf16[32,40,512]{2,1,0:T(8,128)(2,1)S(1)}, u32[]{:S(2)}, u32[]{:S(2)}) async-start(bf16[32,40,512]{2,1,0:T(8,128)(2,1)} %bitcast.27), calls=%async_computation.2 | async-start | bytes 2621440 | tf_op jit(solution)/shard_map/all_to_all | solution.py:21
  304.1 32.8 %all-to-all-done.2 = bf16[32,40,512]{2,1,0:T(8,128)(2,1)S(1)} async-done(((bf16[32,40,512]{2,1,0:T(8,128)(2,1)}), bf16[32,40,512]{2,1,0:T(8,128)(2,1)S(1)}, u32[]{:S(2)}, u32[]{:S(2)}) %all-to-all-start.2) | async-done | bytes 1310752 | tf_op jit(solution)/shard_map/all_to_all | solution.py:21
  339.1 3.7 all-to-all-start.3
  342.8 50.5 %all-to-all-done.3 = bf16[8,48,512]{2,1,0:T(8,128)(2,1)S(1)} async-done(((bf16[8,48,512]{2,1,0:T(8,128)(2,1)}), bf16[8,48,512]{2,1,0:T(8,128)(2,1)S(1)}, u32[]{:S(2)}, u32[]{:S(2)}) %all-to-all-start.3) | async-done | bytes 393248 | tf_op jit(solution)/shard_map/all_to_all | solution.py:21
  393.8 1.9 fusion.5
  (41 shorter events, 7.5 us)
Async XLA Ops:
  148.0 135.3 %all-to-all-start.1 = ((bf16[32,40,512]{2,1,0:T(8,128)(2,1)}), bf16[32,40,512]{2,1,0:T(8,128)(2,1)S(1)}, u32[]{:S(2)}, u32[]{:S(2)}) async-start(bf16[32,40,512]{2,1,0:T(8,128)(2,1)} %bitcast.34), calls=%async_computation.1 | async-start | bytes 2621440 | tf_op jit(solution)/shard_map/all_to_all | solution.py:21
  175.5 60.9 %collective-permute-start = (bf16[2048,512]{1,0:T(8,128)(2,1)}, bf16[2048,512]{1,0:T(8,128)(2,1)S(1)}, u32[]{:S(2)}, u32[]{:S(2)}) collective-permute-start(bf16[2048,512]{1,0:T(8,128)(2,1)} %get-tuple-element.18), channel_id=1, source_target_pairs={{0,3},{1,0},{2,1},{3,2},{4,7},{5,4},{6,5},{7,6},{8,11},{9,8},{10,9... | collective-permute-start | bytes 6291464 | tf_op jit(solution)/shard_map/ppermute | solution.py:26
  180.2 60.9 %collective-permute-start.1 = (bf16[2048,512]{1,0:T(8,128)(2,1)}, bf16[2048,512]{1,0:T(8,128)(2,1)S(1)}, u32[]{:S(2)}, u32[]{:S(2)}) collective-permute-start(bf16[2048,512]{1,0:T(8,128)(2,1)} %get-tuple-element.18), channel_id=1, source_target_pairs={{0,1},{1,2},{2,3},{3,0},{4,5},{5,6},{6,7},{7,4},{8,9},{9,10},{10,1... | collective-permute-start | bytes 6291464 | tf_op jit(solution)/shard_map/ppermute | solution.py:26
  182.2 76.7 %collective-permute-start.4 = (bf16[1024,512]{1,0:T(8,128)(2,1)}, bf16[1024,512]{1,0:T(8,128)(2,1)S(1)}, u32[]{:S(2)}, u32[]{:S(2)}) collective-permute-start(bf16[1024,512]{1,0:T(8,128)(2,1)} %bitcast.9.refs_7_), channel_id=1, source_target_pairs={{0,3},{1,0},{2,1},{3,2},{4,7},{5,4},{6,5},{7,6},{8,11},{9,8},{10,9... | collective-permute-start | bytes 3145736 | tf_op jit(solution)/shard_map/ppermute | solution.py:26
  186.8 77.6 %collective-permute-start.5 = (bf16[1024,512]{1,0:T(8,128)(2,1)}, bf16[1024,512]{1,0:T(8,128)(2,1)S(1)}, u32[]{:S(2)}, u32[]{:S(2)}) collective-permute-start(bf16[1024,512]{1,0:T(8,128)(2,1)} %bitcast.9.refs_7_), channel_id=1, source_target_pairs={{0,1},{1,2},{2,3},{3,0},{4,5},{5,6},{6,7},{7,4},{8,9},{9,10},{10,1... | collective-permute-start | bytes 3145736 | tf_op jit(solution)/shard_map/ppermute | solution.py:26
  236.4 4.7 %copy-start.1 = (bf16[2048,512]{1,0:T(8,128)(2,1)}, bf16[2048,512]{1,0:T(8,128)(2,1)S(1)}, u32[]{:S(2)}) copy-start(bf16[2048,512]{1,0:T(8,128)(2,1)S(1)} %collective-permute-done.refs_3_) | copy-start | bytes 6291460
  236.5 45.0 %collective-permute-start.2 = (bf16[1024,512]{1,0:T(8,128)(2,1)S(1)}, bf16[1024,512]{1,0:T(8,128)(2,1)}, u32[]{:S(2)}, u32[]{:S(2)}) collective-permute-start(bf16[1024,512]{1,0:T(8,128)(2,1)S(1)} %slice.48), channel_id=1, source_target_pairs={{0,3},{1,0},{2,1},{3,2},{4,7},{5,4},{6,5},{7,6},{8,11},{9,8},{10,9... | collective-permute-start | bytes 3145736 | tf_op jit(solution)/shard_map/ppermute | solution.py:26
  241.1 18.8 %copy-start.2 = (bf16[2048,512]{1,0:T(8,128)(2,1)}, bf16[2048,512]{1,0:T(8,128)(2,1)S(1)}, u32[]{:S(2)}) copy-start(bf16[2048,512]{1,0:T(8,128)(2,1)S(1)} %collective-permute-done.1.refs_4_) | copy-start | bytes 6291460
  241.2 27.0 %copy-start.6 = (f32[2048]{0:T(1024)S(1)}, f32[2048]{0:T(1024)}, u32[]{:S(2)}) copy-start(f32[2048]{0:T(1024)} %param.14) | copy-start | bytes 24580
  241.2 42.2 %collective-permute-start.3 = (bf16[1024,512]{1,0:T(8,128)(2,1)S(1)}, bf16[1024,512]{1,0:T(8,128)(2,1)}, u32[]{:S(2)}, u32[]{:S(2)}) collective-permute-start(bf16[1024,512]{1,0:T(8,128)(2,1)S(1)} %slice.49), channel_id=1, source_target_pairs={{0,1},{1,2},{2,3},{3,0},{4,5},{5,6},{6,7},{7,4},{8,9},{9,10},{10,1... | collective-permute-start | bytes 3145736 | tf_op jit(solution)/shard_map/ppermute | solution.py:26
  258.9 5.5 %copy-start.3 = (bf16[1024,512]{1,0:T(8,128)(2,1)}, bf16[1024,512]{1,0:T(8,128)(2,1)S(1)}, u32[]{:S(2)}) copy-start(bf16[1024,512]{1,0:T(8,128)(2,1)S(1)} %collective-permute-done.4.refs_8_) | copy-start | bytes 3145732
  259.8 33.1 %collective-permute-start.6 = (bf16[512,512]{1,0:T(8,128)(2,1)}, bf16[512,512]{1,0:T(8,128)(2,1)}, u32[]{:S(2)}, u32[]{:S(2)}) collective-permute-start(bf16[512,512]{1,0:T(8,128)(2,1)} %slice.50), channel_id=1, source_target_pairs={{0,3},{1,0},{2,1},{3,2},{4,7},{5,4},{6,5},{7,6},{8,11},{9,8},{10,9... | collective-permute-start | bytes 1572872 | tf_op jit(solution)/shard_map/ppermute | solution.py:26
  264.4 1.0 copy-start.4
  266.2 28.4 %collective-permute-start.7 = (bf16[512,512]{1,0:T(8,128)(2,1)}, bf16[512,512]{1,0:T(8,128)(2,1)}, u32[]{:S(2)}, u32[]{:S(2)}) collective-permute-start(bf16[512,512]{1,0:T(8,128)(2,1)} %slice.51), channel_id=1, source_target_pairs={{0,1},{1,2},{2,3},{3,0},{4,5},{5,6},{6,7},{7,4},{8,9},{9,10},{10,1... | collective-permute-start | bytes 1572872 | tf_op jit(solution)/shard_map/ppermute | solution.py:26
  283.3 1.1 copy-start
  297.2 6.5 %copy-start.8 = (s32[2,8,128]{2,1,0:T(8,128)S(1)}, s32[2,8,128]{2,1,0:T(8,128)}, u32[]{:S(2)}) copy-start(s32[2,8,128]{2,1,0:T(8,128)} %get-tuple-element.16) | copy-start | bytes 24580
  297.3 6.6 %copy-start.7 = (f32[2,8,128]{2,1,0:T(8,128)S(1)}, f32[2,8,128]{2,1,0:T(8,128)}, u32[]{:S(2)}) copy-start(f32[2,8,128]{2,1,0:T(8,128)} %get-tuple-element.15) | copy-start | bytes 24580
  297.3 39.6 %all-to-all-start.2 = ((bf16[32,40,512]{2,1,0:T(8,128)(2,1)}), bf16[32,40,512]{2,1,0:T(8,128)(2,1)S(1)}, u32[]{:S(2)}, u32[]{:S(2)}) async-start(bf16[32,40,512]{2,1,0:T(8,128)(2,1)} %bitcast.27), calls=%async_computation.2 | async-start | bytes 2621440 | tf_op jit(solution)/shard_map/all_to_all | solution.py:21
  337.6 5.2 %copy-start.9 = (s32[1,384]{1,0:T(1,128)S(1)}, s32[1,384]{1,0:T(1,128)}, u32[]{:S(2)}) copy-start(s32[1,384]{1,0:T(1,128)} %get-tuple-element.13) | copy-start | bytes 4612
  337.6 5.2 %copy-start.5 = (s32[384]{0:T(512)S(1)}, s32[384]{0:T(512)}, u32[]{:S(2)}) copy-start(s32[384]{0:T(512)} %group.1) | copy-start | bytes 4612
  339.1 54.2 %all-to-all-start.3 = ((bf16[8,48,512]{2,1,0:T(8,128)(2,1)}), bf16[8,48,512]{2,1,0:T(8,128)(2,1)S(1)}, u32[]{:S(2)}, u32[]{:S(2)}) async-start(bf16[8,48,512]{2,1,0:T(8,128)(2,1)} %bitcast.14), calls=%async_computation.3 | async-start | bytes 786432 | tf_op jit(solution)/shard_map/all_to_all | solution.py:21

commit v8 on v7

--- a/solution.py
+++ b/solution.py
@@ -67,9 +67,9 @@
 
 
 def depart(group, choice, group_share, expert_share, tokens, gate, up, *refs):
-    blocks, ranks, joined, semaphores = refs
+    blocks, ranks, joined, held, semaphores = refs
     units = gate.shape[1]
-    sides = joined.at[:, pl.ds(0, units)], joined.at[:, pl.ds(units, units)]
+    sides = held.at[:, pl.ds(0, units)], held.at[:, pl.ds(units, units)]
     joining = fetch((gate, up), sides, semaphores)
     groups, _, lanes = blocks.shape
     count, width = tokens.shape
@@ -80,6 +80,10 @@
     rank = jnp.sum(jnp.where(member, earlier, 0.0), 0, keepdims=True).astype(jnp.int32)
     ranks[...] = rank
     seating = ones(iota((count, count), 0) == group * per_group + rank)
+    for copy in joining:
+        copy.wait()
+    leaving = pltpu.make_async_copy(held, joined, semaphores.at[2])
+    leaving.start()
     seated = dot(seating, tokens[...]).astype(jnp.bfloat16)
     mixing = group_share[...].reshape(1, count) * expert_share[...]
     mixing = mixing / jnp.sum(expert_share[...], 0, keepdims=True)
@@ -101,8 +105,7 @@
             piece = seated[g * per_group : (g + 1) * per_group, c * lanes : (c + 1) * lanes]
             blocks[g, c * per_group : (c + 1) * per_group, :] = piece
         blocks[g, chunks * per_group :, :] = told[g * TILE : (g + 1) * TILE]
-    for copy in joining:
-        copy.wait()
+    leaving.wait()
 
 
 def arrive(capacity, landed, buffer, places, shares, seats):
@@ -299,7 +302,10 @@
         ),
         in_specs=[VMEM] * 5 + [HBM] * 2,
         out_specs=(VMEM, VMEM, HBM),
-        scratch_shapes=[pltpu.SemaphoreType.DMA((2,))],
+        scratch_shapes=[
+            pltpu.VMEM((gate.shape[0], 2 * gate.shape[1]), jnp.bfloat16),
+            pltpu.SemaphoreType.DMA((3,)),
+        ],
         name="depart",
     )(group_choice, expert_choice.T, group_weight, expert_weight.T, tokens, gate, up)
     gate_up_ring = around(joined, "tp")

time: 397 us -> 335 us (0.84)
  Pallas kernels: 80.5 us -> 18.7 us
    pallas_call x1, Pallas kernels: 66.5 us -> 4.69 us  [layer(): pl.pallas_call(depart, out_shape=(shaped((groups, chunks * per_group + TI...]
  transfers between devices with their start and end apart: 11 -> 11, of which waited for: 7 -> 7; matrix products, arithmetic and copies ran while one was open for 1% -> 1% of each run, Pallas kernels for 2% -> 3%
where the time goes in v8:
time: 335 us; the launch traced here: 334 us
  waiting for transfers between devices  163 us (49%)
  blocking collectives  78.7 us (23%)
  starting transfers between devices  63.8 us (19%)
  Pallas kernels  18.7 us (6%)
  local copies, waits for them, and re-layouts  4.9 us (1%)
  matrix products  4.46 us (1%)
    all_to_all x3, waiting for transfers between devices, exchange(): return lax.all_to_all(array, axis, 0, 0, tiled=True)  83.4 us
    ppermute x8, waiting for transfers between devices, shifted(): lax.ppermute(array, axis, [(a, (a + by) % length) for a in range(length)])  79.6 us
    all_to_all x1, blocking collectives, exchange(): return lax.all_to_all(array, axis, 0, 0, tiled=True)  78.7 us
    all_to_all x3, starting transfers between devices, exchange(): return lax.all_to_all(array, axis, 0, 0, tiled=True)  37.6 us
    ppermute x8, starting transfers between devices, shifted(): lax.ppermute(array, axis, [(a, (a + by) % length) for a in range(length)])  26.2 us
    pallas_call x1, Pallas kernels, expert(): pl.pallas_call(main_part, out_shape=(whole, shaped((parts, count, width))...  8.46 us
  transfers between devices with their start and end apart: 11, of which 7 were waited for; matrix products, arithmetic and copies ran while one was open for 1% of the time, Pallas kernels for 3%

profile of v8, /device:TPU:33, one launch (start us, length us, event | category | flops | bytes accessed | tf_op | source)
XLA Modules:
  0.0 334.0 jit_solution(3715382123409730856)
XLA Ops:
  0.0 4.7 %depart.1 = (bf16[8,200,128]{2,1,0:T(8,128)(2,1)}, s32[1,384]{1,0:T(1,128)}, bf16[2048,512]{1,0:T(8,128)(2,1)}) custom-call(s32[384]{0:T(512)} %group.1, s32[2,384]{1,0:T(2,128)} %bitcast.41, f32[384]{0:T(512)} %group_share.1, f32[2,384]{1,0:T(2,128)} %bitcast.42, bf16[384,512]{1,0:T(8,128)(2,1)} %tokens.1, bf16[2048,256]{1,0:T(8,128)(2,1)} %bitcast.29, ...), custom_call_target="tpu_custom_call" | custom-call | tf_op jit(solution)/shard_map/depart/pallas_call | solution.py:296
  4.7 78.7 %all_to_all.20.landed = bf16[8,200,128]{2,1,0:T(8,128)(2,1)} all-to-all(bf16[8,200,128]{2,1,0:T(8,128)(2,1)} %get-tuple-element.14), channel_id=1, replica_groups=mesh['grp'=2,'g'=8,'m'=8,'tp'=4] {'g'}, dimensions={0} | all-to-all | bytes 819200 | tf_op jit(solution)/shard_map/all_to_all | solution.py:21
  83.4 2.9 arrive.1
  86.3 27.5 %all-to-all-start.1 = ((bf16[32,40,512]{2,1,0:T(8,128)(2,1)}), bf16[32,40,512]{2,1,0:T(8,128)(2,1)S(1)}, u32[]{:S(2)}, u32[]{:S(2)}) async-start(bf16[32,40,512]{2,1,0:T(8,128)(2,1)} %bitcast.34), calls=%async_computation.1 | async-start | bytes 2621440 | tf_op jit(solution)/shard_map/all_to_all | solution.py:21
  113.8 4.6 %collective-permute-start = (bf16[2048,512]{1,0:T(8,128)(2,1)}, bf16[2048,512]{1,0:T(8,128)(2,1)S(1)}, u32[]{:S(2)}, u32[]{:S(2)}) collective-permute-start(bf16[2048,512]{1,0:T(8,128)(2,1)} %get-tuple-element.18), channel_id=1, source_target_pairs={{0,3},{1,0},{2,1},{3,2},{4,7},{5,4},{6,5},{7,6},{8,11},{9,8},{10,9... | collective-permute-start | bytes 6291464 | tf_op jit(solution)/shard_map/ppermute | solution.py:26
  118.4 2.0 collective-permute-start.1
  120.4 4.6 %collective-permute-start.4 = (bf16[1024,512]{1,0:T(8,128)(2,1)}, bf16[1024,512]{1,0:T(8,128)(2,1)S(1)}, u32[]{:S(2)}, u32[]{:S(2)}) collective-permute-start(bf16[1024,512]{1,0:T(8,128)(2,1)} %bitcast.9.refs_7_), channel_id=1, source_target_pairs={{0,3},{1,0},{2,1},{3,2},{4,7},{5,4},{6,5},{7,6},{8,11},{9,8},{10,9... | collective-permute-start | bytes 3145736 | tf_op jit(solution)/shard_map/ppermute | solution.py:26
  125.0 2.0 collective-permute-start.5
  126.9 47.7 %collective-permute-done.refs_3_ = bf16[2048,512]{1,0:T(8,128)(2,1)S(1)} collective-permute-done((bf16[2048,512]{1,0:T(8,128)(2,1)}, bf16[2048,512]{1,0:T(8,128)(2,1)S(1)}, u32[]{:S(2)}, u32[]{:S(2)}) %collective-permute-start) | collective-permute-done | bytes 2097184 | tf_op jit(solution)/shard_map/ppermute | solution.py:26
  174.7 4.5 %collective-permute-start.2 = (bf16[1024,512]{1,0:T(8,128)(2,1)S(1)}, bf16[1024,512]{1,0:T(8,128)(2,1)}, u32[]{:S(2)}, u32[]{:S(2)}) collective-permute-start(bf16[1024,512]{1,0:T(8,128)(2,1)S(1)} %slice.48), channel_id=1, source_target_pairs={{0,3},{1,0},{2,1},{3,2},{4,7},{5,4},{6,5},{7,6},{8,11},{9,8},{10,9... | collective-permute-start | bytes 3145736 | tf_op jit(solution)/shard_map/ppermute | solution.py:26
  179.4 2.1 collective-permute-start.3
  181.5 15.6 %collective-permute-done.4.refs_8_ = bf16[1024,512]{1,0:T(8,128)(2,1)S(1)} collective-permute-done((bf16[1024,512]{1,0:T(8,128)(2,1)}, bf16[1024,512]{1,0:T(8,128)(2,1)S(1)}, u32[]{:S(2)}, u32[]{:S(2)}) %collective-permute-start.4) | collective-permute-done | bytes 1048608 | tf_op jit(solution)/shard_map/ppermute | solution.py:26
  198.0 4.5 %collective-permute-start.6 = (bf16[512,512]{1,0:T(8,128)(2,1)}, bf16[512,512]{1,0:T(8,128)(2,1)}, u32[]{:S(2)}, u32[]{:S(2)}) collective-permute-start(bf16[512,512]{1,0:T(8,128)(2,1)} %slice.50), channel_id=1, source_target_pairs={{0,3},{1,0},{2,1},{3,2},{4,7},{5,4},{6,5},{7,6},{8,11},{9,8},{10,9... | collective-permute-start | bytes 1572872 | tf_op jit(solution)/shard_map/ppermute | solution.py:26
  204.4 1.9 collective-permute-start.7
  207.0 12.7 %collective-permute-done.2.refs_5_ = bf16[1024,512]{1,0:T(8,128)(2,1)} collective-permute-done((bf16[1024,512]{1,0:T(8,128)(2,1)S(1)}, bf16[1024,512]{1,0:T(8,128)(2,1)}, u32[]{:S(2)}, u32[]{:S(2)}) %collective-permute-start.2) | collective-permute-done | bytes 1048608 | tf_op jit(solution)/shard_map/ppermute | solution.py:26
  219.7 1.9 collective-permute-done.3.refs_6_
  222.6 8.5 %main_part.1 = (bf16[320,1024]{1,0:T(8,128)(2,1)}, bf16[4,320,512]{2,1,0:T(8,128)(2,1)}) custom-call(s32[1]{0:T(128)} %bitcast.6.me, f32[4,512]{1,0:T(4,128)} %reshape.32.gains, bf16[4,320,512]{2,1,0:T(8,128)(2,1)} %bitcast.28, bf16[2048,256]{1,0:T(8,128)(2,1)} %bitcast.30, bf16[2048,256]{1,0:T(8,128)(2,1)} %bitcast.32, bf16[2048,512]{1,0:T(8,128)(2,1)} %copy-done.1, ...), custom_call_target="tpu_custom_call" | custom-call | tf_op jit(solution)/shard_map/main_part/pallas_call | solution.py:249
  231.1 1.7 collective-permute-done.7.refs_2_
  232.8 2.7 last_part.1
  235.5 6.4 %all-to-all-start.2 = ((bf16[32,40,512]{2,1,0:T(8,128)(2,1)}), bf16[32,40,512]{2,1,0:T(8,128)(2,1)S(1)}, u32[]{:S(2)}, u32[]{:S(2)}) async-start(bf16[32,40,512]{2,1,0:T(8,128)(2,1)} %bitcast.27), calls=%async_computation.2 | async-start | bytes 2621440 | tf_op jit(solution)/shard_map/all_to_all | solution.py:21
  242.3 32.8 %all-to-all-done.2 = bf16[32,40,512]{2,1,0:T(8,128)(2,1)S(1)} async-done(((bf16[32,40,512]{2,1,0:T(8,128)(2,1)}), bf16[32,40,512]{2,1,0:T(8,128)(2,1)S(1)}, u32[]{:S(2)}, u32[]{:S(2)}) %all-to-all-start.2) | async-done | bytes 1310752 | tf_op jit(solution)/shard_map/all_to_all | solution.py:21
  277.3 3.7 %all-to-all-start.3 = ((bf16[8,48,512]{2,1,0:T(8,128)(2,1)}), bf16[8,48,512]{2,1,0:T(8,128)(2,1)S(1)}, u32[]{:S(2)}, u32[]{:S(2)}) async-start(bf16[8,48,512]{2,1,0:T(8,128)(2,1)} %bitcast.14), calls=%async_computation.3 | async-start | bytes 786432 | tf_op jit(solution)/shard_map/all_to_all | solution.py:21
  281.1 50.6 %all-to-all-done.3 = bf16[8,48,512]{2,1,0:T(8,128)(2,1)S(1)} async-done(((bf16[8,48,512]{2,1,0:T(8,128)(2,1)}), bf16[8,48,512]{2,1,0:T(8,128)(2,1)S(1)}, u32[]{:S(2)}, u32[]{:S(2)}) %all-to-all-start.3) | async-done | bytes 393248 | tf_op jit(solution)/shard_map/all_to_all | solution.py:21
  332.1 1.9 fusion.5
  (41 shorter events, 7.5 us)
Async XLA Ops:
  86.3 135.3 %all-to-all-start.1 = ((bf16[32,40,512]{2,1,0:T(8,128)(2,1)}), bf16[32,40,512]{2,1,0:T(8,128)(2,1)S(1)}, u32[]{:S(2)}, u32[]{:S(2)}) async-start(bf16[32,40,512]{2,1,0:T(8,128)(2,1)} %bitcast.34), calls=%async_computation.1 | async-start | bytes 2621440 | tf_op jit(solution)/shard_map/all_to_all | solution.py:21
  113.8 60.9 %collective-permute-start = (bf16[2048,512]{1,0:T(8,128)(2,1)}, bf16[2048,512]{1,0:T(8,128)(2,1)S(1)}, u32[]{:S(2)}, u32[]{:S(2)}) collective-permute-start(bf16[2048,512]{1,0:T(8,128)(2,1)} %get-tuple-element.18), channel_id=1, source_target_pairs={{0,3},{1,0},{2,1},{3,2},{4,7},{5,4},{6,5},{7,6},{8,11},{9,8},{10,9... | collective-permute-start | bytes 6291464 | tf_op jit(solution)/shard_map/ppermute | solution.py:26
  118.4 60.9 %collective-permute-start.1 = (bf16[2048,512]{1,0:T(8,128)(2,1)}, bf16[2048,512]{1,0:T(8,128)(2,1)S(1)}, u32[]{:S(2)}, u32[]{:S(2)}) collective-permute-start(bf16[2048,512]{1,0:T(8,128)(2,1)} %get-tuple-element.18), channel_id=1, source_target_pairs={{0,1},{1,2},{2,3},{3,0},{4,5},{5,6},{6,7},{7,4},{8,9},{9,10},{10,1... | collective-permute-start | bytes 6291464 | tf_op jit(solution)/shard_map/ppermute | solution.py:26
  120.4 76.7 %collective-permute-start.4 = (bf16[1024,512]{1,0:T(8,128)(2,1)}, bf16[1024,512]{1,0:T(8,128)(2,1)S(1)}, u32[]{:S(2)}, u32[]{:S(2)}) collective-permute-start(bf16[1024,512]{1,0:T(8,128)(2,1)} %bitcast.9.refs_7_), channel_id=1, source_target_pairs={{0,3},{1,0},{2,1},{3,2},{4,7},{5,4},{6,5},{7,6},{8,11},{9,8},{10,9... | collective-permute-start | bytes 3145736 | tf_op jit(solution)/shard_map/ppermute | solution.py:26
  125.0 77.6 %collective-permute-start.5 = (bf16[1024,512]{1,0:T(8,128)(2,1)}, bf16[1024,512]{1,0:T(8,128)(2,1)S(1)}, u32[]{:S(2)}, u32[]{:S(2)}) collective-permute-start(bf16[1024,512]{1,0:T(8,128)(2,1)} %bitcast.9.refs_7_), channel_id=1, source_target_pairs={{0,1},{1,2},{2,3},{3,0},{4,5},{5,6},{6,7},{7,4},{8,9},{9,10},{10,1... | collective-permute-start | bytes 3145736 | tf_op jit(solution)/shard_map/ppermute | solution.py:26
  174.6 4.7 %copy-start.1 = (bf16[2048,512]{1,0:T(8,128)(2,1)}, bf16[2048,512]{1,0:T(8,128)(2,1)S(1)}, u32[]{:S(2)}) copy-start(bf16[2048,512]{1,0:T(8,128)(2,1)S(1)} %collective-permute-done.refs_3_) | copy-start | bytes 6291460
  174.7 45.0 %collective-permute-start.2 = (bf16[1024,512]{1,0:T(8,128)(2,1)S(1)}, bf16[1024,512]{1,0:T(8,128)(2,1)}, u32[]{:S(2)}, u32[]{:S(2)}) collective-permute-start(bf16[1024,512]{1,0:T(8,128)(2,1)S(1)} %slice.48), channel_id=1, source_target_pairs={{0,3},{1,0},{2,1},{3,2},{4,7},{5,4},{6,5},{7,6},{8,11},{9,8},{10,9... | collective-permute-start | bytes 3145736 | tf_op jit(solution)/shard_map/ppermute | solution.py:26
  179.3 18.8 %copy-start.2 = (bf16[2048,512]{1,0:T(8,128)(2,1)}, bf16[2048,512]{1,0:T(8,128)(2,1)S(1)}, u32[]{:S(2)}) copy-start(bf16[2048,512]{1,0:T(8,128)(2,1)S(1)} %collective-permute-done.1.refs_4_) | copy-start | bytes 6291460
  179.4 27.0 %copy-start.6 = (f32[2048]{0:T(1024)S(1)}, f32[2048]{0:T(1024)}, u32[]{:S(2)}) copy-start(f32[2048]{0:T(1024)} %param.14) | copy-start | bytes 24580
  179.4 42.2 %collective-permute-start.3 = (bf16[1024,512]{1,0:T(8,128)(2,1)S(1)}, bf16[1024,512]{1,0:T(8,128)(2,1)}, u32[]{:S(2)}, u32[]{:S(2)}) collective-permute-start(bf16[1024,512]{1,0:T(8,128)(2,1)S(1)} %slice.49), channel_id=1, source_target_pairs={{0,1},{1,2},{2,3},{3,0},{4,5},{5,6},{6,7},{7,4},{8,9},{9,10},{10,1... | collective-permute-start | bytes 3145736 | tf_op jit(solution)/shard_map/ppermute | solution.py:26
  197.1 5.5 %copy-start.3 = (bf16[1024,512]{1,0:T(8,128)(2,1)}, bf16[1024,512]{1,0:T(8,128)(2,1)S(1)}, u32[]{:S(2)}) copy-start(bf16[1024,512]{1,0:T(8,128)(2,1)S(1)} %collective-permute-done.4.refs_8_) | copy-start | bytes 3145732
  198.0 33.1 %collective-permute-start.6 = (bf16[512,512]{1,0:T(8,128)(2,1)}, bf16[512,512]{1,0:T(8,128)(2,1)}, u32[]{:S(2)}, u32[]{:S(2)}) collective-permute-start(bf16[512,512]{1,0:T(8,128)(2,1)} %slice.50), channel_id=1, source_target_pairs={{0,3},{1,0},{2,1},{3,2},{4,7},{5,4},{6,5},{7,6},{8,11},{9,8},{10,9... | collective-permute-start | bytes 1572872 | tf_op jit(solution)/shard_map/ppermute | solution.py:26
  202.6 1.0 copy-start.4
  204.4 28.4 %collective-permute-start.7 = (bf16[512,512]{1,0:T(8,128)(2,1)}, bf16[512,512]{1,0:T(8,128)(2,1)}, u32[]{:S(2)}, u32[]{:S(2)}) collective-permute-start(bf16[512,512]{1,0:T(8,128)(2,1)} %slice.51), channel_id=1, source_target_pairs={{0,1},{1,2},{2,3},{3,0},{4,5},{5,6},{6,7},{7,4},{8,9},{9,10},{10,1... | collective-permute-start | bytes 1572872 | tf_op jit(solution)/shard_map/ppermute | solution.py:26
  221.6 1.1 copy-start
  235.5 6.5 %copy-start.8 = (s32[2,8,128]{2,1,0:T(8,128)S(1)}, s32[2,8,128]{2,1,0:T(8,128)}, u32[]{:S(2)}) copy-start(s32[2,8,128]{2,1,0:T(8,128)} %get-tuple-element.16) | copy-start | bytes 24580
  235.5 6.6 %copy-start.7 = (f32[2,8,128]{2,1,0:T(8,128)S(1)}, f32[2,8,128]{2,1,0:T(8,128)}, u32[]{:S(2)}) copy-start(f32[2,8,128]{2,1,0:T(8,128)} %get-tuple-element.15) | copy-start | bytes 24580
  235.5 39.6 %all-to-all-start.2 = ((bf16[32,40,512]{2,1,0:T(8,128)(2,1)}), bf16[32,40,512]{2,1,0:T(8,128)(2,1)S(1)}, u32[]{:S(2)}, u32[]{:S(2)}) async-start(bf16[32,40,512]{2,1,0:T(8,128)(2,1)} %bitcast.27), calls=%async_computation.2 | async-start | bytes 2621440 | tf_op jit(solution)/shard_map/all_to_all | solution.py:21
  275.8 5.2 %copy-start.9 = (s32[1,384]{1,0:T(1,128)S(1)}, s32[1,384]{1,0:T(1,128)}, u32[]{:S(2)}) copy-start(s32[1,384]{1,0:T(1,128)} %get-tuple-element.13) | copy-start | bytes 4612
  275.8 5.2 %copy-start.5 = (s32[384]{0:T(512)S(1)}, s32[384]{0:T(512)}, u32[]{:S(2)}) copy-start(s32[384]{0:T(512)} %group.1) | copy-start | bytes 4612
  277.3 54.3 %all-to-all-start.3 = ((bf16[8,48,512]{2,1,0:T(8,128)(2,1)}), bf16[8,48,512]{2,1,0:T(8,128)(2,1)S(1)}, u32[]{:S(2)}, u32[]{:S(2)}) async-start(bf16[8,48,512]{2,1,0:T(8,128)(2,1)} %bitcast.14), calls=%async_computation.3 | async-start | bytes 786432 | tf_op jit(solution)/shard_map/all_to_all | solution.py:21

commit v9 on v6

--- a/solution.py
+++ b/solution.py
@@ -167,11 +167,12 @@
     given, (hidden_out, results), (rows, *slots) = refs[:10], refs[10:12], refs[12:22]
     normed, hidden, pieces, semaphores, leaving = refs[22:]
     gate, up, one, three, top, bottom, *down = slots
-    arrived, *copies = fetch(given, (rows, *slots), semaphores)
+    arrived, *copies = fetch(given[:3], (rows, *slots[:2]), semaphores)
     parts, _, width = rows.shape
     units = gate.shape[1]
     total = None
     arrived.wait()
+    copies += fetch(given[3:], slots[2:], semaphores.at[pl.ds(3, len(given) - 3)])
     for t in range(parts):
         values = rows[t].astype(jnp.float32)
         squares = jnp.sum(values * values, -1, keepdims=True)
@@ -318,23 +319,28 @@
         rows, norm_gain, w_gate[0], w_up[0], w_down[0], gate_up_ring, down_ring, me
     )
 
+    places = jnp.arange(tp_count * members * depth, dtype=jnp.int32)
+    targets, shares, results = lax.optimization_barrier((targets, shares, results))
+    coarse = lax.reduce_precision(shares, 8, 7)
+    mixers = []
+    for share in (coarse, shares - coarse):
+        weights = 0.0
+        for k in range(2):
+            back = targets[k][:, :per_group].reshape(-1)
+            part = share[k][:, :per_group].reshape(-1)
+            weights += jnp.where(back[:, None] == places[None, :], part[:, None], 0.0)
+        mixers.append(weights.astype(jnp.bfloat16))
+    mixers = lax.optimization_barrier(mixers)
     returned = exchange(results.reshape(tp_count * members, depth, piece_width), BLOCK)
     returned = returned.reshape(-1, piece_width)
-    places = jnp.arange(returned.shape[0], dtype=jnp.int32)
-    combined = jnp.zeros((tok_rows, piece_width), jnp.float32)
-    for k in range(2):
-        back = targets[k][:, :per_group].reshape(-1)
-        share = shares[k][:, :per_group].reshape(-1)
-        picker = (back[:, None] == places[None, :]).astype(jnp.bfloat16)
-        combined = combined + share[:, None] * dot(picker, returned)
-    combined = combined.astype(jnp.bfloat16)
+    combined = sum(dot(weights, returned) for weights in mixers).astype(jnp.bfloat16)
     home = exchange(combined.reshape(groups, per_group, piece_width), "g")
     home = home.reshape(tok_rows, piece_width)
     here = lax.axis_index("g")
     seats = jnp.arange(per_group, dtype=jnp.int32)[None, :]
     stayed = (group_choice == here)[:, None] & (rank[:, None] == seats)
     own = lax.dynamic_slice_in_dim(combined, here * per_group, per_group, 0)
-    kept = dot(stayed.astype(jnp.bfloat16), own)
+    kept = lax.optimization_barrier(dot(stayed.astype(jnp.bfloat16), own))
     slot = jnp.where(group_choice == here, -1, group_choice * per_group + rank)
     unseating = slot[:, None] == jnp.arange(tok_rows, dtype=jnp.int32)[None, :]
     return (dot(unseating.astype(jnp.bfloat16), home) + kept).astype(jnp.bfloat16)

time: 333 us -> 331 us (level)
  transfers between devices with their start and end apart: 11 -> 11, of which waited for: 7 -> 7; matrix products, arithmetic and copies ran while one was open for 1% -> 2% of each run, Pallas kernels for 3% -> 3%
where the time goes in v9:
time: 331 us; the launch traced here: 330 us
  waiting for transfers between devices  161 us (49%)
  blocking collectives  78.8 us (24%)
  starting transfers between devices  63.9 us (19%)
  Pallas kernels  16.6 us (5%)
  matrix products  4.36 us (1%)
  local copies, waits for them, and re-layouts  4.2 us (1%)
    all_to_all x3, waiting for transfers between devices, exchange(): return lax.all_to_all(array, axis, 0, 0, tiled=True)  81.2 us
    ppermute x8, waiting for transfers between devices, shifted(): lax.ppermute(array, axis, [(a, (a + by) % length) for a in range(length)])  79.8 us
    all_to_all x1, blocking collectives, exchange(): return lax.all_to_all(array, axis, 0, 0, tiled=True)  78.8 us
    all_to_all x3, starting transfers between devices, exchange(): return lax.all_to_all(array, axis, 0, 0, tiled=True)  37.5 us
    ppermute x8, starting transfers between devices, shifted(): lax.ppermute(array, axis, [(a, (a + by) % length) for a in range(length)])  26.4 us
    pallas_call x1, Pallas kernels, expert(): pl.pallas_call(main_part, out_shape=(whole, shaped((parts, count, width))...  8.71 us
  transfers between devices with their start and end apart: 11, of which 7 were waited for; matrix products, arithmetic and copies ran while one was open for 2% of the time, Pallas kernels for 3%

profile of v9, /device:TPU:33, one launch (start us, length us, event | category | flops | bytes accessed | tf_op | source)
XLA Modules:
  0.0 330.3 jit_solution(687770919004797756)
XLA Ops:
  0.0 2.4 depart.1
  2.4 78.8 %all_to_all.20.landed = bf16[8,200,128]{2,1,0:T(8,128)(2,1)} all-to-all(bf16[8,200,128]{2,1,0:T(8,128)(2,1)} %get-tuple-element.18), channel_id=1, replica_groups=mesh['grp'=2,'g'=8,'m'=8,'tp'=4] {'g'}, dimensions={0} | all-to-all | bytes 819200 | tf_op jit(solution)/shard_map/all_to_all | solution.py:21
  81.2 2.9 arrive.1
  84.1 27.5 %all-to-all-start.1 = ((bf16[32,40,512]{2,1,0:T(8,128)(2,1)}), bf16[32,40,512]{2,1,0:T(8,128)(2,1)S(1)}, u32[]{:S(2)}, u32[]{:S(2)}) async-start(bf16[32,40,512]{2,1,0:T(8,128)(2,1)} %bitcast.42), calls=%async_computation.1 | async-start | bytes 2621440 | tf_op jit(solution)/shard_map/all_to_all | solution.py:21
  111.8 4.8 %collective-permute-start = (bf16[2048,512]{1,0:T(8,128)(2,1)S(1)}, bf16[2048,512]{1,0:T(8,128)(2,1)S(1)}, u32[]{:S(2)}, u32[]{:S(2)}) collective-permute-start(bf16[2048,512]{1,0:T(8,128)(2,1)S(1)} %pad_maximum_fusion), channel_id=1, source_target_pairs={{0,3},{1,0},{2,1},{3,2},{4,7},{5,4},{6,5},{7,6},{8,11},{9,8},{10,9... | collective-permute-start | bytes 6291464 | tf_op jit(solution)/shard_map/ppermute | solution.py:26
  116.5 2.0 collective-permute-start.1
  118.5 4.6 %collective-permute-start.4 = (bf16[1024,512]{1,0:T(8,128)(2,1)S(1)}, bf16[1024,512]{1,0:T(8,128)(2,1)S(1)}, u32[]{:S(2)}, u32[]{:S(2)}) collective-permute-start(bf16[1024,512]{1,0:T(8,128)(2,1)S(1)} %bitcast.46), channel_id=1, source_target_pairs={{0,3},{1,0},{2,1},{3,2},{4,7},{5,4},{6,5},{7,6},{8,11},{9,8},{10,9... | collective-permute-start | bytes 3145736 | tf_op jit(solution)/shard_map/ppermute | solution.py:26
  123.1 2.0 collective-permute-start.5
  125.1 47.4 %collective-permute-done.refs_3_ = bf16[2048,512]{1,0:T(8,128)(2,1)S(1)} collective-permute-done((bf16[2048,512]{1,0:T(8,128)(2,1)S(1)}, bf16[2048,512]{1,0:T(8,128)(2,1)S(1)}, u32[]{:S(2)}, u32[]{:S(2)}) %collective-permute-start) | collective-permute-done | bytes 2097184 | tf_op jit(solution)/shard_map/ppermute | solution.py:26
  172.5 4.7 %collective-permute-start.2 = (bf16[1024,512]{1,0:T(8,128)(2,1)S(1)}, bf16[1024,512]{1,0:T(8,128)(2,1)}, u32[]{:S(2)}, u32[]{:S(2)}) collective-permute-start(bf16[1024,512]{1,0:T(8,128)(2,1)S(1)} %slice.68), channel_id=1, source_target_pairs={{0,3},{1,0},{2,1},{3,2},{4,7},{5,4},{6,5},{7,6},{8,11},{9,8},{10,9... | collective-permute-start | bytes 3145736 | tf_op jit(solution)/shard_map/ppermute | solution.py:26
  177.3 2.0 collective-permute-start.3
  179.3 15.6 %collective-permute-done.4.refs_8_ = bf16[1024,512]{1,0:T(8,128)(2,1)S(1)} collective-permute-done((bf16[1024,512]{1,0:T(8,128)(2,1)S(1)}, bf16[1024,512]{1,0:T(8,128)(2,1)S(1)}, u32[]{:S(2)}, u32[]{:S(2)}) %collective-permute-start.4) | collective-permute-done | bytes 1048608 | tf_op jit(solution)/shard_map/ppermute | solution.py:26
  195.8 4.5 %collective-permute-start.6 = (bf16[512,512]{1,0:T(8,128)(2,1)}, bf16[512,512]{1,0:T(8,128)(2,1)}, u32[]{:S(2)}, u32[]{:S(2)}) collective-permute-start(bf16[512,512]{1,0:T(8,128)(2,1)} %slice.70), channel_id=1, source_target_pairs={{0,3},{1,0},{2,1},{3,2},{4,7},{5,4},{6,5},{7,6},{8,11},{9,8},{10,9... | collective-permute-start | bytes 1572872 | tf_op jit(solution)/shard_map/ppermute | solution.py:26
  201.3 1.9 collective-permute-start.7
  203.9 13.6 %collective-permute-done.2.refs_5_ = bf16[1024,512]{1,0:T(8,128)(2,1)} collective-permute-done((bf16[1024,512]{1,0:T(8,128)(2,1)S(1)}, bf16[1024,512]{1,0:T(8,128)(2,1)}, u32[]{:S(2)}, u32[]{:S(2)}) %collective-permute-start.2) | collective-permute-done | bytes 1048608 | tf_op jit(solution)/shard_map/ppermute | solution.py:26
  217.5 1.8 collective-permute-done.3.refs_6_
  220.4 8.7 %main_part.1 = (bf16[320,1024]{1,0:T(8,128)(2,1)}, bf16[4,320,512]{2,1,0:T(8,128)(2,1)}) custom-call(s32[1]{0:T(128)} %bitcast.2.me, f32[4,512]{1,0:T(4,128)} %reshape.34.gains, bf16[4,320,512]{2,1,0:T(8,128)(2,1)} %bitcast.36, bf16[2048,256]{1,0:T(8,128)(2,1)} %bitcast.37, bf16[2048,256]{1,0:T(8,128)(2,1)} %bitcast.39, bf16[2048,512]{1,0:T(8,128)(2,1)} %copy-done.1, ...), custom_call_target="tpu_custom_call" | custom-call | tf_op jit(solution)/shard_map/main_part/pallas_call | solution.py:241
  229.2 1.4 collective-permute-done.7.refs_2_
  230.5 2.7 last_part.1
  233.2 6.4 %all-to-all-start.2 = ((bf16[32,40,512]{2,1,0:T(8,128)(2,1)}), bf16[32,40,512]{2,1,0:T(8,128)(2,1)S(1)}, u32[]{:S(2)}, u32[]{:S(2)}) async-start(bf16[32,40,512]{2,1,0:T(8,128)(2,1)} %bitcast.35), calls=%async_computation.2 | async-start | bytes 2621440 | tf_op jit(solution)/shard_map/all_to_all | solution.py:21
  241.0 31.8 %all-to-all-done.2 = bf16[32,40,512]{2,1,0:T(8,128)(2,1)S(1)} async-done(((bf16[32,40,512]{2,1,0:T(8,128)(2,1)}), bf16[32,40,512]{2,1,0:T(8,128)(2,1)S(1)}, u32[]{:S(2)}, u32[]{:S(2)}) %all-to-all-start.2) | async-done | bytes 1310752 | tf_op jit(solution)/shard_map/all_to_all | solution.py:21
  273.5 1.4 fusion
  274.9 3.7 %all-to-all-start.3 = ((bf16[8,48,512]{2,1,0:T(8,128)(2,1)}), bf16[8,48,512]{2,1,0:T(8,128)(2,1)S(1)}, u32[]{:S(2)}, u32[]{:S(2)}) async-start(bf16[8,48,512]{2,1,0:T(8,128)(2,1)} %bitcast.16), calls=%async_computation.3 | async-start | bytes 786432 | tf_op jit(solution)/shard_map/all_to_all | solution.py:21
  279.8 49.4 %all-to-all-done.3 = bf16[8,48,512]{2,1,0:T(8,128)(2,1)S(1)} async-done(((bf16[8,48,512]{2,1,0:T(8,128)(2,1)}), bf16[8,48,512]{2,1,0:T(8,128)(2,1)S(1)}, u32[]{:S(2)}, u32[]{:S(2)}) %all-to-all-start.3) | async-done | bytes 393248 | tf_op jit(solution)/shard_map/all_to_all | solution.py:21
  (52 shorter events, 8.2 us)
Async XLA Ops:
  2.4 109.2 %copy-start.3 = (bf16[1,2048,256]{2,1,0:T(8,128)(2,1)S(1)}, bf16[1,2048,256]{2,1,0:T(8,128)(2,1)}, u32[]{:S(2)}) copy-start(bf16[1,2048,256]{2,1,0:T(8,128)(2,1)} %param.15) | copy-start | bytes 3145732
  2.4 109.2 %copy-start.4 = (bf16[1,2048,256]{2,1,0:T(8,128)(2,1)S(1)}, bf16[1,2048,256]{2,1,0:T(8,128)(2,1)}, u32[]{:S(2)}) copy-start(bf16[1,2048,256]{2,1,0:T(8,128)(2,1)} %param.16) | copy-start | bytes 3145732
  84.1 135.2 %all-to-all-start.1 = ((bf16[32,40,512]{2,1,0:T(8,128)(2,1)}), bf16[32,40,512]{2,1,0:T(8,128)(2,1)S(1)}, u32[]{:S(2)}, u32[]{:S(2)}) async-start(bf16[32,40,512]{2,1,0:T(8,128)(2,1)} %bitcast.42), calls=%async_computation.1 | async-start | bytes 2621440 | tf_op jit(solution)/shard_map/all_to_all | solution.py:21
  111.6 6.9 %copy-start.7 = (bf16[1,1024,512]{2,1,0:T(8,128)(2,1)S(1)}, bf16[1,1024,512]{2,1,0:T(8,128)(2,1)}, u32[]{:S(2)}) copy-start(bf16[1,1024,512]{2,1,0:T(8,128)(2,1)} %param.17) | copy-start | bytes 3145732
  111.8 60.7 %collective-permute-start = (bf16[2048,512]{1,0:T(8,128)(2,1)S(1)}, bf16[2048,512]{1,0:T(8,128)(2,1)S(1)}, u32[]{:S(2)}, u32[]{:S(2)}) collective-permute-start(bf16[2048,512]{1,0:T(8,128)(2,1)S(1)} %pad_maximum_fusion), channel_id=1, source_target_pairs={{0,3},{1,0},{2,1},{3,2},{4,7},{5,4},{6,5},{7,6},{8,11},{9,8},{10,9... | collective-permute-start | bytes 6291464 | tf_op jit(solution)/shard_map/ppermute | solution.py:26
  116.5 60.7 %collective-permute-start.1 = (bf16[2048,512]{1,0:T(8,128)(2,1)S(1)}, bf16[2048,512]{1,0:T(8,128)(2,1)S(1)}, u32[]{:S(2)}, u32[]{:S(2)}) collective-permute-start(bf16[2048,512]{1,0:T(8,128)(2,1)S(1)} %pad_maximum_fusion), channel_id=1, source_target_pairs={{0,1},{1,2},{2,3},{3,0},{4,5},{5,6},{6,7},{7,4},{8,9},{9,10},{10,1... | collective-permute-start | bytes 6291464 | tf_op jit(solution)/shard_map/ppermute | solution.py:26
  118.5 76.4 %collective-permute-start.4 = (bf16[1024,512]{1,0:T(8,128)(2,1)S(1)}, bf16[1024,512]{1,0:T(8,128)(2,1)S(1)}, u32[]{:S(2)}, u32[]{:S(2)}) collective-permute-start(bf16[1024,512]{1,0:T(8,128)(2,1)S(1)} %bitcast.46), channel_id=1, source_target_pairs={{0,3},{1,0},{2,1},{3,2},{4,7},{5,4},{6,5},{7,6},{8,11},{9,8},{10,9... | collective-permute-start | bytes 3145736 | tf_op jit(solution)/shard_map/ppermute | solution.py:26
  123.1 77.2 %collective-permute-start.5 = (bf16[1024,512]{1,0:T(8,128)(2,1)S(1)}, bf16[1024,512]{1,0:T(8,128)(2,1)S(1)}, u32[]{:S(2)}, u32[]{:S(2)}) collective-permute-start(bf16[1024,512]{1,0:T(8,128)(2,1)S(1)} %bitcast.47), channel_id=1, source_target_pairs={{0,1},{1,2},{2,3},{3,0},{4,5},{5,6},{6,7},{7,4},{8,9},{9,10},{10,1... | collective-permute-start | bytes 3145736 | tf_op jit(solution)/shard_map/ppermute | solution.py:26
  172.4 4.9 %copy-start.1 = (bf16[2048,512]{1,0:T(8,128)(2,1)}, bf16[2048,512]{1,0:T(8,128)(2,1)S(1)}, u32[]{:S(2)}) copy-start(bf16[2048,512]{1,0:T(8,128)(2,1)S(1)} %collective-permute-done.refs_3_) | copy-start | bytes 6291460
  172.5 30.7 %copy-start.10 = (f32[2048]{0:T(1024)S(1)}, f32[2048]{0:T(1024)}, u32[]{:S(2)}) copy-start(f32[2048]{0:T(1024)} %param.14) | copy-start | bytes 24580
  172.5 45.0 %collective-permute-start.2 = (bf16[1024,512]{1,0:T(8,128)(2,1)S(1)}, bf16[1024,512]{1,0:T(8,128)(2,1)}, u32[]{:S(2)}, u32[]{:S(2)}) collective-permute-start(bf16[1024,512]{1,0:T(8,128)(2,1)S(1)} %slice.68), channel_id=1, source_target_pairs={{0,3},{1,0},{2,1},{3,2},{4,7},{5,4},{6,5},{7,6},{8,11},{9,8},{10,9... | collective-permute-start | bytes 3145736 | tf_op jit(solution)/shard_map/ppermute | solution.py:26
  177.2 24.1 %copy-start.2 = (bf16[2048,512]{1,0:T(8,128)(2,1)}, bf16[2048,512]{1,0:T(8,128)(2,1)S(1)}, u32[]{:S(2)}) copy-start(bf16[2048,512]{1,0:T(8,128)(2,1)S(1)} %collective-permute-done.1.refs_4_) | copy-start | bytes 6291460
  177.3 42.0 %collective-permute-start.3 = (bf16[1024,512]{1,0:T(8,128)(2,1)S(1)}, bf16[1024,512]{1,0:T(8,128)(2,1)}, u32[]{:S(2)}, u32[]{:S(2)}) collective-permute-start(bf16[1024,512]{1,0:T(8,128)(2,1)S(1)} %slice.69), channel_id=1, source_target_pairs={{0,1},{1,2},{2,3},{3,0},{4,5},{5,6},{6,7},{7,4},{8,9},{9,10},{10,1... | collective-permute-start | bytes 3145736 | tf_op jit(solution)/shard_map/ppermute | solution.py:26
  194.9 8.3 %copy-start.5 = (bf16[1024,512]{1,0:T(8,128)(2,1)}, bf16[1024,512]{1,0:T(8,128)(2,1)S(1)}, u32[]{:S(2)}) copy-start(bf16[1024,512]{1,0:T(8,128)(2,1)S(1)} %collective-permute-done.4.refs_8_) | copy-start | bytes 3145732
  195.8 33.3 %collective-permute-start.6 = (bf16[512,512]{1,0:T(8,128)(2,1)}, bf16[512,512]{1,0:T(8,128)(2,1)}, u32[]{:S(2)}, u32[]{:S(2)}) collective-permute-start(bf16[512,512]{1,0:T(8,128)(2,1)} %slice.70), channel_id=1, source_target_pairs={{0,3},{1,0},{2,1},{3,2},{4,7},{5,4},{6,5},{7,6},{8,11},{9,8},{10,9... | collective-permute-start | bytes 1572872 | tf_op jit(solution)/shard_map/ppermute | solution.py:26
  200.4 2.9 copy-start.6
  201.3 29.3 %collective-permute-start.7 = (bf16[512,512]{1,0:T(8,128)(2,1)}, bf16[512,512]{1,0:T(8,128)(2,1)}, u32[]{:S(2)}, u32[]{:S(2)}) collective-permute-start(bf16[512,512]{1,0:T(8,128)(2,1)} %slice.71), channel_id=1, source_target_pairs={{0,1},{1,2},{2,3},{3,0},{4,5},{5,6},{6,7},{7,4},{8,9},{9,10},{10,1... | collective-permute-start | bytes 1572872 | tf_op jit(solution)/shard_map/ppermute | solution.py:26
  219.3 1.1 copy-start
  233.2 6.4 %copy-start.9 = (f32[2,8,128]{2,1,0:T(8,128)S(1)}, f32[2,8,128]{2,1,0:T(8,128)}, u32[]{:S(2)}) copy-start(f32[2,8,128]{2,1,0:T(8,128)} %get-tuple-element.25) | copy-start | bytes 24580
  233.2 6.7 %copy-start.11 = (s32[2,8,128]{2,1,0:T(8,128)S(1)}, s32[2,8,128]{2,1,0:T(8,128)}, u32[]{:S(2)}) copy-start(s32[2,8,128]{2,1,0:T(8,128)} %get-tuple-element.24) | copy-start | bytes 24580
  233.2 39.5 %all-to-all-start.2 = ((bf16[32,40,512]{2,1,0:T(8,128)(2,1)}), bf16[32,40,512]{2,1,0:T(8,128)(2,1)S(1)}, u32[]{:S(2)}, u32[]{:S(2)}) async-start(bf16[32,40,512]{2,1,0:T(8,128)(2,1)} %bitcast.35), calls=%async_computation.2 | async-start | bytes 2621440 | tf_op jit(solution)/shard_map/all_to_all | solution.py:21
  273.4 5.1 %copy-start.12 = (s32[1,384]{1,0:T(1,128)S(1)}, s32[1,384]{1,0:T(1,128)}, u32[]{:S(2)}) copy-start(s32[1,384]{1,0:T(1,128)} %get-tuple-element.17) | copy-start | bytes 4612
  273.5 5.1 %copy-start.8 = (s32[384]{0:T(512)S(1)}, s32[384]{0:T(512)}, u32[]{:S(2)}) copy-start(s32[384]{0:T(512)} %group.1) | copy-start | bytes 4612
  274.9 54.2 %all-to-all-start.3 = ((bf16[8,48,512]{2,1,0:T(8,128)(2,1)}), bf16[8,48,512]{2,1,0:T(8,128)(2,1)S(1)}, u32[]{:S(2)}, u32[]{:S(2)}) async-start(bf16[8,48,512]{2,1,0:T(8,128)(2,1)} %bitcast.16), calls=%async_computation.3 | async-start | bytes 786432 | tf_op jit(solution)/shard_map/all_to_all | solution.py:21

commit v10 on v9

--- a/solution.py
+++ b/solution.py
@@ -64,6 +64,29 @@
 
 def ones(condition):
     return jnp.where(condition, 1.0, 0.0).astype(jnp.bfloat16)
+
+
+def join(gate, up, joined, held, semaphores):
+    chunks = semaphores.shape[1]
+    units, count = gate.shape[1], gate.shape[0] // chunks
+    arriving = []
+    for c in range(chunks):
+        rows = pl.ds(c * count, count)
+        for i, side in enumerate((gate, up)):
+            slot = held.at[rows, pl.ds(i * units, units)]
+            copy = pltpu.make_async_copy(side.at[rows, :], slot, semaphores.at[i, c])
+            copy.start()
+            arriving.append(copy)
+    leaving = []
+    for c in range(chunks):
+        rows = pl.ds(c * count, count)
+        arriving[2 * c].wait()
+        arriving[2 * c + 1].wait()
+        copy = pltpu.make_async_copy(held.at[rows, :], joined.at[rows, :], semaphores.at[2, c])
+        copy.start()
+        leaving.append(copy)
+    for copy in leaving:
+        copy.wait()
 
 
 def depart(group, choice, group_share, expert_share, tokens, blocks, ranks):
@@ -167,12 +190,11 @@
     given, (hidden_out, results), (rows, *slots) = refs[:10], refs[10:12], refs[12:22]
     normed, hidden, pieces, semaphores, leaving = refs[22:]
     gate, up, one, three, top, bottom, *down = slots
-    arrived, *copies = fetch(given[:3], (rows, *slots[:2]), semaphores)
+    arrived, *copies = fetch(given, (rows, *slots), semaphores)
     parts, _, width = rows.shape
     units = gate.shape[1]
     total = None
     arrived.wait()
-    copies += fetch(given[3:], slots[2:], semaphores.at[pl.ds(3, len(given) - 3)])
     for t in range(parts):
         values = rows[t].astype(jnp.float32)
         squares = jnp.sum(values * values, -1, keepdims=True)
@@ -284,7 +306,16 @@
     chunks = piece_width // LANES
     depth = up_to(groups // tp_count * capacity, TILE)
 
-    gate_up_ring = around(jnp.concatenate([w_gate[0], w_up[0]], 1), "tp")
+    both = shaped((w_gate.shape[1], 2 * w_gate.shape[2]))
+    joined = pl.pallas_call(
+        join,
+        out_shape=both,
+        in_specs=[HBM, HBM],
+        out_specs=HBM,
+        scratch_shapes=slots_for([both]) + [pltpu.SemaphoreType.DMA((3, 4))],
+        name="join",
+    )(w_gate[0], w_up[0])
+    gate_up_ring = around(joined, "tp")
     down_ring = around(w_down[0], "tp")
 
     blocks, rank = pl.pallas_call(

time: 331 us -> 331 us (level)
  no operation moved by 1% of the time
where the time goes in v10:
time: 331 us; the launch traced here: 330 us
  waiting for transfers between devices  161 us (49%)
  blocking collectives  78.7 us (24%)
  starting transfers between devices  61.6 us (19%)
  Pallas kernels  18.8 us (6%)
  matrix products  4.37 us (1%)
  local copies, waits for them, and re-layouts  4.19 us (1%)
    all_to_all x3, waiting for transfers between devices, exchange(): return lax.all_to_all(array, axis, 0, 0, tiled=True)  81.2 us
    ppermute x8, waiting for transfers between devices, shifted(): lax.ppermute(array, axis, [(a, (a + by) % length) for a in range(length)])  80.2 us
    all_to_all x1, blocking collectives, exchange(): return lax.all_to_all(array, axis, 0, 0, tiled=True)  78.7 us
    all_to_all x3, starting transfers between devices, exchange(): return lax.all_to_all(array, axis, 0, 0, tiled=True)  36.2 us
    ppermute x8, starting transfers between devices, shifted(): lax.ppermute(array, axis, [(a, (a + by) % length) for a in range(length)])  25.4 us
    pallas_call x1, Pallas kernels, expert(): pl.pallas_call(main_part, out_shape=(whole, shaped((parts, count, width))...  8.47 us
  transfers between devices with their start and end apart: 11, of which 7 were waited for; matrix products, arithmetic and copies ran while one was open for 2% of the time, Pallas kernels for 3%

profile of v10, /device:TPU:33, one launch (start us, length us, event | category | flops | bytes accessed | tf_op | source)
XLA Modules:
  0.0 330.3 jit_solution(4595971002344669880)
XLA Ops:
  0.0 2.3 depart.1
  2.3 78.7 %all_to_all.20.landed = bf16[8,200,128]{2,1,0:T(8,128)(2,1)} all-to-all(bf16[8,200,128]{2,1,0:T(8,128)(2,1)} %get-tuple-element.18), channel_id=1, replica_groups=mesh['grp'=2,'g'=8,'m'=8,'tp'=4] {'g'}, dimensions={0} | all-to-all | bytes 819200 | tf_op jit(solution)/shard_map/all_to_all | solution.py:21
  81.0 2.9 arrive.1
  83.9 27.5 %all-to-all-start.1 = ((bf16[32,40,512]{2,1,0:T(8,128)(2,1)}), bf16[32,40,512]{2,1,0:T(8,128)(2,1)S(1)}, u32[]{:S(2)}, u32[]{:S(2)}) async-start(bf16[32,40,512]{2,1,0:T(8,128)(2,1)} %bitcast.42), calls=%async_computation.1 | async-start | bytes 2621440 | tf_op jit(solution)/shard_map/all_to_all | solution.py:21
  111.4 2.4 join.1
  113.9 4.6 %collective-permute-start = (bf16[2048,512]{1,0:T(8,128)(2,1)}, bf16[2048,512]{1,0:T(8,128)(2,1)S(1)}, u32[]{:S(2)}, u32[]{:S(2)}) collective-permute-start(bf16[2048,512]{1,0:T(8,128)(2,1)} %join.1), channel_id=1, source_target_pairs={{0,3},{1,0},{2,1},{3,2},{4,7},{5,4},{6,5},{7,6},{8,11},{9,8},{10,9... | collective-permute-start | bytes 6291464 | tf_op jit(solution)/shard_map/ppermute | solution.py:26
  118.5 2.0 collective-permute-start.1
  120.5 4.6 %collective-permute-start.4 = (bf16[1024,512]{1,0:T(8,128)(2,1)}, bf16[1024,512]{1,0:T(8,128)(2,1)S(1)}, u32[]{:S(2)}, u32[]{:S(2)}) collective-permute-start(bf16[1024,512]{1,0:T(8,128)(2,1)} %bitcast.7.refs_7_), channel_id=1, source_target_pairs={{0,3},{1,0},{2,1},{3,2},{4,7},{5,4},{6,5},{7,6},{8,11},{9,8},{10,9... | collective-permute-start | bytes 3145736 | tf_op jit(solution)/shard_map/ppermute | solution.py:26
  125.1 2.0 collective-permute-start.5
  127.0 45.2 %collective-permute-done.refs_3_ = bf16[2048,512]{1,0:T(8,128)(2,1)S(1)} collective-permute-done((bf16[2048,512]{1,0:T(8,128)(2,1)}, bf16[2048,512]{1,0:T(8,128)(2,1)S(1)}, u32[]{:S(2)}, u32[]{:S(2)}) %collective-permute-start) | collective-permute-done | bytes 2097184 | tf_op jit(solution)/shard_map/ppermute | solution.py:26
  172.4 4.1 %collective-permute-start.2 = (bf16[1024,512]{1,0:T(8,128)(2,1)S(1)}, bf16[1024,512]{1,0:T(8,128)(2,1)}, u32[]{:S(2)}, u32[]{:S(2)}) collective-permute-start(bf16[1024,512]{1,0:T(8,128)(2,1)S(1)} %slice.68), channel_id=1, source_target_pairs={{0,3},{1,0},{2,1},{3,2},{4,7},{5,4},{6,5},{7,6},{8,11},{9,8},{10,9... | collective-permute-start | bytes 3145736 | tf_op jit(solution)/shard_map/ppermute | solution.py:26
  176.6 2.1 collective-permute-start.3
  178.7 16.0 %collective-permute-done.4.refs_8_ = bf16[1024,512]{1,0:T(8,128)(2,1)S(1)} collective-permute-done((bf16[1024,512]{1,0:T(8,128)(2,1)}, bf16[1024,512]{1,0:T(8,128)(2,1)S(1)}, u32[]{:S(2)}, u32[]{:S(2)}) %collective-permute-start.4) | collective-permute-done | bytes 1048608 | tf_op jit(solution)/shard_map/ppermute | solution.py:26
  195.7 4.0 %collective-permute-start.6 = (bf16[512,512]{1,0:T(8,128)(2,1)}, bf16[512,512]{1,0:T(8,128)(2,1)}, u32[]{:S(2)}, u32[]{:S(2)}) collective-permute-start(bf16[512,512]{1,0:T(8,128)(2,1)} %slice.70), channel_id=1, source_target_pairs={{0,3},{1,0},{2,1},{3,2},{4,7},{5,4},{6,5},{7,6},{8,11},{9,8},{10,9... | collective-permute-start | bytes 1572872 | tf_op jit(solution)/shard_map/ppermute | solution.py:26
  200.6 2.1 collective-permute-start.7
  203.3 14.0 %collective-permute-done.2.refs_5_ = bf16[1024,512]{1,0:T(8,128)(2,1)} collective-permute-done((bf16[1024,512]{1,0:T(8,128)(2,1)S(1)}, bf16[1024,512]{1,0:T(8,128)(2,1)}, u32[]{:S(2)}, u32[]{:S(2)}) %collective-permute-start.2) | collective-permute-done | bytes 1048608 | tf_op jit(solution)/shard_map/ppermute | solution.py:26
  217.3 3.3 collective-permute-done.3.refs_6_
  221.7 8.5 %main_part.1 = (bf16[320,1024]{1,0:T(8,128)(2,1)}, bf16[4,320,512]{2,1,0:T(8,128)(2,1)}) custom-call(s32[1]{0:T(128)} %bitcast.2.me, f32[4,512]{1,0:T(4,128)} %reshape.34.gains, bf16[4,320,512]{2,1,0:T(8,128)(2,1)} %bitcast.36, bf16[2048,256]{1,0:T(8,128)(2,1)} %bitcast.38, bf16[2048,256]{1,0:T(8,128)(2,1)} %bitcast.40, bf16[2048,512]{1,0:T(8,128)(2,1)} %copy-done.1, ...), custom_call_target="tpu_custom_call" | custom-call | tf_op jit(solution)/shard_map/main_part/pallas_call | solution.py:263
  230.2 1.6 collective-permute-done.7.refs_2_
  231.9 2.7 last_part.1
  234.6 5.1 %all-to-all-start.2 = ((bf16[32,40,512]{2,1,0:T(8,128)(2,1)}), bf16[32,40,512]{2,1,0:T(8,128)(2,1)S(1)}, u32[]{:S(2)}, u32[]{:S(2)}) async-start(bf16[32,40,512]{2,1,0:T(8,128)(2,1)} %bitcast.35), calls=%async_computation.2 | async-start | bytes 2621440 | tf_op jit(solution)/shard_map/all_to_all | solution.py:21
  241.0 31.8 %all-to-all-done.2 = bf16[32,40,512]{2,1,0:T(8,128)(2,1)S(1)} async-done(((bf16[32,40,512]{2,1,0:T(8,128)(2,1)}), bf16[32,40,512]{2,1,0:T(8,128)(2,1)S(1)}, u32[]{:S(2)}, u32[]{:S(2)}) %all-to-all-start.2) | async-done | bytes 1310752 | tf_op jit(solution)/shard_map/all_to_all | solution.py:21
  274.9 3.7 %all-to-all-start.3 = ((bf16[8,48,512]{2,1,0:T(8,128)(2,1)}), bf16[8,48,512]{2,1,0:T(8,128)(2,1)S(1)}, u32[]{:S(2)}, u32[]{:S(2)}) async-start(bf16[8,48,512]{2,1,0:T(8,128)(2,1)} %bitcast.16), calls=%async_computation.3 | async-start | bytes 786432 | tf_op jit(solution)/shard_map/all_to_all | solution.py:21
  279.8 49.4 %all-to-all-done.3 = bf16[8,48,512]{2,1,0:T(8,128)(2,1)S(1)} async-done(((bf16[8,48,512]{2,1,0:T(8,128)(2,1)}), bf16[8,48,512]{2,1,0:T(8,128)(2,1)S(1)}, u32[]{:S(2)}, u32[]{:S(2)}) %all-to-all-start.3) | async-done | bytes 393248 | tf_op jit(solution)/shard_map/all_to_all | solution.py:21
  (46 shorter events, 9.4 us)
Async XLA Ops:
  83.9 136.7 %all-to-all-start.1 = ((bf16[32,40,512]{2,1,0:T(8,128)(2,1)}), bf16[32,40,512]{2,1,0:T(8,128)(2,1)S(1)}, u32[]{:S(2)}, u32[]{:S(2)}) async-start(bf16[32,40,512]{2,1,0:T(8,128)(2,1)} %bitcast.42), calls=%async_computation.1 | async-start | bytes 2621440 | tf_op jit(solution)/shard_map/all_to_all | solution.py:21
  113.9 58.4 %collective-permute-start = (bf16[2048,512]{1,0:T(8,128)(2,1)}, bf16[2048,512]{1,0:T(8,128)(2,1)S(1)}, u32[]{:S(2)}, u32[]{:S(2)}) collective-permute-start(bf16[2048,512]{1,0:T(8,128)(2,1)} %join.1), channel_id=1, source_target_pairs={{0,3},{1,0},{2,1},{3,2},{4,7},{5,4},{6,5},{7,6},{8,11},{9,8},{10,9... | collective-permute-start | bytes 6291464 | tf_op jit(solution)/shard_map/ppermute | solution.py:26
  118.5 58.0 %collective-permute-start.1 = (bf16[2048,512]{1,0:T(8,128)(2,1)}, bf16[2048,512]{1,0:T(8,128)(2,1)S(1)}, u32[]{:S(2)}, u32[]{:S(2)}) collective-permute-start(bf16[2048,512]{1,0:T(8,128)(2,1)} %join.1), channel_id=1, source_target_pairs={{0,1},{1,2},{2,3},{3,0},{4,5},{5,6},{6,7},{7,4},{8,9},{9,10},{10,1... | collective-permute-start | bytes 6291464 | tf_op jit(solution)/shard_map/ppermute | solution.py:26
  120.5 74.3 %collective-permute-start.4 = (bf16[1024,512]{1,0:T(8,128)(2,1)}, bf16[1024,512]{1,0:T(8,128)(2,1)S(1)}, u32[]{:S(2)}, u32[]{:S(2)}) collective-permute-start(bf16[1024,512]{1,0:T(8,128)(2,1)} %bitcast.7.refs_7_), channel_id=1, source_target_pairs={{0,3},{1,0},{2,1},{3,2},{4,7},{5,4},{6,5},{7,6},{8,11},{9,8},{10,9... | collective-permute-start | bytes 3145736 | tf_op jit(solution)/shard_map/ppermute | solution.py:26
  125.1 74.6 %collective-permute-start.5 = (bf16[1024,512]{1,0:T(8,128)(2,1)}, bf16[1024,512]{1,0:T(8,128)(2,1)S(1)}, u32[]{:S(2)}, u32[]{:S(2)}) collective-permute-start(bf16[1024,512]{1,0:T(8,128)(2,1)} %bitcast.7.refs_7_), channel_id=1, source_target_pairs={{0,1},{1,2},{2,3},{3,0},{4,5},{5,6},{6,7},{7,4},{8,9},{9,10},{10,1... | collective-permute-start | bytes 3145736 | tf_op jit(solution)/shard_map/ppermute | solution.py:26
  172.3 4.3 %copy-start.1 = (bf16[2048,512]{1,0:T(8,128)(2,1)}, bf16[2048,512]{1,0:T(8,128)(2,1)S(1)}, u32[]{:S(2)}) copy-start(bf16[2048,512]{1,0:T(8,128)(2,1)S(1)} %collective-permute-done.refs_3_) | copy-start | bytes 6291460
  172.4 30.3 %copy-start.7 = (f32[2048]{0:T(1024)S(1)}, f32[2048]{0:T(1024)}, u32[]{:S(2)}) copy-start(f32[2048]{0:T(1024)} %param.14) | copy-start | bytes 24580
  172.4 45.0 %collective-permute-start.2 = (bf16[1024,512]{1,0:T(8,128)(2,1)S(1)}, bf16[1024,512]{1,0:T(8,128)(2,1)}, u32[]{:S(2)}, u32[]{:S(2)}) collective-permute-start(bf16[1024,512]{1,0:T(8,128)(2,1)S(1)} %slice.68), channel_id=1, source_target_pairs={{0,3},{1,0},{2,1},{3,2},{4,7},{5,4},{6,5},{7,6},{8,11},{9,8},{10,9... | collective-permute-start | bytes 3145736 | tf_op jit(solution)/shard_map/ppermute | solution.py:26
  176.5 24.1 %copy-start.2 = (bf16[2048,512]{1,0:T(8,128)(2,1)}, bf16[2048,512]{1,0:T(8,128)(2,1)S(1)}, u32[]{:S(2)}) copy-start(bf16[2048,512]{1,0:T(8,128)(2,1)S(1)} %collective-permute-done.1.refs_4_) | copy-start | bytes 6291460
  176.6 44.0 %collective-permute-start.3 = (bf16[1024,512]{1,0:T(8,128)(2,1)S(1)}, bf16[1024,512]{1,0:T(8,128)(2,1)}, u32[]{:S(2)}, u32[]{:S(2)}) collective-permute-start(bf16[1024,512]{1,0:T(8,128)(2,1)S(1)} %slice.69), channel_id=1, source_target_pairs={{0,1},{1,2},{2,3},{3,0},{4,5},{5,6},{6,7},{7,4},{8,9},{9,10},{10,1... | collective-permute-start | bytes 3145736 | tf_op jit(solution)/shard_map/ppermute | solution.py:26
  194.8 7.9 %copy-start.3 = (bf16[1024,512]{1,0:T(8,128)(2,1)}, bf16[1024,512]{1,0:T(8,128)(2,1)S(1)}, u32[]{:S(2)}) copy-start(bf16[1024,512]{1,0:T(8,128)(2,1)S(1)} %collective-permute-done.4.refs_8_) | copy-start | bytes 3145732
  195.7 34.5 %collective-permute-start.6 = (bf16[512,512]{1,0:T(8,128)(2,1)}, bf16[512,512]{1,0:T(8,128)(2,1)}, u32[]{:S(2)}, u32[]{:S(2)}) collective-permute-start(bf16[512,512]{1,0:T(8,128)(2,1)} %slice.70), channel_id=1, source_target_pairs={{0,3},{1,0},{2,1},{3,2},{4,7},{5,4},{6,5},{7,6},{8,11},{9,8},{10,9... | collective-permute-start | bytes 1572872 | tf_op jit(solution)/shard_map/ppermute | solution.py:26
  199.7 3.0 copy-start.4
  200.6 31.3 %collective-permute-start.7 = (bf16[512,512]{1,0:T(8,128)(2,1)}, bf16[512,512]{1,0:T(8,128)(2,1)}, u32[]{:S(2)}, u32[]{:S(2)}) collective-permute-start(bf16[512,512]{1,0:T(8,128)(2,1)} %slice.71), channel_id=1, source_target_pairs={{0,1},{1,2},{2,3},{3,0},{4,5},{5,6},{6,7},{7,4},{8,9},{9,10},{10,1... | collective-permute-start | bytes 1572872 | tf_op jit(solution)/shard_map/ppermute | solution.py:26
  220.6 1.1 copy-start
  234.5 5.1 %copy-start.6 = (f32[2,8,128]{2,1,0:T(8,128)S(1)}, f32[2,8,128]{2,1,0:T(8,128)}, u32[]{:S(2)}) copy-start(f32[2,8,128]{2,1,0:T(8,128)} %get-tuple-element.25) | copy-start | bytes 24580
  234.6 5.4 %copy-start.8 = (s32[2,8,128]{2,1,0:T(8,128)S(1)}, s32[2,8,128]{2,1,0:T(8,128)}, u32[]{:S(2)}) copy-start(s32[2,8,128]{2,1,0:T(8,128)} %get-tuple-element.24) | copy-start | bytes 24580
  234.6 38.2 %all-to-all-start.2 = ((bf16[32,40,512]{2,1,0:T(8,128)(2,1)}), bf16[32,40,512]{2,1,0:T(8,128)(2,1)S(1)}, u32[]{:S(2)}, u32[]{:S(2)}) async-start(bf16[32,40,512]{2,1,0:T(8,128)(2,1)} %bitcast.35), calls=%async_computation.2 | async-start | bytes 2621440 | tf_op jit(solution)/shard_map/all_to_all | solution.py:21
  273.5 5.1 %copy-start.9 = (s32[1,384]{1,0:T(1,128)S(1)}, s32[1,384]{1,0:T(1,128)}, u32[]{:S(2)}) copy-start(s32[1,384]{1,0:T(1,128)} %get-tuple-element.17) | copy-start | bytes 4612
  273.5 5.1 %copy-start.5 = (s32[384]{0:T(512)S(1)}, s32[384]{0:T(512)}, u32[]{:S(2)}) copy-start(s32[384]{0:T(512)} %group.1) | copy-start | bytes 4612
  274.9 54.2 %all-to-all-start.3 = ((bf16[8,48,512]{2,1,0:T(8,128)(2,1)}), bf16[8,48,512]{2,1,0:T(8,128)(2,1)S(1)}, u32[]{:S(2)}, u32[]{:S(2)}) async-start(bf16[8,48,512]{2,1,0:T(8,128)(2,1)} %bitcast.16), calls=%async_computation.3 | async-start | bytes 786432 | tf_op jit(solution)/shard_map/all_to_all | solution.py:21
